TPU v7x, 32 devices: a whole 2x2x4 slice. The times are simulated.
32 devices in a mesh: fs: 8 (over z, x), tp: 4 (over y, core).
Axes of the slice: x: 2, y: 2, z: 4, core: 2. Of those that a mesh axis runs over, the one named last changes fastest.
Arguments:
- inputs: bfloat16 [1024, 2048], P('fs', 'tp'), may hold values from -6 to 6
- query_grad: bfloat16 [1024, 1024], P('fs', 'tp'), may hold values from -6 to 6
- forget_grad: bfloat16 [1024, 1024], P('fs', 'tp'), may hold values from -6 to 6
- forget_pre: bfloat16 [1024, 1024], P('fs', 'tp'), may hold values from -8 to 8
- lower_bound: float32 [1024], P('tp'), may hold values from 0.1 to 0.9
- query_weight: float32 [2048, 1024], P('fs', 'tp'), may hold values from -0.125 to 0.125
- forget_weight: float32 [2048, 1024], P('fs', 'tp'), may hold values from -0.125 to 0.125
- query_moment: float32 [2048, 1024], P('fs', 'tp'), may hold values from -6 to 6
- forget_moment: float32 [2048, 1024], P('fs', 'tp'), may hold values from -6 to 6
- query_rows: float32 [2048, 2048], P('fs'), may hold values from -0.6 to 0.6
- forget_rows: float32 [2048, 2048], P('fs'), may hold values from -0.6 to 0.6
- query_cols: float32 [8, 128, 128], P('tp'), may hold values from -0.6 to 0.6
- forget_cols: float32 [8, 128, 128], P('tp'), may hold values from -0.6 to 0.6
- query_row_root: bfloat16 [2048, 2048], P('fs'), may hold values from -2 to 2, as said below
- forget_row_root: bfloat16 [2048, 2048], P('fs'), may hold values from -2 to 2, as said below
- query_col_root: bfloat16 [8, 128, 128], P('tp'), may hold values from -2 to 2, as said below
- forget_col_root: bfloat16 [8, 128, 128], P('tp'), may hold values from -2 to 2, as said below
Outputs:
- query_master: float32 [2048, 1024], P('fs', 'tp')
- forget_master: float32 [2048, 1024], P('fs', 'tp')
- query_copy: bfloat16 [2048, 1024], P('fs', 'tp')
- forget_copy: bfloat16 [2048, 1024], P('fs', 'tp')
- query_step: float32 [2048, 1024], P('fs', 'tp')
- forget_step: float32 [2048, 1024], P('fs', 'tp')
- query_moment_next: float32 [2048, 1024], P('fs', 'tp')
- forget_moment_next: float32 [2048, 1024], P('fs', 'tp')
- query_rows_next: float32 [2048, 2048], P('fs')
- forget_rows_next: float32 [2048, 2048], P('fs')
- query_cols_next: float32 [8, 128, 128], P('tp')
- forget_cols_next: float32 [8, 128, 128], P('tp')
Inputs may be any that keep to these rules, and one draw needn't show every extreme that they name: `query_row_root`: diagonal entries 0.5 to 1.5, the others of order 2048 ** -0.5. `forget_row_root`: diagonal entries 0.5 to 1.5, the others of order 2048 ** -0.5. `query_col_root`: diagonal entries 0.5 to 1.5, the others of order 128 ** -0.5. `forget_col_root`: diagonal entries 0.5 to 1.5, the others of order 128 ** -0.5.
All inputs are finite; a program needn't handle non-finite values.
Results may differ from a plain program's by a relative error of at most 0.005.
Values may be sent and summed in bfloat16 or wider, within the bound.
No kernel may reach another device: no remote copies, remote signals or barrier semaphores. Data moves between devices by JAX's collectives and lax.ppermute only.
A program may use at most 64 MiB of HBM per device.

v0:
```python
from functools import partial

import jax
import jax.numpy as jnp
from jax import lax
from jax.experimental import pallas as pl
from jax.experimental.pallas import tpu as pltpu
from jax.sharding import PartitionSpec as P


D = 2048
HW = 1024
HEAD = 128


stat_decay = 0.9
moment_decay = 0.9
learn_rate = 0.02
highest = lax.Precision.HIGHEST


def fold_one(carry_state, shard_piece, offset, root_mine, grad_mine):
    left_sum, outer_rows, column_total = carry_state
    row_count, col_width = shard_piece.shape
    left_sum = left_sum + jnp.dot(root_mine, shard_piece, precision=highest)
    outer_piece = lax.dot_general(
        grad_mine, shard_piece, (((1,), (1,)), ((), ())), precision=highest
    )
    outer_rows = lax.dynamic_update_slice_in_dim(outer_rows, outer_piece, offset, 1)
    by_head = shard_piece.reshape(row_count, col_width // HEAD, HEAD)
    column_total = column_total + jnp.einsum("rhi,rhj->hij", by_head, by_head, precision=highest)
    return (left_sum, outer_rows, column_total)


def finish(weight, moment, rows, cols, col_root, left_sum, outer_rows, column_total, square):
    norm_scale = jnp.sqrt(D * HW / (square + 1.0))
    scale_twice = norm_scale * norm_scale
    rows_next = stat_decay * rows + (1.0 - stat_decay) / HW * scale_twice * outer_rows
    cols_next = stat_decay * cols + (1.0 - stat_decay) / D * scale_twice * column_total
    shard_rows, col_width = left_sum.shape
    shaped = left_sum.reshape(shard_rows, col_width // HEAD, HEAD)
    precond = norm_scale * jnp.einsum(
        "rhi,hij->rhj", shaped, col_root.astype(jnp.float32), precision=highest
    ).reshape(shard_rows, col_width)
    moment_next = moment_decay * moment + (1.0 - moment_decay) * precond
    update_step = moment_decay * moment_next + (1.0 - moment_decay) * precond
    master = weight - learn_rate * update_step
    return (master, master.astype(jnp.bfloat16), update_step, moment_next, rows_next, cols_next)


def summed_plan(
    inputs,
    query_grad,
    forget_cot,
    query_weight,
    forget_weight,
    query_moment,
    forget_moment,
    query_rows,
    forget_rows,
    query_cols,
    forget_cols,
    query_row_root,
    forget_row_root,
    query_col_root,
    forget_col_root,
):
    gathered = lax.all_gather(inputs, "tp", axis=1, tiled=True)
    shard_rows, col_width = query_weight.shape
    heads_here = col_width // HEAD
    row_roots = (query_row_root.astype(jnp.float32), forget_row_root.astype(jnp.float32))
    empty = (
        jnp.zeros((shard_rows, col_width), jnp.float32),
        jnp.zeros((shard_rows, D), jnp.float32),
        jnp.zeros((heads_here, HEAD, HEAD), jnp.float32),
    )
    joined = jnp.concatenate([query_grad, forget_cot], axis=1)
    summed = lax.psum_scatter(
        lax.dot_general(
            gathered, joined, (((0,), (0,)), ((), ())), preferred_element_type=jnp.float32
        ),
        "fs",
        scatter_dimension=0,
        tiled=True,
    )
    gradients = (summed[:, :col_width], summed[:, col_width:])
    offset = jnp.int32(0)
    results = (
        fold_one(
            empty,
            lax.all_gather(gradients[0].astype(jnp.bfloat16), "fs", axis=0, tiled=True).astype(
                jnp.float32
            ),
            offset,
            row_roots[0],
            gradients[0],
        ),
        fold_one(
            empty,
            lax.all_gather(gradients[1].astype(jnp.bfloat16), "fs", axis=0, tiled=True).astype(
                jnp.float32
            ),
            offset,
            row_roots[1],
            gradients[1],
        ),
    )
    query_trace = jnp.sum(jnp.diagonal(results[0][2], axis1=1, axis2=2))
    forget_trace = jnp.sum(jnp.diagonal(results[1][2], axis1=1, axis2=2))
    query_outer, forget_outer, query_square, forget_square = (
        lax.psum(results[0][1].astype(jnp.bfloat16), "tp").astype(jnp.float32),
        lax.psum(results[1][1].astype(jnp.bfloat16), "tp").astype(jnp.float32),
        lax.psum(query_trace.astype(jnp.bfloat16), "tp").astype(jnp.float32),
        lax.psum(forget_trace.astype(jnp.bfloat16), "tp").astype(jnp.float32),
    )
    query_out = finish(
        query_weight,
        query_moment,
        query_rows,
        query_cols,
        query_col_root,
        results[0][0],
        query_outer,
        results[0][2],
        query_square,
    )
    forget_out = finish(
        forget_weight,
        forget_moment,
        forget_rows,
        forget_cols,
        forget_col_root,
        results[1][0],
        forget_outer,
        results[1][2],
        forget_square,
    )
    return (
        query_out[0],
        forget_out[0],
        query_out[1],
        forget_out[1],
        query_out[2],
        forget_out[2],
        query_out[3],
        forget_out[3],
        query_out[4],
        forget_out[4],
        query_out[5],
        forget_out[5],
    )


def linear_pairs(fs_size, tp_size, target):
    pairs = []
    for f in range(fs_size):
        for t in range(tp_size):
            to_f, to_t = target(f, t)
            pairs.append((f * tp_size + t, to_f * tp_size + to_t))
    return pairs


def gather_operands(x_block, y_block, fs_size, tp_size):
    axes = ("fs", "tp")

    def move(value, target):
        return lax.ppermute(value, axes, linear_pairs(fs_size, tp_size, target))

    odd = lax.axis_index("tp") % 2 == 1

    def partner(f, t):
        return (f, t ^ 1)

    def first_hop(f, t):
        return (f ^ 1, t) if t % 2 == 0 else (f, t ^ 2)

    def second_hop(f, t):
        return (f, t ^ 2) if t % 2 == 0 else (f ^ 1, t)

    swapped = move(jnp.where(odd, x_block, y_block), partner)
    lanes = [jnp.stack([jnp.where(odd, swapped, x_block), jnp.where(odd, y_block, swapped)])]
    for k in range(1, fs_size // 2):
        step = k & -k if k & (k - 1) == 0 else k & (k - 1) ^ k
        source = lanes[k ^ step]
        lanes.append(move(source, lambda f, t, step=step: (f ^ (2 * step), t)))
    sets = []
    for lane in lanes:
        pair = jnp.stack([lane, move(lane, first_hop)])
        far = move(pair, second_hop)
        sets.append((pair, far, move(pair, partner), move(far, partner)))
    return sets


def assemble(place, pieces, x_set, y_set, sem):
    odd, upper = place[0], place[1]
    tokens, width = pieces[0].shape[2:]
    own = width // 2
    hidden = y_set.shape[1] // 2

    def copies(x_pieces, y_pieces):
        for p in range(2):
            rows = pl.ds(p * tokens, tokens)
            for h in range(2):
                for c in range(2):
                    col = pl.multiple_of(((upper ^ h) * 2 + c) * width, width)
                    pltpu.make_async_copy(
                        x_pieces[h].at[p, c], x_set.at[rows, pl.ds(col, width)], sem.at[0]
                    ).start()
                    for i in range(2):
                        pltpu.make_async_copy(
                            y_pieces[p].at[h, c, :, pl.ds(i * own, own)],
                            y_set.at[rows, pl.ds(i * hidden + (2 * h + c) * own, own)],
                            sem.at[1],
                        ).start()

    pair, far, pair_other, far_other = pieces

    @pl.when(odd == 0)
    def _():
        copies((pair, far), (pair_other, far_other))

    @pl.when(odd == 1)
    def _():
        copies((pair_other, far_other), (pair, far))


def assembled(x_set, y_set, sem):
    for k, whole in enumerate((x_set, y_set)):
        pltpu.make_async_copy(whole, whole, sem.at[k]).wait()


def chunk_product(x_set, y_set, m, n, rows, chunk):
    at = pl.multiple_of(m * rows, rows)
    return lax.dot_general(
        x_set[:, pl.ds(at, rows)],
        y_set[:, n * chunk : (n + 1) * chunk],
        (((0,), (0,)), ((), ())),
        preferred_element_type=jnp.float32,
    )


def sum_kernel(first, place, *refs):
    pieces, refs = refs[:4], refs[4:]
    if not first:
        refs = refs[1:]
    acc, x_set, y_set, sem = refs
    assemble(place, pieces, x_set, y_set, sem)
    assembled(x_set, y_set, sem)
    model, total = acc.shape
    rows = pieces[0].shape[3] // 2
    chunk = total // 4

    def product(m, carry):
        at = pl.multiple_of(m * rows, rows)
        for n in range(total // chunk):
            cols = slice(n * chunk, (n + 1) * chunk)
            part = chunk_product(x_set, y_set, m, n, rows, chunk)
            acc[pl.ds(at, rows), cols] = part if first else acc[pl.ds(at, rows), cols] + part
        return carry

    lax.fori_loop(0, model // rows, product, 0)


def tail_kernel(place, *refs):
    pieces, acc, refs = refs[:4], refs[4], refs[5:]
    sides = [refs[6 * i : 6 * i + 6] for i in range(2)]
    refs = refs[12:]
    outs = [refs[6 * i : 6 * i + 6] for i in range(2)]
    refs = refs[12:]
    x_set, y_set, grad, sem, load_sem, store_sem = refs[:6]
    held = [refs[6 + 10 * i : 16 + 10 * i] for i in range(2)]
    odd, band = place[0], place[2]
    model, total = grad.shape
    hidden = total // 2
    own = pieces[0].shape[3] // 2
    rows_here = held[0][0].shape[0]

    assemble(place, pieces, x_set, y_set, sem)
    loads = [
        [
            pltpu.make_async_copy(src, dst, load_sem.at[i, j])
            for j, (src, dst) in enumerate(zip(sides[i], held[i][:6], strict=True))
        ]
        for i in range(2)
    ]
    for side in loads:
        for copy in side:
            copy.start()
    assembled(x_set, y_set, sem)

    chunk = hidden // 2

    def product(m, squares):
        at = pl.multiple_of(m * rows_here, rows_here)
        squares = list(squares)
        for n in range(total // chunk):
            cols = slice(n * chunk, (n + 1) * chunk)
            part = acc[pl.ds(at, rows_here), cols] + chunk_product(
                x_set, y_set, m, n, rows_here, chunk
            )
            grad[pl.ds(at, rows_here), cols] = part.astype(jnp.bfloat16)
            i = n * chunk // hidden
            squares[i] = squares[i] + jnp.sum((part * part).reshape(-1, 8, chunk), axis=0)
        return tuple(squares)

    zero = jnp.zeros((8, chunk), jnp.float32)
    squares = lax.fori_loop(0, model // rows_here, product, (zero, zero))

    stores = []
    first = pl.multiple_of(band * rows_here, rows_here)
    for i in range(2):
        rows, row_root, weight, moment, cols, col_root = held[i][:6]
        master_out, copy_out, step_out, moment_out = held[i][6:]
        for copy in loads[i]:
            copy.wait()
        square = jnp.sum(squares[i], keepdims=True)
        scale = jnp.sqrt(model * hidden / (square + 1.0))
        twice = scale * scale
        mine = pl.multiple_of(i * hidden + odd * own, own)
        band_grad = grad[pl.ds(first, rows_here), i * hidden : (i + 1) * hidden]
        row_factor = (1.0 - stat_decay) / hidden * twice

        def outer(n, carry):
            at = pl.multiple_of(n * rows_here, rows_here)
            part = lax.dot_general(
                band_grad,
                grad[pl.ds(at, rows_here), i * hidden : (i + 1) * hidden],
                (((1,), (1,)), ((), ())),
                preferred_element_type=jnp.float32,
            )
            rows[:, pl.ds(at, rows_here)] = (
                stat_decay * rows[:, pl.ds(at, rows_here)] + row_factor * part
            )
            return carry

        lax.fori_loop(0, model // rows_here, outer, 0)
        stores.append(pltpu.make_async_copy(rows, outs[i][4], store_sem.at[i, 4]))
        stores[-1].start()
        own_grad = grad[:, pl.ds(mine, own)]
        column_total = lax.dot_general(
            own_grad, own_grad, (((0,), (0,)), ((), ())), preferred_element_type=jnp.float32
        )
        left = jnp.dot(row_root[...], own_grad, preferred_element_type=jnp.float32)
        left_high = left.astype(jnp.bfloat16)
        left_low = (left - left_high.astype(jnp.float32)).astype(jnp.bfloat16)
        for h in range(own // HEAD):
            at = slice(h * HEAD, (h + 1) * HEAD)
            cols[h] = (
                stat_decay * cols[h]
                + (1.0 - stat_decay) / model * twice * column_total[at, at]
            )
            root = col_root[h]
            precond = scale * (
                jnp.dot(left_high[:, at], root, preferred_element_type=jnp.float32)
                + jnp.dot(left_low[:, at], root, preferred_element_type=jnp.float32)
            )
            moment_next = moment_decay * moment[:, at] + (1.0 - moment_decay) * precond
            update_step = moment_decay * moment_next + (1.0 - moment_decay) * precond
            master = weight[:, at] - learn_rate * update_step
            master_out[:, at] = master
            copy_out[:, at] = master.astype(jnp.bfloat16)
            step_out[:, at] = update_step
            moment_out[:, at] = moment_next
        for src, dst in ((master_out, 0), (copy_out, 1), (step_out, 2), (moment_out, 3), (cols, 5)):
            stores.append(pltpu.make_async_copy(src, outs[i][dst], store_sem.at[i, dst]))
            stores[-1].start()
    for copy in stores:
        copy.wait()


def gathered_plan(
    inputs,
    query_grad,
    forget_cot,
    query_weight,
    forget_weight,
    query_moment,
    forget_moment,
    query_rows,
    forget_rows,
    query_cols,
    forget_cols,
    query_row_root,
    forget_row_root,
    query_col_root,
    forget_col_root,
    fs_size,
    tp_size,
):
    sets = gather_operands(
        inputs, jnp.concatenate([query_grad, forget_cot], axis=1), fs_size, tp_size
    )
    tp_at = lax.axis_index("tp")
    place = jnp.stack([tp_at % 2, tp_at // 2, lax.axis_index("fs")]).astype(jnp.int32)
    model = inputs.shape[1] * tp_size
    total = 2 * query_grad.shape[1] * tp_size
    sides = (
        (query_rows, query_row_root, query_weight, query_moment, query_cols, query_col_root),
        (forget_rows, forget_row_root, forget_weight, forget_moment, forget_cols, forget_col_root),
    )
    wide = jax.ShapeDtypeStruct(query_weight.shape, jnp.float32)
    narrow = jax.ShapeDtypeStruct(query_weight.shape, jnp.bfloat16)
    row_kind = jax.ShapeDtypeStruct(query_rows.shape, jnp.float32)
    col_kind = jax.ShapeDtypeStruct(query_cols.shape, jnp.float32)
    kinds = (wide, narrow, wide, wide, row_kind, col_kind)
    held = []
    for side in sides:
        held += [pltpu.VMEM(v.shape, v.dtype) for v in side]
        held += [pltpu.VMEM(k.shape, k.dtype) for k in kinds[:4]]
    anywhere = pl.BlockSpec(memory_space=pl.ANY)
    hbm = pl.BlockSpec(memory_space=pltpu.HBM)
    vmem = pl.BlockSpec(memory_space=pltpu.VMEM)
    smem = pl.BlockSpec(memory_space=pltpu.SMEM)
    set_scratch = [
        pltpu.VMEM((2 * inputs.shape[0], model), jnp.bfloat16),
        pltpu.VMEM((2 * inputs.shape[0], total), jnp.bfloat16),
    ]
    params = pltpu.CompilerParams(vmem_limit_bytes=26 * 2**20)
    acc = []
    for pieces in sets[:-1]:
        acc = [
            pl.pallas_call(
                partial(sum_kernel, not acc),
                out_shape=pltpu.VMEM((model, total), jnp.float32),
                in_specs=[smem] + [anywhere] * 4 + [vmem] * len(acc),
                out_specs=vmem,
                scratch_shapes=set_scratch + [pltpu.SemaphoreType.DMA((2,))],
                input_output_aliases={5: 0} if acc else {},
                compiler_params=params,
            )(place, *pieces, *acc)
        ]
    operands = [*sets[-1], pltpu.with_memory_space_constraint(*acc, pltpu.VMEM)]
    operands += [pltpu.with_memory_space_constraint(v, pltpu.HBM) for side in sides for v in side]
    out = pl.pallas_call(
        tail_kernel,
        out_shape=kinds * 2,
        in_specs=[smem] + [anywhere] * 4 + [vmem] + [hbm] * 12,
        out_specs=[hbm] * 12,
        scratch_shapes=set_scratch
        + [
            pltpu.VMEM((model, total), jnp.bfloat16),
            pltpu.SemaphoreType.DMA((2,)),
            pltpu.SemaphoreType.DMA((2, 6)),
            pltpu.SemaphoreType.DMA((2, 6)),
        ]
        + held,
        compiler_params=params,
        name="tail",
    )(place, *operands)
    return tuple(v for both in zip(out[:6], out[6:], strict=True) for v in both)


def use_gathered(tokens, model, hidden, fs_size, tp_size):
    blocks = fs_size // 2
    square_grid = tp_size == 4 and fs_size % 2 == 0 and blocks & (blocks - 1) == 0
    return square_grid and tokens * (model + 2 * hidden) <= model * 2 * hidden


def on_device(fs_size, tp_size, inputs, query_grad, forget_grad, forget_pre, lower_bound, *rest):
    sigma_gate = jax.nn.sigmoid(forget_pre.astype(jnp.float32))
    forget_cot = (
        forget_grad.astype(jnp.float32) * (1.0 - lower_bound) * sigma_gate * (1.0 - sigma_gate)
    ).astype(jnp.bfloat16)
    tokens = inputs.shape[0] * fs_size
    if use_gathered(tokens, inputs.shape[1] * tp_size, query_grad.shape[1] * tp_size, fs_size, tp_size):
        return gathered_plan(inputs, query_grad, forget_cot, *rest, fs_size, tp_size)
    return summed_plan(inputs, query_grad, forget_cot, *rest)


def solution(mesh):
    in_specs = (
        P("fs", "tp"),
        P("fs", "tp"),
        P("fs", "tp"),
        P("fs", "tp"),
        P("tp"),
        P("fs", "tp"),
        P("fs", "tp"),
        P("fs", "tp"),
        P("fs", "tp"),
        P("fs", None),
        P("fs", None),
        P("tp", None, None),
        P("tp", None, None),
        P("fs", None),
        P("fs", None),
        P("tp", None, None),
        P("tp", None, None),
    )
    out_specs = (
        P("fs", "tp"),
        P("fs", "tp"),
        P("fs", "tp"),
        P("fs", "tp"),
        P("fs", "tp"),
        P("fs", "tp"),
        P("fs", "tp"),
        P("fs", "tp"),
        P("fs", None),
        P("fs", None),
        P("tp", None, None),
        P("tp", None, None),
    )
    sizes = (mesh.shape["fs"], mesh.shape["tp"])
    return jax.shard_map(
        partial(on_device, *sizes), mesh=mesh, in_specs=in_specs, out_specs=out_specs, check_vma=False
    )
```

profile of v0, /device:TPU:0, one launch (start us, length us, event | category | flops | bytes accessed | tf_op | source)
XLA Modules:
  0.0 92.3 jit_solution(32797989953451767)
XLA Ops:
  0.7 0.7 broadcast_subtract_fusion
  1.3 0.9 multiply_convert_fusion
  2.3 0.9 broadcast_select_fusion
  3.2 0.6 collective-permute-start
  3.8 1.0 %collective-permute-done = bf16[128,512]{1,0:T(8,128)(2,1)S(1)} collective-permute-done((bf16[128,512]{1,0:T(8,128)(2,1)S(1)}, bf16[128,512]{1,0:T(8,128)(2,1)S(1)}, u32[]{:S(2)}, u32[]{:S(2)}) %collective-permute-start) | collective-permute-done | bytes 131104 | tf_op jit(solution)/shard_map/ppermute | solution.py:167
  4.8 1.0 %select_bitcast_fusion.1 = (bf16[1,128,512]{2,1,0:T(8,128)(2,1)S(1)}, bf16[1,128,512]{2,1,0:T(8,128)(2,1)S(1)}) fusion(bf16[128,512]{1,0:T(8,128)(2,1)S(1)} %collective-permute-done, bf16[128,512]{1,0:T(8,128)(2,1)} %param.17, pred[]{:T(512)S(6)} %eq.6, bf16[128,256]{1,0:T(8,128)(2,1)S(1)} %multiply_convert_fusion, bf16[128,256]{1,0:T(8,128)(2,1)} %param.18), kind=kLoop, calls=%fused_computation.7 | loop fusion | flops 393216 | bytes 655361 | tf_op jit(solution)/shard_map/stack | solution.py:181
  5.8 3.9 %collective-permute-start.1 = (bf16[2,128,512]{2,1,0:T(8,128)(2,1)S(1)}, bf16[2,128,512]{2,1,0:T(8,128)(2,1)S(1)}, u32[]{:S(2)}, u32[]{:S(2)}) collective-permute-start(bf16[2,128,512]{2,1,0:T(8,128)(2,1)S(1)} %get-tuple-element.37), channel_id=1, source_target_pairs={{0,16},{1,17},{2,18},{3,19},{4,20},{5,21},{6,22},{7,23},{8,24},{9,... | collective-permute-start | bytes 786440 | tf_op jit(solution)/shard_map/ppermute | solution.py:167
  9.7 1.6 %collective-permute-start.11 = (bf16[2,128,512]{2,1,0:T(8,128)(2,1)S(1)}, bf16[2,128,512]{2,1,0:T(8,128)(2,1)S(1)}, u32[]{:S(2)}, u32[]{:S(2)}) collective-permute-start(bf16[2,128,512]{2,1,0:T(8,128)(2,1)S(1)} %get-tuple-element.37), channel_id=1, source_target_pairs={{0,8},{1,9},{2,10},{3,11},{4,12},{5,13},{6,14},{7,15},{8,0},{9,1},... | collective-permute-start | bytes 786440 | tf_op jit(solution)/shard_map/ppermute | solution.py:167
  11.3 1.5 %collective-permute-start.16 = (bf16[2,128,512]{2,1,0:T(8,128)(2,1)S(1)}, bf16[2,128,512]{2,1,0:T(8,128)(2,1)S(1)}, u32[]{:S(2)}, u32[]{:S(2)}) collective-permute-start(bf16[2,128,512]{2,1,0:T(8,128)(2,1)S(1)} %get-tuple-element.37), channel_id=1, source_target_pairs={{0,4},{1,3},{2,6},{3,1},{4,0},{5,7},{6,2},{7,5},{8,12},{9,11},{10,... | collective-permute-start | bytes 786440 | tf_op jit(solution)/shard_map/ppermute | solution.py:167
  12.8 9.2 %collective-permute-done.1 = bf16[2,128,512]{2,1,0:T(8,128)(2,1)S(1)} collective-permute-done((bf16[2,128,512]{2,1,0:T(8,128)(2,1)S(1)}, bf16[2,128,512]{2,1,0:T(8,128)(2,1)S(1)}, u32[]{:S(2)}, u32[]{:S(2)}) %collective-permute-start.1) | collective-permute-done | bytes 262176 | tf_op jit(solution)/shard_map/ppermute | solution.py:167
  22.0 0.6 collective-permute-start.2
  22.6 1.5 %collective-permute-start.12 = (bf16[2,128,512]{2,1,0:T(8,128)(2,1)S(1)}, bf16[2,128,512]{2,1,0:T(8,128)(2,1)S(1)}, u32[]{:S(2)}, u32[]{:S(2)}) collective-permute-start(bf16[2,128,512]{2,1,0:T(8,128)(2,1)S(1)} %collective-permute-done.11), channel_id=1, source_target_pairs={{0,4},{1,3},{2,6},{3,1},{4,0},{5,7},{6,2},{7,5},{8,12},{9,11},{10,... | collective-permute-start | bytes 786440 | tf_op jit(solution)/shard_map/ppermute | solution.py:167
  24.1 0.1 pad_maximum_fusion.3.refs_0_
  24.2 1.6 %collective-permute-start.17 = (bf16[2,2,128,512]{3,2,1,0:T(8,128)(2,1)S(1)}, bf16[2,2,128,512]{3,2,1,0:T(8,128)(2,1)S(1)}, u32[]{:S(2)}, u32[]{:S(2)}) collective-permute-start(bf16[2,2,128,512]{3,2,1,0:T(8,128)(2,1)S(1)} %pad_maximum_fusion.3.refs_0_), channel_id=1, source_target_pairs={{0,2},{1,5},{2,0},{3,7},{4,6},{5,1},{6,4},{7,3},{8,10},{9,13},{10,... | collective-permute-start | bytes 1572872 | tf_op jit(solution)/shard_map/ppermute | solution.py:167
  25.7 0.0 collective-permute-start.18
  25.7 0.5 collective-permute-start.7
  26.3 3.4 %collective-permute-done.2 = bf16[2,128,512]{2,1,0:T(8,128)(2,1)S(1)} collective-permute-done((bf16[2,128,512]{2,1,0:T(8,128)(2,1)S(1)}, bf16[2,128,512]{2,1,0:T(8,128)(2,1)S(1)}, u32[]{:S(2)}, u32[]{:S(2)}) %collective-permute-start.2) | collective-permute-done | bytes 262176 | tf_op jit(solution)/shard_map/ppermute | solution.py:167
  29.6 1.3 %collective-permute-start.3 = (bf16[2,128,512]{2,1,0:T(8,128)(2,1)S(1)}, bf16[2,128,512]{2,1,0:T(8,128)(2,1)S(1)}, u32[]{:S(2)}, u32[]{:S(2)}) collective-permute-start(bf16[2,128,512]{2,1,0:T(8,128)(2,1)S(1)} %collective-permute-done.2), channel_id=1, source_target_pairs={{0,4},{1,3},{2,6},{3,1},{4,0},{5,7},{6,2},{7,5},{8,12},{9,11},{10,... | collective-permute-start | bytes 786440 | tf_op jit(solution)/shard_map/ppermute | solution.py:167
  30.9 0.7 collective-permute-done.12
  31.7 0.1 pad_maximum_fusion.2.refs_0_
  31.7 1.7 %collective-permute-start.13 = (bf16[2,2,128,512]{3,2,1,0:T(8,128)(2,1)S(1)}, bf16[2,2,128,512]{3,2,1,0:T(8,128)(2,1)S(1)}, u32[]{:S(2)}, u32[]{:S(2)}) collective-permute-start(bf16[2,2,128,512]{3,2,1,0:T(8,128)(2,1)S(1)} %pad_maximum_fusion.2.refs_0_), channel_id=1, source_target_pairs={{0,2},{1,5},{2,0},{3,7},{4,6},{5,1},{6,4},{7,3},{8,10},{9,13},{10,... | collective-permute-start | bytes 1572872 | tf_op jit(solution)/shard_map/ppermute | solution.py:167
  33.4 3.8 %collective-permute-done.7 = bf16[2,128,512]{2,1,0:T(8,128)(2,1)S(1)} collective-permute-done((bf16[2,128,512]{2,1,0:T(8,128)(2,1)S(1)}, bf16[2,128,512]{2,1,0:T(8,128)(2,1)S(1)}, u32[]{:S(2)}, u32[]{:S(2)}) %collective-permute-start.7) | collective-permute-done | bytes 262176 | tf_op jit(solution)/shard_map/ppermute | solution.py:167
  37.3 0.1 pad_maximum_fusion.1.refs_0_
  37.3 5.6 %collective-permute-done.3 = bf16[2,128,512]{2,1,0:T(8,128)(2,1)S(1)} collective-permute-done((bf16[2,128,512]{2,1,0:T(8,128)(2,1)S(1)}, bf16[2,128,512]{2,1,0:T(8,128)(2,1)S(1)}, u32[]{:S(2)}, u32[]{:S(2)}) %collective-permute-start.3) | collective-permute-done | bytes 262176 | tf_op jit(solution)/shard_map/ppermute | solution.py:167
  42.9 1.7 %collective-permute-start.8 = (bf16[2,2,128,512]{3,2,1,0:T(8,128)(2,1)S(1)}, bf16[2,2,128,512]{3,2,1,0:T(8,128)(2,1)S(1)}, u32[]{:S(2)}, u32[]{:S(2)}) collective-permute-start(bf16[2,2,128,512]{3,2,1,0:T(8,128)(2,1)S(1)} %pad_maximum_fusion.1.refs_0_), channel_id=1, source_target_pairs={{0,2},{1,5},{2,0},{3,7},{4,6},{5,1},{6,4},{7,3},{8,10},{9,13},{10,... | collective-permute-start | bytes 1572872 | tf_op jit(solution)/shard_map/ppermute | solution.py:167
  44.5 0.1 pad_maximum_fusion.refs_0_
  44.6 0.0 collective-permute-done.17.refs_1_
  44.6 0.1 collective-permute-start.19
  44.7 0.0 copy-start.2
  44.7 0.8 copy-done.2
  45.5 0.8 copy-done.4
  46.3 0.4 collective-permute-start.4
  46.7 1.3 %collective-permute-start.9 = (bf16[2,2,128,512]{3,2,1,0:T(8,128)(2,1)S(1)}, bf16[2,2,128,512]{3,2,1,0:T(8,128)(2,1)}, u32[]{:S(2)}, u32[]{:S(2)}) collective-permute-start(bf16[2,2,128,512]{3,2,1,0:T(8,128)(2,1)S(1)} %pad_maximum_fusion.1.refs_0_), channel_id=1, source_target_pairs={{0,1},{1,0},{2,3},{3,2},{4,5},{5,4},{6,7},{7,6},{8,9},{9,8},{10,11... | collective-permute-start | bytes 1572872 | tf_op jit(solution)/shard_map/ppermute | solution.py:167
  48.0 0.0 collective-permute-done.14.refs_2_
  48.0 0.8 copy-done
  48.8 0.0 collective-permute-start.15
  48.8 3.3 %collective-permute-done.8.refs_1_ = bf16[2,2,128,512]{3,2,1,0:T(8,128)(2,1)S(1)} collective-permute-done((bf16[2,2,128,512]{3,2,1,0:T(8,128)(2,1)S(1)}, bf16[2,2,128,512]{3,2,1,0:T(8,128)(2,1)S(1)}, u32[]{:S(2)}, u32[]{:S(2)}) %collective-permute-start.8) | collective-permute-done | bytes 524320 | tf_op jit(solution)/shard_map/ppermute | solution.py:167
  52.1 0.8 copy-done.6
  52.9 0.5 collective-permute-start.5
  53.4 4.4 %collective-permute-done.4.refs_1_ = bf16[2,2,128,512]{3,2,1,0:T(8,128)(2,1)} collective-permute-done((bf16[2,2,128,512]{3,2,1,0:T(8,128)(2,1)S(1)}, bf16[2,2,128,512]{3,2,1,0:T(8,128)(2,1)}, u32[]{:S(2)}, u32[]{:S(2)}) %collective-permute-start.4) | collective-permute-done | bytes 524320 | tf_op jit(solution)/shard_map/ppermute | solution.py:167
  57.8 0.1 pad_add_fusion.place
  57.9 1.0 %copy-done.3 = bf16[2,2,128,512]{3,2,1,0:T(8,128)(2,1)S(1)} copy-done((bf16[2,2,128,512]{3,2,1,0:T(8,128)(2,1)S(1)}, bf16[2,2,128,512]{3,2,1,0:T(8,128)(2,1)}, u32[]{:S(2)}) %copy-start.3) | copy-done | bytes 524312
  58.9 1.0 %copy-done.5 = bf16[2,2,128,512]{3,2,1,0:T(8,128)(2,1)S(1)} copy-done((bf16[2,2,128,512]{3,2,1,0:T(8,128)(2,1)S(1)}, bf16[2,2,128,512]{3,2,1,0:T(8,128)(2,1)}, u32[]{:S(2)}) %copy-start.5) | copy-done | bytes 524312
  60.0 1.0 %copy-done.7 = bf16[2,2,128,512]{3,2,1,0:T(8,128)(2,1)S(1)} copy-done((bf16[2,2,128,512]{3,2,1,0:T(8,128)(2,1)S(1)}, bf16[2,2,128,512]{3,2,1,0:T(8,128)(2,1)}, u32[]{:S(2)}) %copy-start.7) | copy-done | bytes 524312
  61.0 4.8 %shard_map.256.refs_4_ = f32[2048,2048]{1,0:T(8,128)S(1)} custom-call(s32[3]{0:T(128)S(1)} %pad_add_fusion.place, bf16[2,2,128,512]{3,2,1,0:T(8,128)(2,1)S(1)} %pad_maximum_fusion.3.refs_0_, bf16[2,2,128,512]{3,2,1,0:T(8,128)(2,1)S(1)} %copy-done.3, bf16[2,2,128,512]{3,2,1,0:T(8,128)(2,1)S(1)} %copy-done.5, bf16[2,2,128,512]{3,2,1,0:T(8,128)(2,1)S(1)} %copy-done.7), custom_call_target="tpu_custom_call" | custom-call | tf_op jit(solution)/shard_map/pallas_call | solution.py:422
  65.8 5.7 %shard_map.257.refs_4_ = f32[2048,2048]{1,0:T(8,128)S(1)} custom-call(s32[3]{0:T(128)S(1)} %pad_add_fusion.place, bf16[2,2,128,512]{3,2,1,0:T(8,128)(2,1)S(1)} %pad_maximum_fusion.2.refs_0_, bf16[2,2,128,512]{3,2,1,0:T(8,128)(2,1)S(1)} %collective-permute-done.13.refs_1_, bf16[2,2,128,512]{3,2,1,0:T(8,128)(2,1)S(1)} %copy-done.1, ...), custom_call_target="tpu_custom_call", output_to_operand_aliasing={{}: (5, {})} | custom-call | tf_op jit(solution)/shard_map/pallas_call | solution.py:422
  71.6 5.8 %shard_map.258.refs_4_ = f32[2048,2048]{1,0:T(8,128)S(1)} custom-call(s32[3]{0:T(128)S(1)} %pad_add_fusion.place, bf16[2,2,128,512]{3,2,1,0:T(8,128)(2,1)S(1)} %pad_maximum_fusion.1.refs_0_, bf16[2,2,128,512]{3,2,1,0:T(8,128)(2,1)S(1)} %collective-permute-done.8.refs_1_, ...), custom_call_target="tpu_custom_call", output_to_operand_aliasing={{}: (5, {})} | custom-call | tf_op jit(solution)/shard_map/pallas_call | solution.py:422
  77.4 14.9 %tail.1 = (f32[256,256]{1,0:T(8,128)}, bf16[256,256]{1,0:T(8,128)(2,1)}, f32[256,256]{1,0:T(8,128)}, f32[256,256]{1,0:T(8,128)}, f32[256,2048]{1,0:T(8,128)}, /*...) custom-call(s32[3]{0:T(128)S(1)} %pad_add_fusion.place, ...), custom_call_target="tpu_custom_call" | custom-call | tf_op jit(solution)/shard_map/tail/pallas_call | solution.py:434
  (22 shorter events, 0.1 us)
Async XLA Ops:
  3.2 1.6 %collective-permute-start = (bf16[128,512]{1,0:T(8,128)(2,1)S(1)}, bf16[128,512]{1,0:T(8,128)(2,1)S(1)}, u32[]{:S(2)}, u32[]{:S(2)}) collective-permute-start(bf16[128,512]{1,0:T(8,128)(2,1)S(1)} %broadcast_select_fusion), channel_id=1, source_target_pairs={{0,1},{1,0},{2,3},{3,2},{4,5},{5,4},{6,7},{7,6},{8,9},{9,8},{10,11... | collective-permute-start | bytes 393224 | tf_op jit(solution)/shard_map/ppermute | solution.py:167
  5.8 16.2 %collective-permute-start.1 = (bf16[2,128,512]{2,1,0:T(8,128)(2,1)S(1)}, bf16[2,128,512]{2,1,0:T(8,128)(2,1)S(1)}, u32[]{:S(2)}, u32[]{:S(2)}) collective-permute-start(bf16[2,128,512]{2,1,0:T(8,128)(2,1)S(1)} %get-tuple-element.37), channel_id=1, source_target_pairs={{0,16},{1,17},{2,18},{3,19},{4,20},{5,21},{6,22},{7,23},{8,24},{9,... | collective-permute-start | bytes 786440 | tf_op jit(solution)/shard_map/ppermute | solution.py:167
  9.7 12.9 %collective-permute-start.11 = (bf16[2,128,512]{2,1,0:T(8,128)(2,1)S(1)}, bf16[2,128,512]{2,1,0:T(8,128)(2,1)S(1)}, u32[]{:S(2)}, u32[]{:S(2)}) collective-permute-start(bf16[2,128,512]{2,1,0:T(8,128)(2,1)S(1)} %get-tuple-element.37), channel_id=1, source_target_pairs={{0,8},{1,9},{2,10},{3,11},{4,12},{5,13},{6,14},{7,15},{8,0},{9,1},... | collective-permute-start | bytes 786440 | tf_op jit(solution)/shard_map/ppermute | solution.py:167
  11.3 12.8 %collective-permute-start.16 = (bf16[2,128,512]{2,1,0:T(8,128)(2,1)S(1)}, bf16[2,128,512]{2,1,0:T(8,128)(2,1)S(1)}, u32[]{:S(2)}, u32[]{:S(2)}) collective-permute-start(bf16[2,128,512]{2,1,0:T(8,128)(2,1)S(1)} %get-tuple-element.37), channel_id=1, source_target_pairs={{0,4},{1,3},{2,6},{3,1},{4,0},{5,7},{6,2},{7,5},{8,12},{9,11},{10,... | collective-permute-start | bytes 786440 | tf_op jit(solution)/shard_map/ppermute | solution.py:167
  22.0 7.7 %collective-permute-start.2 = (bf16[2,128,512]{2,1,0:T(8,128)(2,1)S(1)}, bf16[2,128,512]{2,1,0:T(8,128)(2,1)S(1)}, u32[]{:S(2)}, u32[]{:S(2)}) collective-permute-start(bf16[2,128,512]{2,1,0:T(8,128)(2,1)S(1)} %collective-permute-done.1), channel_id=1, source_target_pairs={{0,8},{1,9},{2,10},{3,11},{4,12},{5,13},{6,14},{7,15},{8,0},{9,1},... | collective-permute-start | bytes 786440 | tf_op jit(solution)/shard_map/ppermute | solution.py:167
  22.6 9.0 %collective-permute-start.12 = (bf16[2,128,512]{2,1,0:T(8,128)(2,1)S(1)}, bf16[2,128,512]{2,1,0:T(8,128)(2,1)S(1)}, u32[]{:S(2)}, u32[]{:S(2)}) collective-permute-start(bf16[2,128,512]{2,1,0:T(8,128)(2,1)S(1)} %collective-permute-done.11), channel_id=1, source_target_pairs={{0,4},{1,3},{2,6},{3,1},{4,0},{5,7},{6,2},{7,5},{8,12},{9,11},{10,... | collective-permute-start | bytes 786440 | tf_op jit(solution)/shard_map/ppermute | solution.py:167
  24.2 20.4 %collective-permute-start.17 = (bf16[2,2,128,512]{3,2,1,0:T(8,128)(2,1)S(1)}, bf16[2,2,128,512]{3,2,1,0:T(8,128)(2,1)S(1)}, u32[]{:S(2)}, u32[]{:S(2)}) collective-permute-start(bf16[2,2,128,512]{3,2,1,0:T(8,128)(2,1)S(1)} %pad_maximum_fusion.3.refs_0_), channel_id=1, source_target_pairs={{0,2},{1,5},{2,0},{3,7},{4,6},{5,1},{6,4},{7,3},{8,10},{9,13},{10,... | collective-permute-start | bytes 1572872 | tf_op jit(solution)/shard_map/ppermute | solution.py:167
  25.7 19.7 %collective-permute-start.18 = (bf16[2,2,128,512]{3,2,1,0:T(8,128)(2,1)S(1)}, bf16[2,2,128,512]{3,2,1,0:T(8,128)(2,1)S(1)}, u32[]{:S(2)}, u32[]{:S(2)}) collective-permute-start(bf16[2,2,128,512]{3,2,1,0:T(8,128)(2,1)S(1)} %pad_maximum_fusion.3.refs_0_), channel_id=1, source_target_pairs={{0,1},{1,0},{2,3},{3,2},{4,5},{5,4},{6,7},{7,6},{8,9},{9,8},{10,11... | collective-permute-start | bytes 1572872 | tf_op jit(solution)/shard_map/ppermute | solution.py:167
  25.7 11.5 %collective-permute-start.7 = (bf16[2,128,512]{2,1,0:T(8,128)(2,1)S(1)}, bf16[2,128,512]{2,1,0:T(8,128)(2,1)S(1)}, u32[]{:S(2)}, u32[]{:S(2)}) collective-permute-start(bf16[2,128,512]{2,1,0:T(8,128)(2,1)S(1)} %collective-permute-done.1), channel_id=1, source_target_pairs={{0,4},{1,3},{2,6},{3,1},{4,0},{5,7},{6,2},{7,5},{8,12},{9,11},{10,... | collective-permute-start | bytes 786440 | tf_op jit(solution)/shard_map/ppermute | solution.py:167
  29.6 13.2 %collective-permute-start.3 = (bf16[2,128,512]{2,1,0:T(8,128)(2,1)S(1)}, bf16[2,128,512]{2,1,0:T(8,128)(2,1)S(1)}, u32[]{:S(2)}, u32[]{:S(2)}) collective-permute-start(bf16[2,128,512]{2,1,0:T(8,128)(2,1)S(1)} %collective-permute-done.2), channel_id=1, source_target_pairs={{0,4},{1,3},{2,6},{3,1},{4,0},{5,7},{6,2},{7,5},{8,12},{9,11},{10,... | collective-permute-start | bytes 786440 | tf_op jit(solution)/shard_map/ppermute | solution.py:167
  31.7 14.9 %collective-permute-start.13 = (bf16[2,2,128,512]{3,2,1,0:T(8,128)(2,1)S(1)}, bf16[2,2,128,512]{3,2,1,0:T(8,128)(2,1)S(1)}, u32[]{:S(2)}, u32[]{:S(2)}) collective-permute-start(bf16[2,2,128,512]{3,2,1,0:T(8,128)(2,1)S(1)} %pad_maximum_fusion.2.refs_0_), channel_id=1, source_target_pairs={{0,2},{1,5},{2,0},{3,7},{4,6},{5,1},{6,4},{7,3},{8,10},{9,13},{10,... | collective-permute-start | bytes 1572872 | tf_op jit(solution)/shard_map/ppermute | solution.py:167
  37.3 10.7 %collective-permute-start.14 = (bf16[2,2,128,512]{3,2,1,0:T(8,128)(2,1)S(1)}, bf16[2,2,128,512]{3,2,1,0:T(8,128)(2,1)S(1)}, u32[]{:S(2)}, u32[]{:S(2)}) collective-permute-start(bf16[2,2,128,512]{3,2,1,0:T(8,128)(2,1)S(1)} %pad_maximum_fusion.2.refs_0_), channel_id=1, source_target_pairs={{0,1},{1,0},{2,3},{3,2},{4,5},{5,4},{6,7},{7,6},{8,9},{9,8},{10,11... | collective-permute-start | bytes 1572872 | tf_op jit(solution)/shard_map/ppermute | solution.py:167
  42.9 9.2 %collective-permute-start.8 = (bf16[2,2,128,512]{3,2,1,0:T(8,128)(2,1)S(1)}, bf16[2,2,128,512]{3,2,1,0:T(8,128)(2,1)S(1)}, u32[]{:S(2)}, u32[]{:S(2)}) collective-permute-start(bf16[2,2,128,512]{3,2,1,0:T(8,128)(2,1)S(1)} %pad_maximum_fusion.1.refs_0_), channel_id=1, source_target_pairs={{0,2},{1,5},{2,0},{3,7},{4,6},{5,1},{6,4},{7,3},{8,10},{9,13},{10,... | collective-permute-start | bytes 1572872 | tf_op jit(solution)/shard_map/ppermute | solution.py:167
  44.6 7.5 %collective-permute-start.19 = (bf16[2,2,128,512]{3,2,1,0:T(8,128)(2,1)S(1)}, bf16[2,2,128,512]{3,2,1,0:T(8,128)(2,1)S(1)}, u32[]{:S(2)}, u32[]{:S(2)}) collective-permute-start(bf16[2,2,128,512]{3,2,1,0:T(8,128)(2,1)S(1)} %collective-permute-done.17.refs_1_), channel_id=1, source_target_pairs={{0,1},{1,0},{2,3},{3,2},{4,5},{5,4},{6,7},{7,6},{8,9},{9,8},{10,11... | collective-permute-start | bytes 1572872 | tf_op jit(solution)/shard_map/ppermute | solution.py:167
  44.7 0.8 copy-start.2
  45.5 0.8 copy-start.4
  46.3 11.5 %collective-permute-start.4 = (bf16[2,2,128,512]{3,2,1,0:T(8,128)(2,1)S(1)}, bf16[2,2,128,512]{3,2,1,0:T(8,128)(2,1)}, u32[]{:S(2)}, u32[]{:S(2)}) collective-permute-start(bf16[2,2,128,512]{3,2,1,0:T(8,128)(2,1)S(1)} %pad_maximum_fusion.refs_0_), channel_id=1, source_target_pairs={{0,2},{1,5},{2,0},{3,7},{4,6},{5,1},{6,4},{7,3},{8,10},{9,13},{10,... | collective-permute-start | bytes 1572872 | tf_op jit(solution)/shard_map/ppermute | solution.py:167
  46.7 24.9 %collective-permute-start.9 = (bf16[2,2,128,512]{3,2,1,0:T(8,128)(2,1)S(1)}, bf16[2,2,128,512]{3,2,1,0:T(8,128)(2,1)}, u32[]{:S(2)}, u32[]{:S(2)}) collective-permute-start(bf16[2,2,128,512]{3,2,1,0:T(8,128)(2,1)S(1)} %pad_maximum_fusion.1.refs_0_), channel_id=1, source_target_pairs={{0,1},{1,0},{2,3},{3,2},{4,5},{5,4},{6,7},{7,6},{8,9},{9,8},{10,11... | collective-permute-start | bytes 1572872 | tf_op jit(solution)/shard_map/ppermute | solution.py:167
  48.0 0.8 copy-start
  48.8 17.0 %collective-permute-start.15 = (bf16[2,2,128,512]{3,2,1,0:T(8,128)(2,1)S(1)}, bf16[2,2,128,512]{3,2,1,0:T(8,128)(2,1)}, u32[]{:S(2)}, u32[]{:S(2)}) collective-permute-start(bf16[2,2,128,512]{3,2,1,0:T(8,128)(2,1)S(1)} %collective-permute-done.13.refs_1_), channel_id=1, source_target_pairs={{0,1},{1,0},{2,3},{3,2},{4,5},{5,4},{6,7},{7,6},{8,9},{9,8},{10,11... | collective-permute-start | bytes 1572872 | tf_op jit(solution)/shard_map/ppermute | solution.py:167
  52.1 19.5 %collective-permute-start.10 = (bf16[2,2,128,512]{3,2,1,0:T(8,128)(2,1)S(1)}, bf16[2,2,128,512]{3,2,1,0:T(8,128)(2,1)}, u32[]{:S(2)}, u32[]{:S(2)}) collective-permute-start(bf16[2,2,128,512]{3,2,1,0:T(8,128)(2,1)S(1)} %collective-permute-done.8.refs_1_), channel_id=1, source_target_pairs={{0,1},{1,0},{2,3},{3,2},{4,5},{5,4},{6,7},{7,6},{8,9},{9,8},{10,11... | collective-permute-start | bytes 1572872 | tf_op jit(solution)/shard_map/ppermute | solution.py:167
  52.1 0.8 copy-start.6
  52.9 24.5 %collective-permute-start.5 = (bf16[2,2,128,512]{3,2,1,0:T(8,128)(2,1)S(1)}, bf16[2,2,128,512]{3,2,1,0:T(8,128)(2,1)}, u32[]{:S(2)}, u32[]{:S(2)}) collective-permute-start(bf16[2,2,128,512]{3,2,1,0:T(8,128)(2,1)S(1)} %pad_maximum_fusion.refs_0_), channel_id=1, source_target_pairs={{0,1},{1,0},{2,3},{3,2},{4,5},{5,4},{6,7},{7,6},{8,9},{9,8},{10,11... | collective-permute-start | bytes 1572872 | tf_op jit(solution)/shard_map/ppermute | solution.py:167
  57.8 19.6 %collective-permute-start.6 = (bf16[2,2,128,512]{3,2,1,0:T(8,128)(2,1)}, bf16[2,2,128,512]{3,2,1,0:T(8,128)(2,1)}, u32[]{:S(2)}, u32[]{:S(2)}) collective-permute-start(bf16[2,2,128,512]{3,2,1,0:T(8,128)(2,1)} %collective-permute-done.4.refs_1_), channel_id=1, source_target_pairs={{0,1},{1,0},{2,3},{3,2},{4,5},{5,4},{6,7},{7,6},{8,9},{9,8},{10,11... | collective-permute-start | bytes 1572872 | tf_op jit(solution)/shard_map/ppermute | solution.py:167
  57.9 1.0 %copy-start.3 = (bf16[2,2,128,512]{3,2,1,0:T(8,128)(2,1)S(1)}, bf16[2,2,128,512]{3,2,1,0:T(8,128)(2,1)}, u32[]{:S(2)}) copy-start(bf16[2,2,128,512]{3,2,1,0:T(8,128)(2,1)} %copy-done.2) | copy-start | bytes 1572868
  58.9 1.0 %copy-start.5 = (bf16[2,2,128,512]{3,2,1,0:T(8,128)(2,1)S(1)}, bf16[2,2,128,512]{3,2,1,0:T(8,128)(2,1)}, u32[]{:S(2)}) copy-start(bf16[2,2,128,512]{3,2,1,0:T(8,128)(2,1)} %copy-done.4) | copy-start | bytes 1572868
  60.0 1.0 %copy-start.7 = (bf16[2,2,128,512]{3,2,1,0:T(8,128)(2,1)S(1)}, bf16[2,2,128,512]{3,2,1,0:T(8,128)(2,1)}, u32[]{:S(2)}) copy-start(bf16[2,2,128,512]{3,2,1,0:T(8,128)(2,1)} %copy-done.6) | copy-start | bytes 1572868
  61.0 4.8 %copy-start.1 = (bf16[2,2,128,512]{3,2,1,0:T(8,128)(2,1)S(1)}, bf16[2,2,128,512]{3,2,1,0:T(8,128)(2,1)}, u32[]{:S(2)}) copy-start(bf16[2,2,128,512]{3,2,1,0:T(8,128)(2,1)} %copy-done) | copy-start | bytes 1572868
where the time goes:
time: 93 us; the launch traced here: 92.3 us
  waiting for transfers between devices  31.4 us (34%)
  Pallas kernels  31.2 us (34%)
  starting transfers between devices  18.8 us (20%)
  local copies, waits for them, and re-layouts  6.3 us (7%)
  other arithmetic  3.77 us (4%)
    ppermute x20, waiting for transfers between devices, move(): return lax.ppermute(value, axes, linear_pairs(fs_size, tp_size, target))  31.4 us
    ppermute x20, starting transfers between devices, move(): return lax.ppermute(value, axes, linear_pairs(fs_size, tp_size, target))  18.8 us
    pallas_call x3, Pallas kernels, gathered_plan(): pl.pallas_call(partial(sum_kernel, not acc), out_shape=pltpu.VMEM((model,...  16.3 us
    pallas_call x1, Pallas kernels, gathered_plan(): pl.pallas_call(tail_kernel, out_shape=kinds * 2, in_specs=[smem] + [anywh...  14.9 us
    unnamed x16, local copies, waits for them, and re-layouts  6.3 us
  transfers between devices with their start and end apart: 20, of which 8 were waited for; matrix products, arithmetic and copies ran while one was open for 0% of the time, Pallas kernels for 18%

commit v1 on v0

--- a/solution.py
+++ b/solution.py
@@ -160,14 +160,12 @@
     return pairs
 
 
-def gather_operands(x_block, y_block, fs_size, tp_size):
+def gather_operands(keep, send, fs_size, tp_size):
     axes = ("fs", "tp")
 
     def move(value, target):
         return lax.ppermute(value, axes, linear_pairs(fs_size, tp_size, target))
 
-    odd = lax.axis_index("tp") % 2 == 1
-
     def partner(f, t):
         return (f, t ^ 1)
 
@@ -177,8 +175,7 @@
     def second_hop(f, t):
         return (f, t ^ 2) if t % 2 == 0 else (f ^ 1, t)
 
-    swapped = move(jnp.where(odd, x_block, y_block), partner)
-    lanes = [jnp.stack([jnp.where(odd, swapped, x_block), jnp.where(odd, y_block, swapped)])]
+    lanes = [jnp.stack([keep, move(send, partner)])]
     for k in range(1, fs_size // 2):
         step = k & -k if k & (k - 1) == 0 else k & (k - 1) ^ k
         source = lanes[k ^ step]
@@ -208,7 +205,7 @@
                     ).start()
                     for i in range(2):
                         pltpu.make_async_copy(
-                            y_pieces[p].at[h, c, :, pl.ds(i * own, own)],
+                            y_pieces[p].at[h, 1 - c, :, pl.ds(i * own, own)],
                             y_set.at[rows, pl.ds(i * hidden + (2 * h + c) * own, own)],
                             sem.at[1],
                         ).start()
@@ -229,13 +226,9 @@
         pltpu.make_async_copy(whole, whole, sem.at[k]).wait()
 
 
-def chunk_product(x_set, y_set, m, n, rows, chunk):
-    at = pl.multiple_of(m * rows, rows)
+def product(x_set, y_set, cols):
     return lax.dot_general(
-        x_set[:, pl.ds(at, rows)],
-        y_set[:, n * chunk : (n + 1) * chunk],
-        (((0,), (0,)), ((), ())),
-        preferred_element_type=jnp.float32,
+        x_set[...], y_set[:, cols], (((0,), (0,)), ((), ())), preferred_element_type=jnp.float32
     )
 
 
@@ -246,19 +239,11 @@
     acc, x_set, y_set, sem = refs
     assemble(place, pieces, x_set, y_set, sem)
     assembled(x_set, y_set, sem)
-    model, total = acc.shape
-    rows = pieces[0].shape[3] // 2
-    chunk = total // 4
-
-    def product(m, carry):
-        at = pl.multiple_of(m * rows, rows)
-        for n in range(total // chunk):
-            cols = slice(n * chunk, (n + 1) * chunk)
-            part = chunk_product(x_set, y_set, m, n, rows, chunk)
-            acc[pl.ds(at, rows), cols] = part if first else acc[pl.ds(at, rows), cols] + part
-        return carry
-
-    lax.fori_loop(0, model // rows, product, 0)
+    total, chunk = acc.shape[1], x_set.shape[0]
+    for at in range(0, total, chunk):
+        cols = slice(at, at + chunk)
+        part = product(x_set, y_set, cols)
+        acc[:, cols] = part if first else acc[:, cols] + part
 
 
 def tail_kernel(place, *refs):
@@ -288,23 +273,13 @@
             copy.start()
     assembled(x_set, y_set, sem)
 
-    chunk = hidden // 2
-
-    def product(m, squares):
-        at = pl.multiple_of(m * rows_here, rows_here)
-        squares = list(squares)
-        for n in range(total // chunk):
-            cols = slice(n * chunk, (n + 1) * chunk)
-            part = acc[pl.ds(at, rows_here), cols] + chunk_product(
-                x_set, y_set, m, n, rows_here, chunk
-            )
-            grad[pl.ds(at, rows_here), cols] = part.astype(jnp.bfloat16)
-            i = n * chunk // hidden
-            squares[i] = squares[i] + jnp.sum((part * part).reshape(-1, 8, chunk), axis=0)
-        return tuple(squares)
-
-    zero = jnp.zeros((8, chunk), jnp.float32)
-    squares = lax.fori_loop(0, model // rows_here, product, (zero, zero))
+    chunk = x_set.shape[0]
+    squares = [jnp.zeros((8, chunk), jnp.float32)] * 2
+    for at in range(0, total, chunk):
+        cols = slice(at, at + chunk)
+        part = acc[:, cols] + product(x_set, y_set, cols)
+        grad[:, cols] = part.astype(jnp.bfloat16)
+        squares[at // hidden] += jnp.sum((part * part).reshape(-1, 8, chunk), axis=0)
 
     stores = []
     first = pl.multiple_of(band * rows_here, rows_here)
@@ -320,20 +295,15 @@
         band_grad = grad[pl.ds(first, rows_here), i * hidden : (i + 1) * hidden]
         row_factor = (1.0 - stat_decay) / hidden * twice
 
-        def outer(n, carry):
-            at = pl.multiple_of(n * rows_here, rows_here)
+        for at in range(0, model, own * 2):
             part = lax.dot_general(
                 band_grad,
-                grad[pl.ds(at, rows_here), i * hidden : (i + 1) * hidden],
+                grad[at : at + own * 2, i * hidden : (i + 1) * hidden],
                 (((1,), (1,)), ((), ())),
                 preferred_element_type=jnp.float32,
             )
-            rows[:, pl.ds(at, rows_here)] = (
-                stat_decay * rows[:, pl.ds(at, rows_here)] + row_factor * part
-            )
-            return carry
-
-        lax.fori_loop(0, model // rows_here, outer, 0)
+            to = slice(at, at + own * 2)
+            rows[:, to] = stat_decay * rows[:, to] + row_factor * part
         stores.append(pltpu.make_async_copy(rows, outs[i][4], store_sem.at[i, 4]))
         stores[-1].start()
         own_grad = grad[:, pl.ds(mine, own)]
@@ -368,10 +338,46 @@
         copy.wait()
 
 
+def prepare_kernel(place, *refs):
+    sources, (keep, send), held, sem = refs[:5], refs[5:7], refs[7:12], refs[12]
+    copies = [
+        pltpu.make_async_copy(src, dst, sem.at[j])
+        for j, (src, dst) in enumerate(zip(sources, held, strict=True))
+    ]
+    for copy in copies:
+        copy.start()
+    for copy in copies:
+        copy.wait()
+    inputs, query_grad, forget_grad, forget_pre, lower_bound = held
+    own = query_grad.shape[1]
+    sigma_gate = jax.nn.sigmoid(forget_pre[...].astype(jnp.float32))
+    forget_cot = (
+        forget_grad[...].astype(jnp.float32)
+        * (1.0 - lower_bound[...])
+        * sigma_gate
+        * (1.0 - sigma_gate)
+    ).astype(jnp.bfloat16)
+
+    def write(x_to, y_to):
+        x_to[...] = inputs[...]
+        y_to[:, :own] = query_grad[...]
+        y_to[:, own:] = forget_cot
+
+    @pl.when(place[0] == 0)
+    def _():
+        write(keep, send)
+
+    @pl.when(place[0] == 1)
+    def _():
+        write(send, keep)
+
+
 def gathered_plan(
     inputs,
     query_grad,
-    forget_cot,
+    forget_grad,
+    forget_pre,
+    lower_bound,
     query_weight,
     forget_weight,
     query_moment,
@@ -387,11 +393,24 @@
     fs_size,
     tp_size,
 ):
-    sets = gather_operands(
-        inputs, jnp.concatenate([query_grad, forget_cot], axis=1), fs_size, tp_size
-    )
     tp_at = lax.axis_index("tp")
-    place = jnp.stack([tp_at % 2, tp_at // 2, lax.axis_index("fs")]).astype(jnp.int32)
+    place = jnp.stack([tp_at & 1, tp_at >> 1, lax.axis_index("fs")]).astype(jnp.int32)
+    smem = pl.BlockSpec(memory_space=pltpu.SMEM)
+    vmem = pl.BlockSpec(memory_space=pltpu.VMEM)
+    params = pltpu.CompilerParams(vmem_limit_bytes=26 * 2**20)
+    hbm = pl.BlockSpec(memory_space=pltpu.HBM)
+    saved = (inputs, query_grad, forget_grad, forget_pre, lower_bound[None])
+    keep, send = pl.pallas_call(
+        prepare_kernel,
+        out_shape=(pltpu.VMEM(inputs.shape, inputs.dtype),) * 2,
+        in_specs=[smem] + [hbm] * 5,
+        out_specs=[vmem] * 2,
+        scratch_shapes=[pltpu.VMEM(v.shape, v.dtype) for v in saved]
+        + [pltpu.SemaphoreType.DMA((5,))],
+        compiler_params=params,
+        name="prepare",
+    )(place, *(pltpu.with_memory_space_constraint(v, pltpu.HBM) for v in saved))
+    sets = gather_operands(keep, send, fs_size, tp_size)
     model = inputs.shape[1] * tp_size
     total = 2 * query_grad.shape[1] * tp_size
     sides = (
@@ -408,14 +427,10 @@
         held += [pltpu.VMEM(v.shape, v.dtype) for v in side]
         held += [pltpu.VMEM(k.shape, k.dtype) for k in kinds[:4]]
     anywhere = pl.BlockSpec(memory_space=pl.ANY)
-    hbm = pl.BlockSpec(memory_space=pltpu.HBM)
-    vmem = pl.BlockSpec(memory_space=pltpu.VMEM)
-    smem = pl.BlockSpec(memory_space=pltpu.SMEM)
     set_scratch = [
         pltpu.VMEM((2 * inputs.shape[0], model), jnp.bfloat16),
         pltpu.VMEM((2 * inputs.shape[0], total), jnp.bfloat16),
     ]
-    params = pltpu.CompilerParams(vmem_limit_bytes=26 * 2**20)
     acc = []
     for pieces in sets[:-1]:
         acc = [
@@ -457,13 +472,15 @@
 
 
 def on_device(fs_size, tp_size, inputs, query_grad, forget_grad, forget_pre, lower_bound, *rest):
+    tokens = inputs.shape[0] * fs_size
+    if use_gathered(tokens, inputs.shape[1] * tp_size, query_grad.shape[1] * tp_size, fs_size, tp_size):
+        return gathered_plan(
+            inputs, query_grad, forget_grad, forget_pre, lower_bound, *rest, fs_size, tp_size
+        )
     sigma_gate = jax.nn.sigmoid(forget_pre.astype(jnp.float32))
     forget_cot = (
         forget_grad.astype(jnp.float32) * (1.0 - lower_bound) * sigma_gate * (1.0 - sigma_gate)
     ).astype(jnp.bfloat16)
-    tokens = inputs.shape[0] * fs_size
-    if use_gathered(tokens, inputs.shape[1] * tp_size, query_grad.shape[1] * tp_size, fs_size, tp_size):
-        return gathered_plan(inputs, query_grad, forget_cot, *rest, fs_size, tp_size)
     return summed_plan(inputs, query_grad, forget_cot, *rest)
 
 

time: 93 us -> 75.8 us (0.82)
  Pallas kernels: 31.2 us -> 20.9 us
  local copies, waits for them, and re-layouts: 6.3 us -> 0 us
  other arithmetic: 3.77 us -> 0.31 us
  waiting for transfers between devices: 31.4 us -> 34.5 us
    unnamed x16 -> x0, local copies, waits for them, and re-layouts: 6.3 us -> none
    pallas_call x3, Pallas kernels: 16.3 us -> 10 us  [gathered_plan(): pl.pallas_call(partial(sum_kernel, not acc), out_shape=pltpu.VMEM((model,...]
    pallas_call x1, Pallas kernels: 14.9 us -> 9.24 us  [gathered_plan(): pl.pallas_call(tail_kernel, out_shape=kinds * 2, in_specs=[smem] + [anywh...]
    ppermute x20, waiting for transfers between devices: 31.4 us -> 34.5 us  [move(): return lax.ppermute(value, axes, linear_pairs(fs_size, tp_size, target))]
    pallas_call x0 -> x1, Pallas kernels: none -> 1.61 us  [gathered_plan(): pl.pallas_call(prepare_kernel, out_shape=(pltpu.VMEM(inputs.shape, inputs...]
    another operation x2 -> x1, other arithmetic: 1.04 us -> 0.08 us  [gathered_plan(): jnp.stack([tp_at & 1, tp_at >> 1, lax.axis_index('fs')]).astype(jnp.int32)]
  transfers between devices with their start and end apart: 20 -> 20, of which waited for: 8 -> 8; matrix products, arithmetic and copies ran while one was open for 0% -> 0% of each run, Pallas kernels for 18% -> 13%
where the time goes in v1:
time: 75.8 us; the launch traced here: 75.5 us
  waiting for transfers between devices  34.5 us (46%)
  Pallas kernels  20.9 us (28%)
  starting transfers between devices  18.9 us (25%)
  between operations  0.94 us (1%)
    ppermute x20, waiting for transfers between devices, move(): return lax.ppermute(value, axes, linear_pairs(fs_size, tp_size, target))  34.5 us
    ppermute x20, starting transfers between devices, move(): return lax.ppermute(value, axes, linear_pairs(fs_size, tp_size, target))  18.9 us
    pallas_call x3, Pallas kernels, gathered_plan(): pl.pallas_call(partial(sum_kernel, not acc), out_shape=pltpu.VMEM((model,...  10 us
    pallas_call x1, Pallas kernels, gathered_plan(): pl.pallas_call(tail_kernel, out_shape=kinds * 2, in_specs=[smem] + [anywh...  9.24 us
    pallas_call x1, Pallas kernels, gathered_plan(): pl.pallas_call(prepare_kernel, out_shape=(pltpu.VMEM(inputs.shape, inputs...  1.61 us
  transfers between devices with their start and end apart: 20, of which 8 were waited for; matrix products, arithmetic and copies ran while one was open for 0% of the time, Pallas kernels for 13%

profile of v1, /device:TPU:0, one launch (start us, length us, event | category | flops | bytes accessed | tf_op | source)
XLA Modules:
  0.0 75.5 jit_solution(3429537514257917928)
XLA Ops:
  0.6 0.1 pad_add_fusion.place
  0.7 1.6 %prepare.1 = (bf16[128,512]{1,0:T(8,128)(2,1)S(1)}, bf16[128,512]{1,0:T(8,128)(2,1)S(1)}) custom-call(s32[3]{0:T(128)S(1)} %pad_add_fusion.place, bf16[128,512]{1,0:T(8,128)(2,1)} %refs_0_.1, bf16[128,256]{1,0:T(8,128)(2,1)} %refs_1_.1, bf16[128,256]{1,0:T(8,128)(2,1)} %refs_2_.1, bf16[128,256]{1,0:T(8,128)(2,1)} %refs_3_.1, f32[1,256]{1,0:T(1,128)} %bitcast.24), custom_call_target="tpu_custom_call" | custom-call | tf_op jit(solution)/shard_map/prepare/pallas_call | solution.py:403
  2.3 0.6 collective-permute-start
  2.9 1.0 %collective-permute-done = bf16[128,512]{1,0:T(8,128)(2,1)S(1)} collective-permute-done((bf16[128,512]{1,0:T(8,128)(2,1)S(1)}, bf16[128,512]{1,0:T(8,128)(2,1)S(1)}, u32[]{:S(2)}, u32[]{:S(2)}) %collective-permute-start) | collective-permute-done | bytes 131104 | tf_op jit(solution)/shard_map/ppermute | solution.py:167
  3.9 4.0 %collective-permute-start.1 = (bf16[2,128,512]{2,1,0:T(8,128)(2,1)S(1)}, bf16[2,128,512]{2,1,0:T(8,128)(2,1)S(1)}, u32[]{:S(2)}, u32[]{:S(2)}) collective-permute-start(bf16[2,128,512]{2,1,0:T(8,128)(2,1)S(1)} %get-tuple-element.41), channel_id=1, source_target_pairs={{0,16},{1,17},{2,18},{3,19},{4,20},{5,21},{6,22},{7,23},{8,24},{9,... | collective-permute-start | bytes 786440 | tf_op jit(solution)/shard_map/ppermute | solution.py:167
  7.9 1.6 %collective-permute-start.11 = (bf16[2,128,512]{2,1,0:T(8,128)(2,1)S(1)}, bf16[2,128,512]{2,1,0:T(8,128)(2,1)S(1)}, u32[]{:S(2)}, u32[]{:S(2)}) collective-permute-start(bf16[2,128,512]{2,1,0:T(8,128)(2,1)S(1)} %get-tuple-element.41), channel_id=1, source_target_pairs={{0,8},{1,9},{2,10},{3,11},{4,12},{5,13},{6,14},{7,15},{8,0},{9,1},... | collective-permute-start | bytes 786440 | tf_op jit(solution)/shard_map/ppermute | solution.py:167
  9.5 1.5 %collective-permute-start.16 = (bf16[2,128,512]{2,1,0:T(8,128)(2,1)S(1)}, bf16[2,128,512]{2,1,0:T(8,128)(2,1)S(1)}, u32[]{:S(2)}, u32[]{:S(2)}) collective-permute-start(bf16[2,128,512]{2,1,0:T(8,128)(2,1)S(1)} %get-tuple-element.41), channel_id=1, source_target_pairs={{0,4},{1,3},{2,6},{3,1},{4,0},{5,7},{6,2},{7,5},{8,12},{9,11},{10,... | collective-permute-start | bytes 786440 | tf_op jit(solution)/shard_map/ppermute | solution.py:167
  11.0 9.3 %collective-permute-done.1 = bf16[2,128,512]{2,1,0:T(8,128)(2,1)S(1)} collective-permute-done((bf16[2,128,512]{2,1,0:T(8,128)(2,1)S(1)}, bf16[2,128,512]{2,1,0:T(8,128)(2,1)S(1)}, u32[]{:S(2)}, u32[]{:S(2)}) %collective-permute-start.1) | collective-permute-done | bytes 262176 | tf_op jit(solution)/shard_map/ppermute | solution.py:167
  20.3 0.6 collective-permute-start.2
  20.9 0.0 collective-permute-done.11
  20.9 1.5 %collective-permute-start.12 = (bf16[2,128,512]{2,1,0:T(8,128)(2,1)S(1)}, bf16[2,128,512]{2,1,0:T(8,128)(2,1)S(1)}, u32[]{:S(2)}, u32[]{:S(2)}) collective-permute-start(bf16[2,128,512]{2,1,0:T(8,128)(2,1)S(1)} %collective-permute-done.11), channel_id=1, source_target_pairs={{0,4},{1,3},{2,6},{3,1},{4,0},{5,7},{6,2},{7,5},{8,12},{9,11},{10,... | collective-permute-start | bytes 786440 | tf_op jit(solution)/shard_map/ppermute | solution.py:167
  22.4 0.0 collective-permute-done.16
  22.4 0.1 pad_maximum_fusion.3.refs_0_
  22.5 1.6 %collective-permute-start.17 = (bf16[2,2,128,512]{3,2,1,0:T(8,128)(2,1)S(1)}, bf16[2,2,128,512]{3,2,1,0:T(8,128)(2,1)S(1)}, u32[]{:S(2)}, u32[]{:S(2)}) collective-permute-start(bf16[2,2,128,512]{3,2,1,0:T(8,128)(2,1)S(1)} %pad_maximum_fusion.3.refs_0_), channel_id=1, source_target_pairs={{0,2},{1,5},{2,0},{3,7},{4,6},{5,1},{6,4},{7,3},{8,10},{9,13},{10,... | collective-permute-start | bytes 1572872 | tf_op jit(solution)/shard_map/ppermute | solution.py:167
  24.0 0.0 collective-permute-start.18
  24.0 0.5 collective-permute-start.7
  24.6 3.4 %collective-permute-done.2 = bf16[2,128,512]{2,1,0:T(8,128)(2,1)S(1)} collective-permute-done((bf16[2,128,512]{2,1,0:T(8,128)(2,1)S(1)}, bf16[2,128,512]{2,1,0:T(8,128)(2,1)S(1)}, u32[]{:S(2)}, u32[]{:S(2)}) %collective-permute-start.2) | collective-permute-done | bytes 262176 | tf_op jit(solution)/shard_map/ppermute | solution.py:167
  28.0 1.3 %collective-permute-start.3 = (bf16[2,128,512]{2,1,0:T(8,128)(2,1)S(1)}, bf16[2,128,512]{2,1,0:T(8,128)(2,1)S(1)}, u32[]{:S(2)}, u32[]{:S(2)}) collective-permute-start(bf16[2,128,512]{2,1,0:T(8,128)(2,1)S(1)} %collective-permute-done.2), channel_id=1, source_target_pairs={{0,4},{1,3},{2,6},{3,1},{4,0},{5,7},{6,2},{7,5},{8,12},{9,11},{10,... | collective-permute-start | bytes 786440 | tf_op jit(solution)/shard_map/ppermute | solution.py:167
  29.3 0.7 collective-permute-done.12
  29.9 0.1 pad_maximum_fusion.2.refs_0_
  30.0 1.7 %collective-permute-start.13 = (bf16[2,2,128,512]{3,2,1,0:T(8,128)(2,1)S(1)}, bf16[2,2,128,512]{3,2,1,0:T(8,128)(2,1)S(1)}, u32[]{:S(2)}, u32[]{:S(2)}) collective-permute-start(bf16[2,2,128,512]{3,2,1,0:T(8,128)(2,1)S(1)} %pad_maximum_fusion.2.refs_0_), channel_id=1, source_target_pairs={{0,2},{1,5},{2,0},{3,7},{4,6},{5,1},{6,4},{7,3},{8,10},{9,13},{10,... | collective-permute-start | bytes 1572872 | tf_op jit(solution)/shard_map/ppermute | solution.py:167
  31.7 3.8 %collective-permute-done.7 = bf16[2,128,512]{2,1,0:T(8,128)(2,1)S(1)} collective-permute-done((bf16[2,128,512]{2,1,0:T(8,128)(2,1)S(1)}, bf16[2,128,512]{2,1,0:T(8,128)(2,1)S(1)}, u32[]{:S(2)}, u32[]{:S(2)}) %collective-permute-start.7) | collective-permute-done | bytes 262176 | tf_op jit(solution)/shard_map/ppermute | solution.py:167
  35.6 0.0 collective-permute-start.14
  35.6 0.1 pad_maximum_fusion.1.refs_0_
  35.6 5.6 %collective-permute-done.3 = bf16[2,128,512]{2,1,0:T(8,128)(2,1)S(1)} collective-permute-done((bf16[2,128,512]{2,1,0:T(8,128)(2,1)S(1)}, bf16[2,128,512]{2,1,0:T(8,128)(2,1)S(1)}, u32[]{:S(2)}, u32[]{:S(2)}) %collective-permute-start.3) | collective-permute-done | bytes 262176 | tf_op jit(solution)/shard_map/ppermute | solution.py:167
  41.2 1.7 %collective-permute-start.8 = (bf16[2,2,128,512]{3,2,1,0:T(8,128)(2,1)S(1)}, bf16[2,2,128,512]{3,2,1,0:T(8,128)(2,1)S(1)}, u32[]{:S(2)}, u32[]{:S(2)}) collective-permute-start(bf16[2,2,128,512]{3,2,1,0:T(8,128)(2,1)S(1)} %pad_maximum_fusion.1.refs_0_), channel_id=1, source_target_pairs={{0,2},{1,5},{2,0},{3,7},{4,6},{5,1},{6,4},{7,3},{8,10},{9,13},{10,... | collective-permute-start | bytes 1572872 | tf_op jit(solution)/shard_map/ppermute | solution.py:167
  42.8 0.1 pad_maximum_fusion.refs_0_
  42.9 0.0 collective-permute-done.17.refs_1_
  42.9 0.1 collective-permute-start.19
  43.0 0.0 collective-permute-done.18.refs_2_
  43.0 0.4 collective-permute-start.4
  43.4 0.0 collective-permute-done.13.refs_1_
  43.4 1.3 %collective-permute-start.9 = (bf16[2,2,128,512]{3,2,1,0:T(8,128)(2,1)S(1)}, bf16[2,2,128,512]{3,2,1,0:T(8,128)(2,1)S(1)}, u32[]{:S(2)}, u32[]{:S(2)}) collective-permute-start(bf16[2,2,128,512]{3,2,1,0:T(8,128)(2,1)S(1)} %pad_maximum_fusion.1.refs_0_), channel_id=1, source_target_pairs={{0,1},{1,0},{2,3},{3,2},{4,5},{5,4},{6,7},{7,6},{8,9},{9,8},{10,11... | collective-permute-start | bytes 1572872 | tf_op jit(solution)/shard_map/ppermute | solution.py:167
  44.7 0.0 collective-permute-done.14.refs_2_
  44.7 0.1 collective-permute-start.15
  44.8 5.6 %collective-permute-done.8.refs_1_ = bf16[2,2,128,512]{3,2,1,0:T(8,128)(2,1)S(1)} collective-permute-done((bf16[2,2,128,512]{3,2,1,0:T(8,128)(2,1)S(1)}, bf16[2,2,128,512]{3,2,1,0:T(8,128)(2,1)S(1)}, u32[]{:S(2)}, u32[]{:S(2)}) %collective-permute-start.8) | collective-permute-done | bytes 524320 | tf_op jit(solution)/shard_map/ppermute | solution.py:167
  50.4 0.0 collective-permute-start.10
  50.4 0.0 collective-permute-done.19.refs_3_
  50.4 0.5 collective-permute-start.5
  50.9 5.1 %collective-permute-done.4.refs_1_ = bf16[2,2,128,512]{3,2,1,0:T(8,128)(2,1)S(1)} collective-permute-done((bf16[2,2,128,512]{3,2,1,0:T(8,128)(2,1)S(1)}, bf16[2,2,128,512]{3,2,1,0:T(8,128)(2,1)S(1)}, u32[]{:S(2)}, u32[]{:S(2)}) %collective-permute-start.4) | collective-permute-done | bytes 524320 | tf_op jit(solution)/shard_map/ppermute | solution.py:167
  56.0 0.0 collective-permute-start.6
  56.0 3.2 %shard_map.256.refs_4_ = f32[2048,2048]{1,0:T(8,128)S(1)} custom-call(s32[3]{0:T(128)S(1)} %pad_add_fusion.place, bf16[2,2,128,512]{3,2,1,0:T(8,128)(2,1)S(1)} %pad_maximum_fusion.3.refs_0_, bf16[2,2,128,512]{3,2,1,0:T(8,128)(2,1)S(1)} %collective-permute-done.17.refs_1_, bf16[2,2,128,512]{3,2,1,0:T(8,128)(2,1)S(1)} %collective-permute-done.18.refs_2_, ...), custom_call_target="tpu_custom_call" | custom-call | tf_op jit(solution)/shard_map/pallas_call | solution.py:437
  59.2 0.0 collective-permute-done.15.refs_3_
  59.2 3.4 %shard_map.257.refs_4_ = f32[2048,2048]{1,0:T(8,128)S(1)} custom-call(s32[3]{0:T(128)S(1)} %pad_add_fusion.place, bf16[2,2,128,512]{3,2,1,0:T(8,128)(2,1)S(1)} %pad_maximum_fusion.2.refs_0_, bf16[2,2,128,512]{3,2,1,0:T(8,128)(2,1)S(1)} %collective-permute-done.13.refs_1_, ...), custom_call_target="tpu_custom_call", output_to_operand_aliasing={{}: (5, {})} | custom-call | tf_op jit(solution)/shard_map/pallas_call | solution.py:437
  62.6 0.0 collective-permute-done.9.refs_2_
  62.7 0.0 collective-permute-done.10.refs_3_
  62.7 3.4 %shard_map.258.refs_4_ = f32[2048,2048]{1,0:T(8,128)S(1)} custom-call(s32[3]{0:T(128)S(1)} %pad_add_fusion.place, bf16[2,2,128,512]{3,2,1,0:T(8,128)(2,1)S(1)} %pad_maximum_fusion.1.refs_0_, bf16[2,2,128,512]{3,2,1,0:T(8,128)(2,1)S(1)} %collective-permute-done.8.refs_1_, ...), custom_call_target="tpu_custom_call", output_to_operand_aliasing={{}: (5, {})} | custom-call | tf_op jit(solution)/shard_map/pallas_call | solution.py:437
  66.1 9.2 %tail.1 = (f32[256,256]{1,0:T(8,128)}, bf16[256,256]{1,0:T(8,128)(2,1)}, f32[256,256]{1,0:T(8,128)}, f32[256,256]{1,0:T(8,128)}, f32[256,2048]{1,0:T(8,128)}, /*...) custom-call(s32[3]{0:T(128)S(1)} %pad_add_fusion.place, ...), custom_call_target="tpu_custom_call" | custom-call | tf_op jit(solution)/shard_map/tail/pallas_call | solution.py:449
  (3 shorter events, 0.0 us)
Async XLA Ops:
  2.3 1.5 %collective-permute-start = (bf16[128,512]{1,0:T(8,128)(2,1)S(1)}, bf16[128,512]{1,0:T(8,128)(2,1)S(1)}, u32[]{:S(2)}, u32[]{:S(2)}) collective-permute-start(bf16[128,512]{1,0:T(8,128)(2,1)S(1)} %get-tuple-element.27), channel_id=1, source_target_pairs={{0,1},{1,0},{2,3},{3,2},{4,5},{5,4},{6,7},{7,6},{8,9},{9,8},{10,11... | collective-permute-start | bytes 393224 | tf_op jit(solution)/shard_map/ppermute | solution.py:167
  3.9 16.3 %collective-permute-start.1 = (bf16[2,128,512]{2,1,0:T(8,128)(2,1)S(1)}, bf16[2,128,512]{2,1,0:T(8,128)(2,1)S(1)}, u32[]{:S(2)}, u32[]{:S(2)}) collective-permute-start(bf16[2,128,512]{2,1,0:T(8,128)(2,1)S(1)} %get-tuple-element.41), channel_id=1, source_target_pairs={{0,16},{1,17},{2,18},{3,19},{4,20},{5,21},{6,22},{7,23},{8,24},{9,... | collective-permute-start | bytes 786440 | tf_op jit(solution)/shard_map/ppermute | solution.py:167
  7.9 13.0 %collective-permute-start.11 = (bf16[2,128,512]{2,1,0:T(8,128)(2,1)S(1)}, bf16[2,128,512]{2,1,0:T(8,128)(2,1)S(1)}, u32[]{:S(2)}, u32[]{:S(2)}) collective-permute-start(bf16[2,128,512]{2,1,0:T(8,128)(2,1)S(1)} %get-tuple-element.41), channel_id=1, source_target_pairs={{0,8},{1,9},{2,10},{3,11},{4,12},{5,13},{6,14},{7,15},{8,0},{9,1},... | collective-permute-start | bytes 786440 | tf_op jit(solution)/shard_map/ppermute | solution.py:167
  9.5 12.9 %collective-permute-start.16 = (bf16[2,128,512]{2,1,0:T(8,128)(2,1)S(1)}, bf16[2,128,512]{2,1,0:T(8,128)(2,1)S(1)}, u32[]{:S(2)}, u32[]{:S(2)}) collective-permute-start(bf16[2,128,512]{2,1,0:T(8,128)(2,1)S(1)} %get-tuple-element.41), channel_id=1, source_target_pairs={{0,4},{1,3},{2,6},{3,1},{4,0},{5,7},{6,2},{7,5},{8,12},{9,11},{10,... | collective-permute-start | bytes 786440 | tf_op jit(solution)/shard_map/ppermute | solution.py:167
  20.3 7.7 %collective-permute-start.2 = (bf16[2,128,512]{2,1,0:T(8,128)(2,1)S(1)}, bf16[2,128,512]{2,1,0:T(8,128)(2,1)S(1)}, u32[]{:S(2)}, u32[]{:S(2)}) collective-permute-start(bf16[2,128,512]{2,1,0:T(8,128)(2,1)S(1)} %collective-permute-done.1), channel_id=1, source_target_pairs={{0,8},{1,9},{2,10},{3,11},{4,12},{5,13},{6,14},{7,15},{8,0},{9,1},... | collective-permute-start | bytes 786440 | tf_op jit(solution)/shard_map/ppermute | solution.py:167
  20.9 9.0 %collective-permute-start.12 = (bf16[2,128,512]{2,1,0:T(8,128)(2,1)S(1)}, bf16[2,128,512]{2,1,0:T(8,128)(2,1)S(1)}, u32[]{:S(2)}, u32[]{:S(2)}) collective-permute-start(bf16[2,128,512]{2,1,0:T(8,128)(2,1)S(1)} %collective-permute-done.11), channel_id=1, source_target_pairs={{0,4},{1,3},{2,6},{3,1},{4,0},{5,7},{6,2},{7,5},{8,12},{9,11},{10,... | collective-permute-start | bytes 786440 | tf_op jit(solution)/shard_map/ppermute | solution.py:167
  22.5 20.4 %collective-permute-start.17 = (bf16[2,2,128,512]{3,2,1,0:T(8,128)(2,1)S(1)}, bf16[2,2,128,512]{3,2,1,0:T(8,128)(2,1)S(1)}, u32[]{:S(2)}, u32[]{:S(2)}) collective-permute-start(bf16[2,2,128,512]{3,2,1,0:T(8,128)(2,1)S(1)} %pad_maximum_fusion.3.refs_0_), channel_id=1, source_target_pairs={{0,2},{1,5},{2,0},{3,7},{4,6},{5,1},{6,4},{7,3},{8,10},{9,13},{10,... | collective-permute-start | bytes 1572872 | tf_op jit(solution)/shard_map/ppermute | solution.py:167
  24.0 18.9 %collective-permute-start.18 = (bf16[2,2,128,512]{3,2,1,0:T(8,128)(2,1)S(1)}, bf16[2,2,128,512]{3,2,1,0:T(8,128)(2,1)S(1)}, u32[]{:S(2)}, u32[]{:S(2)}) collective-permute-start(bf16[2,2,128,512]{3,2,1,0:T(8,128)(2,1)S(1)} %pad_maximum_fusion.3.refs_0_), channel_id=1, source_target_pairs={{0,1},{1,0},{2,3},{3,2},{4,5},{5,4},{6,7},{7,6},{8,9},{9,8},{10,11... | collective-permute-start | bytes 1572872 | tf_op jit(solution)/shard_map/ppermute | solution.py:167
  24.0 11.5 %collective-permute-start.7 = (bf16[2,128,512]{2,1,0:T(8,128)(2,1)S(1)}, bf16[2,128,512]{2,1,0:T(8,128)(2,1)S(1)}, u32[]{:S(2)}, u32[]{:S(2)}) collective-permute-start(bf16[2,128,512]{2,1,0:T(8,128)(2,1)S(1)} %collective-permute-done.1), channel_id=1, source_target_pairs={{0,4},{1,3},{2,6},{3,1},{4,0},{5,7},{6,2},{7,5},{8,12},{9,11},{10,... | collective-permute-start | bytes 786440 | tf_op jit(solution)/shard_map/ppermute | solution.py:167
  28.0 13.2 %collective-permute-start.3 = (bf16[2,128,512]{2,1,0:T(8,128)(2,1)S(1)}, bf16[2,128,512]{2,1,0:T(8,128)(2,1)S(1)}, u32[]{:S(2)}, u32[]{:S(2)}) collective-permute-start(bf16[2,128,512]{2,1,0:T(8,128)(2,1)S(1)} %collective-permute-done.2), channel_id=1, source_target_pairs={{0,4},{1,3},{2,6},{3,1},{4,0},{5,7},{6,2},{7,5},{8,12},{9,11},{10,... | collective-permute-start | bytes 786440 | tf_op jit(solution)/shard_map/ppermute | solution.py:167
  30.0 13.4 %collective-permute-start.13 = (bf16[2,2,128,512]{3,2,1,0:T(8,128)(2,1)S(1)}, bf16[2,2,128,512]{3,2,1,0:T(8,128)(2,1)S(1)}, u32[]{:S(2)}, u32[]{:S(2)}) collective-permute-start(bf16[2,2,128,512]{3,2,1,0:T(8,128)(2,1)S(1)} %pad_maximum_fusion.2.refs_0_), channel_id=1, source_target_pairs={{0,2},{1,5},{2,0},{3,7},{4,6},{5,1},{6,4},{7,3},{8,10},{9,13},{10,... | collective-permute-start | bytes 1572872 | tf_op jit(solution)/shard_map/ppermute | solution.py:167
  35.6 9.1 %collective-permute-start.14 = (bf16[2,2,128,512]{3,2,1,0:T(8,128)(2,1)S(1)}, bf16[2,2,128,512]{3,2,1,0:T(8,128)(2,1)S(1)}, u32[]{:S(2)}, u32[]{:S(2)}) collective-permute-start(bf16[2,2,128,512]{3,2,1,0:T(8,128)(2,1)S(1)} %pad_maximum_fusion.2.refs_0_), channel_id=1, source_target_pairs={{0,1},{1,0},{2,3},{3,2},{4,5},{5,4},{6,7},{7,6},{8,9},{9,8},{10,11... | collective-permute-start | bytes 1572872 | tf_op jit(solution)/shard_map/ppermute | solution.py:167
  41.2 9.2 %collective-permute-start.8 = (bf16[2,2,128,512]{3,2,1,0:T(8,128)(2,1)S(1)}, bf16[2,2,128,512]{3,2,1,0:T(8,128)(2,1)S(1)}, u32[]{:S(2)}, u32[]{:S(2)}) collective-permute-start(bf16[2,2,128,512]{3,2,1,0:T(8,128)(2,1)S(1)} %pad_maximum_fusion.1.refs_0_), channel_id=1, source_target_pairs={{0,2},{1,5},{2,0},{3,7},{4,6},{5,1},{6,4},{7,3},{8,10},{9,13},{10,... | collective-permute-start | bytes 1572872 | tf_op jit(solution)/shard_map/ppermute | solution.py:167
  42.9 7.5 %collective-permute-start.19 = (bf16[2,2,128,512]{3,2,1,0:T(8,128)(2,1)S(1)}, bf16[2,2,128,512]{3,2,1,0:T(8,128)(2,1)S(1)}, u32[]{:S(2)}, u32[]{:S(2)}) collective-permute-start(bf16[2,2,128,512]{3,2,1,0:T(8,128)(2,1)S(1)} %collective-permute-done.17.refs_1_), channel_id=1, source_target_pairs={{0,1},{1,0},{2,3},{3,2},{4,5},{5,4},{6,7},{7,6},{8,9},{9,8},{10,11... | collective-permute-start | bytes 1572872 | tf_op jit(solution)/shard_map/ppermute | solution.py:167
  43.0 13.0 %collective-permute-start.4 = (bf16[2,2,128,512]{3,2,1,0:T(8,128)(2,1)S(1)}, bf16[2,2,128,512]{3,2,1,0:T(8,128)(2,1)S(1)}, u32[]{:S(2)}, u32[]{:S(2)}) collective-permute-start(bf16[2,2,128,512]{3,2,1,0:T(8,128)(2,1)S(1)} %pad_maximum_fusion.refs_0_), channel_id=1, source_target_pairs={{0,2},{1,5},{2,0},{3,7},{4,6},{5,1},{6,4},{7,3},{8,10},{9,13},{10,... | collective-permute-start | bytes 1572872 | tf_op jit(solution)/shard_map/ppermute | solution.py:167
  43.4 19.2 %collective-permute-start.9 = (bf16[2,2,128,512]{3,2,1,0:T(8,128)(2,1)S(1)}, bf16[2,2,128,512]{3,2,1,0:T(8,128)(2,1)S(1)}, u32[]{:S(2)}, u32[]{:S(2)}) collective-permute-start(bf16[2,2,128,512]{3,2,1,0:T(8,128)(2,1)S(1)} %pad_maximum_fusion.1.refs_0_), channel_id=1, source_target_pairs={{0,1},{1,0},{2,3},{3,2},{4,5},{5,4},{6,7},{7,6},{8,9},{9,8},{10,11... | collective-permute-start | bytes 1572872 | tf_op jit(solution)/shard_map/ppermute | solution.py:167
  44.7 14.5 %collective-permute-start.15 = (bf16[2,2,128,512]{3,2,1,0:T(8,128)(2,1)S(1)}, bf16[2,2,128,512]{3,2,1,0:T(8,128)(2,1)S(1)}, u32[]{:S(2)}, u32[]{:S(2)}) collective-permute-start(bf16[2,2,128,512]{3,2,1,0:T(8,128)(2,1)S(1)} %collective-permute-done.13.refs_1_), channel_id=1, source_target_pairs={{0,1},{1,0},{2,3},{3,2},{4,5},{5,4},{6,7},{7,6},{8,9},{9,8},{10,11... | collective-permute-start | bytes 1572872 | tf_op jit(solution)/shard_map/ppermute | solution.py:167
  50.4 12.3 %collective-permute-start.10 = (bf16[2,2,128,512]{3,2,1,0:T(8,128)(2,1)S(1)}, bf16[2,2,128,512]{3,2,1,0:T(8,128)(2,1)S(1)}, u32[]{:S(2)}, u32[]{:S(2)}) collective-permute-start(bf16[2,2,128,512]{3,2,1,0:T(8,128)(2,1)S(1)} %collective-permute-done.8.refs_1_), channel_id=1, source_target_pairs={{0,1},{1,0},{2,3},{3,2},{4,5},{5,4},{6,7},{7,6},{8,9},{9,8},{10,11... | collective-permute-start | bytes 1572872 | tf_op jit(solution)/shard_map/ppermute | solution.py:167
  50.4 15.7 %collective-permute-start.5 = (bf16[2,2,128,512]{3,2,1,0:T(8,128)(2,1)S(1)}, bf16[2,2,128,512]{3,2,1,0:T(8,128)(2,1)S(1)}, u32[]{:S(2)}, u32[]{:S(2)}) collective-permute-start(bf16[2,2,128,512]{3,2,1,0:T(8,128)(2,1)S(1)} %pad_maximum_fusion.refs_0_), channel_id=1, source_target_pairs={{0,1},{1,0},{2,3},{3,2},{4,5},{5,4},{6,7},{7,6},{8,9},{9,8},{10,11... | collective-permute-start | bytes 1572872 | tf_op jit(solution)/shard_map/ppermute | solution.py:167
  56.0 10.1 %collective-permute-start.6 = (bf16[2,2,128,512]{3,2,1,0:T(8,128)(2,1)S(1)}, bf16[2,2,128,512]{3,2,1,0:T(8,128)(2,1)S(1)}, u32[]{:S(2)}, u32[]{:S(2)}) collective-permute-start(bf16[2,2,128,512]{3,2,1,0:T(8,128)(2,1)S(1)} %collective-permute-done.4.refs_1_), channel_id=1, source_target_pairs={{0,1},{1,0},{2,3},{3,2},{4,5},{5,4},{6,7},{7,6},{8,9},{9,8},{10,11... | collective-permute-start | bytes 1572872 | tf_op jit(solution)/shard_map/ppermute | solution.py:167

commit v2 on v1

--- a/solution.py
+++ b/solution.py
@@ -181,8 +181,13 @@
         source = lanes[k ^ step]
         lanes.append(move(source, lambda f, t, step=step: (f ^ (2 * step), t)))
     sets = []
-    for lane in lanes:
-        pair = jnp.stack([lane, move(lane, first_hop)])
+    nears = []
+    for s, lane in enumerate(lanes):
+        if s & 1:
+            nears.append(move(nears[s ^ 1], lambda f, t: (f ^ 2, t)))
+        else:
+            nears.append(move(lane, first_hop))
+        pair = jnp.stack([lane, nears[s]])
         far = move(pair, second_hop)
         sets.append((pair, far, move(pair, partner), move(far, partner)))
     return sets

time: 75.8 us -> 74.8 us (0.987)
  starting transfers between devices: 18.9 us -> 17.7 us
    ppermute x20, starting transfers between devices: 18.9 us -> 17.7 us  [move(): return lax.ppermute(value, axes, linear_pairs(fs_size, tp_size, target))]
where the time goes in v2:
time: 74.8 us; the launch traced here: 74.5 us
  waiting for transfers between devices  34.8 us (47%)
  Pallas kernels  20.9 us (28%)
  starting transfers between devices  17.7 us (24%)
  between operations  0.94 us (1%)
    ppermute x20, waiting for transfers between devices, move(): return lax.ppermute(value, axes, linear_pairs(fs_size, tp_size, target))  34.8 us
    ppermute x20, starting transfers between devices, move(): return lax.ppermute(value, axes, linear_pairs(fs_size, tp_size, target))  17.7 us
    pallas_call x3, Pallas kernels, gathered_plan(): pl.pallas_call(partial(sum_kernel, not acc), out_shape=pltpu.VMEM((model,...  10 us
    pallas_call x1, Pallas kernels, gathered_plan(): pl.pallas_call(tail_kernel, out_shape=kinds * 2, in_specs=[smem] + [anywh...  9.24 us
    pallas_call x1, Pallas kernels, gathered_plan(): pl.pallas_call(prepare_kernel, out_shape=(pltpu.VMEM(inputs.shape, inputs...  1.61 us
  transfers between devices with their start and end apart: 20, of which 8 were waited for; matrix products, arithmetic and copies ran while one was open for 0% of the time, Pallas kernels for 13%

profile of v2, /device:TPU:0, one launch (start us, length us, event | category | flops | bytes accessed | tf_op | source)
XLA Modules:
  0.0 74.5 jit_solution(8516810502026486064)
XLA Ops:
  0.6 0.1 pad_add_fusion.place
  0.7 1.6 %prepare.1 = (bf16[128,512]{1,0:T(8,128)(2,1)S(1)}, bf16[128,512]{1,0:T(8,128)(2,1)S(1)}) custom-call(s32[3]{0:T(128)S(1)} %pad_add_fusion.place, bf16[128,512]{1,0:T(8,128)(2,1)} %refs_0_.1, bf16[128,256]{1,0:T(8,128)(2,1)} %refs_1_.1, bf16[128,256]{1,0:T(8,128)(2,1)} %refs_2_.1, bf16[128,256]{1,0:T(8,128)(2,1)} %refs_3_.1, f32[1,256]{1,0:T(1,128)} %bitcast.24), custom_call_target="tpu_custom_call" | custom-call | tf_op jit(solution)/shard_map/prepare/pallas_call | solution.py:408
  2.3 0.6 collective-permute-start
  2.9 1.0 %collective-permute-done = bf16[128,512]{1,0:T(8,128)(2,1)S(1)} collective-permute-done((bf16[128,512]{1,0:T(8,128)(2,1)S(1)}, bf16[128,512]{1,0:T(8,128)(2,1)S(1)}, u32[]{:S(2)}, u32[]{:S(2)}) %collective-permute-start) | collective-permute-done | bytes 131104 | tf_op jit(solution)/shard_map/ppermute | solution.py:167
  3.9 4.0 %collective-permute-start.1 = (bf16[2,128,512]{2,1,0:T(8,128)(2,1)S(1)}, bf16[2,128,512]{2,1,0:T(8,128)(2,1)S(1)}, u32[]{:S(2)}, u32[]{:S(2)}) collective-permute-start(bf16[2,128,512]{2,1,0:T(8,128)(2,1)S(1)} %get-tuple-element.41), channel_id=1, source_target_pairs={{0,16},{1,17},{2,18},{3,19},{4,20},{5,21},{6,22},{7,23},{8,24},{9,... | collective-permute-start | bytes 786440 | tf_op jit(solution)/shard_map/ppermute | solution.py:167
  7.9 1.5 %collective-permute-start.12 = (bf16[2,128,512]{2,1,0:T(8,128)(2,1)S(1)}, bf16[2,128,512]{2,1,0:T(8,128)(2,1)S(1)}, u32[]{:S(2)}, u32[]{:S(2)}) collective-permute-start(bf16[2,128,512]{2,1,0:T(8,128)(2,1)S(1)} %get-tuple-element.41), channel_id=1, source_target_pairs={{0,4},{1,3},{2,6},{3,1},{4,0},{5,7},{6,2},{7,5},{8,12},{9,11},{10,... | collective-permute-start | bytes 786440 | tf_op jit(solution)/shard_map/ppermute | solution.py:167
  9.4 1.6 %collective-permute-start.11 = (bf16[2,128,512]{2,1,0:T(8,128)(2,1)S(1)}, bf16[2,128,512]{2,1,0:T(8,128)(2,1)S(1)}, u32[]{:S(2)}, u32[]{:S(2)}) collective-permute-start(bf16[2,128,512]{2,1,0:T(8,128)(2,1)S(1)} %get-tuple-element.41), channel_id=1, source_target_pairs={{0,8},{1,9},{2,10},{3,11},{4,12},{5,13},{6,14},{7,15},{8,0},{9,1},... | collective-permute-start | bytes 786440 | tf_op jit(solution)/shard_map/ppermute | solution.py:167
  11.0 9.3 %collective-permute-done.1 = bf16[2,128,512]{2,1,0:T(8,128)(2,1)S(1)} collective-permute-done((bf16[2,128,512]{2,1,0:T(8,128)(2,1)S(1)}, bf16[2,128,512]{2,1,0:T(8,128)(2,1)S(1)}, u32[]{:S(2)}, u32[]{:S(2)}) %collective-permute-start.1) | collective-permute-done | bytes 262176 | tf_op jit(solution)/shard_map/ppermute | solution.py:167
  20.3 1.5 %collective-permute-start.3 = (bf16[2,128,512]{2,1,0:T(8,128)(2,1)S(1)}, bf16[2,128,512]{2,1,0:T(8,128)(2,1)S(1)}, u32[]{:S(2)}, u32[]{:S(2)}) collective-permute-start(bf16[2,128,512]{2,1,0:T(8,128)(2,1)S(1)} %collective-permute-done.1), channel_id=1, source_target_pairs={{0,4},{1,3},{2,6},{3,1},{4,0},{5,7},{6,2},{7,5},{8,12},{9,11},{10,... | collective-permute-start | bytes 786440 | tf_op jit(solution)/shard_map/ppermute | solution.py:167
  21.8 0.0 collective-permute-done.12
  21.8 0.6 collective-permute-start.13
  22.4 0.1 pad_maximum_fusion.3.refs_0_
  22.5 1.5 %collective-permute-start.17 = (bf16[2,2,128,512]{3,2,1,0:T(8,128)(2,1)S(1)}, bf16[2,2,128,512]{3,2,1,0:T(8,128)(2,1)S(1)}, u32[]{:S(2)}, u32[]{:S(2)}) collective-permute-start(bf16[2,2,128,512]{3,2,1,0:T(8,128)(2,1)S(1)} %pad_maximum_fusion.3.refs_0_), channel_id=1, source_target_pairs={{0,2},{1,5},{2,0},{3,7},{4,6},{5,1},{6,4},{7,3},{8,10},{9,13},{10,... | collective-permute-start | bytes 1572872 | tf_op jit(solution)/shard_map/ppermute | solution.py:167
  24.0 0.0 collective-permute-start.18
  24.0 0.0 collective-permute-done.11
  24.0 1.4 %collective-permute-start.2 = (bf16[2,128,512]{2,1,0:T(8,128)(2,1)S(1)}, bf16[2,128,512]{2,1,0:T(8,128)(2,1)S(1)}, u32[]{:S(2)}, u32[]{:S(2)}) collective-permute-start(bf16[2,128,512]{2,1,0:T(8,128)(2,1)S(1)} %collective-permute-done.1), channel_id=1, source_target_pairs={{0,8},{1,9},{2,10},{3,11},{4,12},{5,13},{6,14},{7,15},{8,0},{9,1},... | collective-permute-start | bytes 786440 | tf_op jit(solution)/shard_map/ppermute | solution.py:167
  25.5 3.2 %collective-permute-done.3 = bf16[2,128,512]{2,1,0:T(8,128)(2,1)S(1)} collective-permute-done((bf16[2,128,512]{2,1,0:T(8,128)(2,1)S(1)}, bf16[2,128,512]{2,1,0:T(8,128)(2,1)S(1)}, u32[]{:S(2)}, u32[]{:S(2)}) %collective-permute-start.3) | collective-permute-done | bytes 262176 | tf_op jit(solution)/shard_map/ppermute | solution.py:167
  28.7 0.7 collective-permute-start.4
  29.4 1.5 %collective-permute-done.13 = bf16[2,128,512]{2,1,0:T(8,128)(2,1)S(1)} collective-permute-done((bf16[2,128,512]{2,1,0:T(8,128)(2,1)S(1)}, bf16[2,128,512]{2,1,0:T(8,128)(2,1)S(1)}, u32[]{:S(2)}, u32[]{:S(2)}) %collective-permute-start.13) | collective-permute-done | bytes 262176 | tf_op jit(solution)/shard_map/ppermute | solution.py:167
  30.9 0.1 pad_maximum_fusion.2.refs_0_
  30.9 1.0 %collective-permute-start.14 = (bf16[2,2,128,512]{3,2,1,0:T(8,128)(2,1)S(1)}, bf16[2,2,128,512]{3,2,1,0:T(8,128)(2,1)S(1)}, u32[]{:S(2)}, u32[]{:S(2)}) collective-permute-start(bf16[2,2,128,512]{3,2,1,0:T(8,128)(2,1)S(1)} %pad_maximum_fusion.2.refs_0_), channel_id=1, source_target_pairs={{0,2},{1,5},{2,0},{3,7},{4,6},{5,1},{6,4},{7,3},{8,10},{9,13},{10,... | collective-permute-start | bytes 1572872 | tf_op jit(solution)/shard_map/ppermute | solution.py:167
  31.9 0.1 pad_maximum_fusion.1.refs_0_
  32.0 4.5 %collective-permute-done.2 = bf16[2,128,512]{2,1,0:T(8,128)(2,1)S(1)} collective-permute-done((bf16[2,128,512]{2,1,0:T(8,128)(2,1)S(1)}, bf16[2,128,512]{2,1,0:T(8,128)(2,1)S(1)}, u32[]{:S(2)}, u32[]{:S(2)}) %collective-permute-start.2) | collective-permute-done | bytes 262176 | tf_op jit(solution)/shard_map/ppermute | solution.py:167
  36.5 0.0 collective-permute-start.15
  36.5 3.7 %collective-permute-done.4 = bf16[2,128,512]{2,1,0:T(8,128)(2,1)S(1)} collective-permute-done((bf16[2,128,512]{2,1,0:T(8,128)(2,1)S(1)}, bf16[2,128,512]{2,1,0:T(8,128)(2,1)S(1)}, u32[]{:S(2)}, u32[]{:S(2)}) %collective-permute-start.4) | collective-permute-done | bytes 262176 | tf_op jit(solution)/shard_map/ppermute | solution.py:167
  40.2 0.7 collective-permute-start.8
  41.0 0.1 pad_maximum_fusion.refs_0_
  41.0 0.0 collective-permute-done.17.refs_1_
  41.0 0.1 collective-permute-start.19
  41.1 0.0 collective-permute-done.18.refs_2_
  41.1 1.4 %collective-permute-start.5 = (bf16[2,2,128,512]{3,2,1,0:T(8,128)(2,1)S(1)}, bf16[2,2,128,512]{3,2,1,0:T(8,128)(2,1)S(1)}, u32[]{:S(2)}, u32[]{:S(2)}) collective-permute-start(bf16[2,2,128,512]{3,2,1,0:T(8,128)(2,1)S(1)} %pad_maximum_fusion.refs_0_), channel_id=1, source_target_pairs={{0,2},{1,5},{2,0},{3,7},{4,6},{5,1},{6,4},{7,3},{8,10},{9,13},{10,... | collective-permute-start | bytes 1572872 | tf_op jit(solution)/shard_map/ppermute | solution.py:167
  42.5 0.0 collective-permute-done.14.refs_1_
  42.5 0.1 collective-permute-start.9
  42.6 0.0 collective-permute-done.15.refs_2_
  42.6 0.4 collective-permute-start.16
  43.0 6.4 %collective-permute-done.8.refs_1_ = bf16[2,2,128,512]{3,2,1,0:T(8,128)(2,1)S(1)} collective-permute-done((bf16[2,2,128,512]{3,2,1,0:T(8,128)(2,1)S(1)}, bf16[2,2,128,512]{3,2,1,0:T(8,128)(2,1)S(1)}, u32[]{:S(2)}, u32[]{:S(2)}) %collective-permute-start.8) | collective-permute-done | bytes 524320 | tf_op jit(solution)/shard_map/ppermute | solution.py:167
  49.4 0.0 collective-permute-start.10
  49.4 0.0 collective-permute-done.19.refs_3_
  49.4 0.5 collective-permute-start.6
  49.9 5.1 %collective-permute-done.5.refs_1_ = bf16[2,2,128,512]{3,2,1,0:T(8,128)(2,1)S(1)} collective-permute-done((bf16[2,2,128,512]{3,2,1,0:T(8,128)(2,1)S(1)}, bf16[2,2,128,512]{3,2,1,0:T(8,128)(2,1)S(1)}, u32[]{:S(2)}, u32[]{:S(2)}) %collective-permute-start.5) | collective-permute-done | bytes 524320 | tf_op jit(solution)/shard_map/ppermute | solution.py:167
  55.0 0.0 collective-permute-start.7
  55.0 3.2 %shard_map.256.refs_4_ = f32[2048,2048]{1,0:T(8,128)S(1)} custom-call(s32[3]{0:T(128)S(1)} %pad_add_fusion.place, bf16[2,2,128,512]{3,2,1,0:T(8,128)(2,1)S(1)} %pad_maximum_fusion.3.refs_0_, bf16[2,2,128,512]{3,2,1,0:T(8,128)(2,1)S(1)} %collective-permute-done.17.refs_1_, bf16[2,2,128,512]{3,2,1,0:T(8,128)(2,1)S(1)} %collective-permute-done.18.refs_2_, ...), custom_call_target="tpu_custom_call" | custom-call | tf_op jit(solution)/shard_map/pallas_call | solution.py:442
  58.3 3.4 %shard_map.257.refs_4_ = f32[2048,2048]{1,0:T(8,128)S(1)} custom-call(s32[3]{0:T(128)S(1)} %pad_add_fusion.place, bf16[2,2,128,512]{3,2,1,0:T(8,128)(2,1)S(1)} %pad_maximum_fusion.2.refs_0_, bf16[2,2,128,512]{3,2,1,0:T(8,128)(2,1)S(1)} %collective-permute-done.14.refs_1_, ...), custom_call_target="tpu_custom_call", output_to_operand_aliasing={{}: (5, {})} | custom-call | tf_op jit(solution)/shard_map/pallas_call | solution.py:442
  61.7 0.0 collective-permute-done.9.refs_2_
  61.7 3.4 %shard_map.258.refs_4_ = f32[2048,2048]{1,0:T(8,128)S(1)} custom-call(s32[3]{0:T(128)S(1)} %pad_add_fusion.place, bf16[2,2,128,512]{3,2,1,0:T(8,128)(2,1)S(1)} %pad_maximum_fusion.1.refs_0_, bf16[2,2,128,512]{3,2,1,0:T(8,128)(2,1)S(1)} %collective-permute-done.8.refs_1_, ...), custom_call_target="tpu_custom_call", output_to_operand_aliasing={{}: (5, {})} | custom-call | tf_op jit(solution)/shard_map/pallas_call | solution.py:442
  65.1 0.0 collective-permute-done.6.refs_2_
  65.1 0.0 collective-permute-done.7.refs_3_
  65.2 9.2 %tail.1 = (f32[256,256]{1,0:T(8,128)}, bf16[256,256]{1,0:T(8,128)(2,1)}, f32[256,256]{1,0:T(8,128)}, f32[256,256]{1,0:T(8,128)}, f32[256,2048]{1,0:T(8,128)}, /*...) custom-call(s32[3]{0:T(128)S(1)} %pad_add_fusion.place, ...), custom_call_target="tpu_custom_call" | custom-call | tf_op jit(solution)/shard_map/tail/pallas_call | solution.py:454
  (3 shorter events, 0.0 us)
Async XLA Ops:
  2.3 1.5 %collective-permute-start = (bf16[128,512]{1,0:T(8,128)(2,1)S(1)}, bf16[128,512]{1,0:T(8,128)(2,1)S(1)}, u32[]{:S(2)}, u32[]{:S(2)}) collective-permute-start(bf16[128,512]{1,0:T(8,128)(2,1)S(1)} %get-tuple-element.27), channel_id=1, source_target_pairs={{0,1},{1,0},{2,3},{3,2},{4,5},{5,4},{6,7},{7,6},{8,9},{9,8},{10,11... | collective-permute-start | bytes 393224 | tf_op jit(solution)/shard_map/ppermute | solution.py:167
  3.9 16.3 %collective-permute-start.1 = (bf16[2,128,512]{2,1,0:T(8,128)(2,1)S(1)}, bf16[2,128,512]{2,1,0:T(8,128)(2,1)S(1)}, u32[]{:S(2)}, u32[]{:S(2)}) collective-permute-start(bf16[2,128,512]{2,1,0:T(8,128)(2,1)S(1)} %get-tuple-element.41), channel_id=1, source_target_pairs={{0,16},{1,17},{2,18},{3,19},{4,20},{5,21},{6,22},{7,23},{8,24},{9,... | collective-permute-start | bytes 786440 | tf_op jit(solution)/shard_map/ppermute | solution.py:167
  7.9 13.9 %collective-permute-start.12 = (bf16[2,128,512]{2,1,0:T(8,128)(2,1)S(1)}, bf16[2,128,512]{2,1,0:T(8,128)(2,1)S(1)}, u32[]{:S(2)}, u32[]{:S(2)}) collective-permute-start(bf16[2,128,512]{2,1,0:T(8,128)(2,1)S(1)} %get-tuple-element.41), channel_id=1, source_target_pairs={{0,4},{1,3},{2,6},{3,1},{4,0},{5,7},{6,2},{7,5},{8,12},{9,11},{10,... | collective-permute-start | bytes 786440 | tf_op jit(solution)/shard_map/ppermute | solution.py:167
  9.4 14.6 %collective-permute-start.11 = (bf16[2,128,512]{2,1,0:T(8,128)(2,1)S(1)}, bf16[2,128,512]{2,1,0:T(8,128)(2,1)S(1)}, u32[]{:S(2)}, u32[]{:S(2)}) collective-permute-start(bf16[2,128,512]{2,1,0:T(8,128)(2,1)S(1)} %get-tuple-element.41), channel_id=1, source_target_pairs={{0,8},{1,9},{2,10},{3,11},{4,12},{5,13},{6,14},{7,15},{8,0},{9,1},... | collective-permute-start | bytes 786440 | tf_op jit(solution)/shard_map/ppermute | solution.py:167
  20.3 8.4 %collective-permute-start.3 = (bf16[2,128,512]{2,1,0:T(8,128)(2,1)S(1)}, bf16[2,128,512]{2,1,0:T(8,128)(2,1)S(1)}, u32[]{:S(2)}, u32[]{:S(2)}) collective-permute-start(bf16[2,128,512]{2,1,0:T(8,128)(2,1)S(1)} %collective-permute-done.1), channel_id=1, source_target_pairs={{0,4},{1,3},{2,6},{3,1},{4,0},{5,7},{6,2},{7,5},{8,12},{9,11},{10,... | collective-permute-start | bytes 786440 | tf_op jit(solution)/shard_map/ppermute | solution.py:167
  21.8 9.1 %collective-permute-start.13 = (bf16[2,128,512]{2,1,0:T(8,128)(2,1)S(1)}, bf16[2,128,512]{2,1,0:T(8,128)(2,1)S(1)}, u32[]{:S(2)}, u32[]{:S(2)}) collective-permute-start(bf16[2,128,512]{2,1,0:T(8,128)(2,1)S(1)} %collective-permute-done.12), channel_id=1, source_target_pairs={{0,8},{1,9},{2,10},{3,11},{4,12},{5,13},{6,14},{7,15},{8,0},{9,1},... | collective-permute-start | bytes 786440 | tf_op jit(solution)/shard_map/ppermute | solution.py:167
  22.5 18.5 %collective-permute-start.17 = (bf16[2,2,128,512]{3,2,1,0:T(8,128)(2,1)S(1)}, bf16[2,2,128,512]{3,2,1,0:T(8,128)(2,1)S(1)}, u32[]{:S(2)}, u32[]{:S(2)}) collective-permute-start(bf16[2,2,128,512]{3,2,1,0:T(8,128)(2,1)S(1)} %pad_maximum_fusion.3.refs_0_), channel_id=1, source_target_pairs={{0,2},{1,5},{2,0},{3,7},{4,6},{5,1},{6,4},{7,3},{8,10},{9,13},{10,... | collective-permute-start | bytes 1572872 | tf_op jit(solution)/shard_map/ppermute | solution.py:167
  24.0 17.1 %collective-permute-start.18 = (bf16[2,2,128,512]{3,2,1,0:T(8,128)(2,1)S(1)}, bf16[2,2,128,512]{3,2,1,0:T(8,128)(2,1)S(1)}, u32[]{:S(2)}, u32[]{:S(2)}) collective-permute-start(bf16[2,2,128,512]{3,2,1,0:T(8,128)(2,1)S(1)} %pad_maximum_fusion.3.refs_0_), channel_id=1, source_target_pairs={{0,1},{1,0},{2,3},{3,2},{4,5},{5,4},{6,7},{7,6},{8,9},{9,8},{10,11... | collective-permute-start | bytes 1572872 | tf_op jit(solution)/shard_map/ppermute | solution.py:167
  24.0 12.5 %collective-permute-start.2 = (bf16[2,128,512]{2,1,0:T(8,128)(2,1)S(1)}, bf16[2,128,512]{2,1,0:T(8,128)(2,1)S(1)}, u32[]{:S(2)}, u32[]{:S(2)}) collective-permute-start(bf16[2,128,512]{2,1,0:T(8,128)(2,1)S(1)} %collective-permute-done.1), channel_id=1, source_target_pairs={{0,8},{1,9},{2,10},{3,11},{4,12},{5,13},{6,14},{7,15},{8,0},{9,1},... | collective-permute-start | bytes 786440 | tf_op jit(solution)/shard_map/ppermute | solution.py:167
  28.7 11.6 %collective-permute-start.4 = (bf16[2,128,512]{2,1,0:T(8,128)(2,1)S(1)}, bf16[2,128,512]{2,1,0:T(8,128)(2,1)S(1)}, u32[]{:S(2)}, u32[]{:S(2)}) collective-permute-start(bf16[2,128,512]{2,1,0:T(8,128)(2,1)S(1)} %collective-permute-done.3), channel_id=1, source_target_pairs={{0,8},{1,9},{2,10},{3,11},{4,12},{5,13},{6,14},{7,15},{8,0},{9,1},... | collective-permute-start | bytes 786440 | tf_op jit(solution)/shard_map/ppermute | solution.py:167
  30.9 11.6 %collective-permute-start.14 = (bf16[2,2,128,512]{3,2,1,0:T(8,128)(2,1)S(1)}, bf16[2,2,128,512]{3,2,1,0:T(8,128)(2,1)S(1)}, u32[]{:S(2)}, u32[]{:S(2)}) collective-permute-start(bf16[2,2,128,512]{3,2,1,0:T(8,128)(2,1)S(1)} %pad_maximum_fusion.2.refs_0_), channel_id=1, source_target_pairs={{0,2},{1,5},{2,0},{3,7},{4,6},{5,1},{6,4},{7,3},{8,10},{9,13},{10,... | collective-permute-start | bytes 1572872 | tf_op jit(solution)/shard_map/ppermute | solution.py:167
  36.5 6.1 %collective-permute-start.15 = (bf16[2,2,128,512]{3,2,1,0:T(8,128)(2,1)S(1)}, bf16[2,2,128,512]{3,2,1,0:T(8,128)(2,1)S(1)}, u32[]{:S(2)}, u32[]{:S(2)}) collective-permute-start(bf16[2,2,128,512]{3,2,1,0:T(8,128)(2,1)S(1)} %pad_maximum_fusion.2.refs_0_), channel_id=1, source_target_pairs={{0,1},{1,0},{2,3},{3,2},{4,5},{5,4},{6,7},{7,6},{8,9},{9,8},{10,11... | collective-permute-start | bytes 1572872 | tf_op jit(solution)/shard_map/ppermute | solution.py:167
  40.2 9.2 %collective-permute-start.8 = (bf16[2,2,128,512]{3,2,1,0:T(8,128)(2,1)S(1)}, bf16[2,2,128,512]{3,2,1,0:T(8,128)(2,1)S(1)}, u32[]{:S(2)}, u32[]{:S(2)}) collective-permute-start(bf16[2,2,128,512]{3,2,1,0:T(8,128)(2,1)S(1)} %pad_maximum_fusion.1.refs_0_), channel_id=1, source_target_pairs={{0,2},{1,5},{2,0},{3,7},{4,6},{5,1},{6,4},{7,3},{8,10},{9,13},{10,... | collective-permute-start | bytes 1572872 | tf_op jit(solution)/shard_map/ppermute | solution.py:167
  41.0 8.4 %collective-permute-start.19 = (bf16[2,2,128,512]{3,2,1,0:T(8,128)(2,1)S(1)}, bf16[2,2,128,512]{3,2,1,0:T(8,128)(2,1)S(1)}, u32[]{:S(2)}, u32[]{:S(2)}) collective-permute-start(bf16[2,2,128,512]{3,2,1,0:T(8,128)(2,1)S(1)} %collective-permute-done.17.refs_1_), channel_id=1, source_target_pairs={{0,1},{1,0},{2,3},{3,2},{4,5},{5,4},{6,7},{7,6},{8,9},{9,8},{10,11... | collective-permute-start | bytes 1572872 | tf_op jit(solution)/shard_map/ppermute | solution.py:167
  41.1 13.9 %collective-permute-start.5 = (bf16[2,2,128,512]{3,2,1,0:T(8,128)(2,1)S(1)}, bf16[2,2,128,512]{3,2,1,0:T(8,128)(2,1)S(1)}, u32[]{:S(2)}, u32[]{:S(2)}) collective-permute-start(bf16[2,2,128,512]{3,2,1,0:T(8,128)(2,1)S(1)} %pad_maximum_fusion.refs_0_), channel_id=1, source_target_pairs={{0,2},{1,5},{2,0},{3,7},{4,6},{5,1},{6,4},{7,3},{8,10},{9,13},{10,... | collective-permute-start | bytes 1572872 | tf_op jit(solution)/shard_map/ppermute | solution.py:167
  42.5 19.2 %collective-permute-start.9 = (bf16[2,2,128,512]{3,2,1,0:T(8,128)(2,1)S(1)}, bf16[2,2,128,512]{3,2,1,0:T(8,128)(2,1)S(1)}, u32[]{:S(2)}, u32[]{:S(2)}) collective-permute-start(bf16[2,2,128,512]{3,2,1,0:T(8,128)(2,1)S(1)} %pad_maximum_fusion.1.refs_0_), channel_id=1, source_target_pairs={{0,1},{1,0},{2,3},{3,2},{4,5},{5,4},{6,7},{7,6},{8,9},{9,8},{10,11... | collective-permute-start | bytes 1572872 | tf_op jit(solution)/shard_map/ppermute | solution.py:167
  42.6 15.7 %collective-permute-start.16 = (bf16[2,2,128,512]{3,2,1,0:T(8,128)(2,1)S(1)}, bf16[2,2,128,512]{3,2,1,0:T(8,128)(2,1)S(1)}, u32[]{:S(2)}, u32[]{:S(2)}) collective-permute-start(bf16[2,2,128,512]{3,2,1,0:T(8,128)(2,1)S(1)} %collective-permute-done.14.refs_1_), channel_id=1, source_target_pairs={{0,1},{1,0},{2,3},{3,2},{4,5},{5,4},{6,7},{7,6},{8,9},{9,8},{10,11... | collective-permute-start | bytes 1572872 | tf_op jit(solution)/shard_map/ppermute | solution.py:167
  49.4 12.3 %collective-permute-start.10 = (bf16[2,2,128,512]{3,2,1,0:T(8,128)(2,1)S(1)}, bf16[2,2,128,512]{3,2,1,0:T(8,128)(2,1)S(1)}, u32[]{:S(2)}, u32[]{:S(2)}) collective-permute-start(bf16[2,2,128,512]{3,2,1,0:T(8,128)(2,1)S(1)} %collective-permute-done.8.refs_1_), channel_id=1, source_target_pairs={{0,1},{1,0},{2,3},{3,2},{4,5},{5,4},{6,7},{7,6},{8,9},{9,8},{10,11... | collective-permute-start | bytes 1572872 | tf_op jit(solution)/shard_map/ppermute | solution.py:167
  49.4 15.7 %collective-permute-start.6 = (bf16[2,2,128,512]{3,2,1,0:T(8,128)(2,1)S(1)}, bf16[2,2,128,512]{3,2,1,0:T(8,128)(2,1)S(1)}, u32[]{:S(2)}, u32[]{:S(2)}) collective-permute-start(bf16[2,2,128,512]{3,2,1,0:T(8,128)(2,1)S(1)} %pad_maximum_fusion.refs_0_), channel_id=1, source_target_pairs={{0,1},{1,0},{2,3},{3,2},{4,5},{5,4},{6,7},{7,6},{8,9},{9,8},{10,11... | collective-permute-start | bytes 1572872 | tf_op jit(solution)/shard_map/ppermute | solution.py:167
  55.0 10.1 %collective-permute-start.7 = (bf16[2,2,128,512]{3,2,1,0:T(8,128)(2,1)S(1)}, bf16[2,2,128,512]{3,2,1,0:T(8,128)(2,1)S(1)}, u32[]{:S(2)}, u32[]{:S(2)}) collective-permute-start(bf16[2,2,128,512]{3,2,1,0:T(8,128)(2,1)S(1)} %collective-permute-done.5.refs_1_), channel_id=1, source_target_pairs={{0,1},{1,0},{2,3},{3,2},{4,5},{5,4},{6,7},{7,6},{8,9},{9,8},{10,11... | collective-permute-start | bytes 1572872 | tf_op jit(solution)/shard_map/ppermute | solution.py:167

commit v3 on v2

--- a/solution.py
+++ b/solution.py
@@ -273,10 +273,10 @@
         ]
         for i in range(2)
     ]
-    for side in loads:
-        for copy in side:
-            copy.start()
     assembled(x_set, y_set, sem)
+    for j in (1, 2, 3, 4, 5, 0):
+        for side in loads:
+            side[j].start()
 
     chunk = x_set.shape[0]
     squares = [jnp.zeros((8, chunk), jnp.float32)] * 2
@@ -287,42 +287,34 @@
         squares[at // hidden] += jnp.sum((part * part).reshape(-1, 8, chunk), axis=0)
 
     stores = []
-    first = pl.multiple_of(band * rows_here, rows_here)
+
+    def store(src, dst, at):
+        stores.append(pltpu.make_async_copy(src, dst, store_sem.at[at]))
+        stores[-1].start()
+
+    scales = []
     for i in range(2):
-        rows, row_root, weight, moment, cols, col_root = held[i][:6]
-        master_out, copy_out, step_out, moment_out = held[i][6:]
-        for copy in loads[i]:
-            copy.wait()
+        _, row_root, weight, moment, cols, col_root = held[i][:6]
+        results = held[i][6:]
         square = jnp.sum(squares[i], keepdims=True)
         scale = jnp.sqrt(model * hidden / (square + 1.0))
-        twice = scale * scale
+        scales.append(scale)
         mine = pl.multiple_of(i * hidden + odd * own, own)
-        band_grad = grad[pl.ds(first, rows_here), i * hidden : (i + 1) * hidden]
-        row_factor = (1.0 - stat_decay) / hidden * twice
-
-        for at in range(0, model, own * 2):
-            part = lax.dot_general(
-                band_grad,
-                grad[at : at + own * 2, i * hidden : (i + 1) * hidden],
-                (((1,), (1,)), ((), ())),
-                preferred_element_type=jnp.float32,
-            )
-            to = slice(at, at + own * 2)
-            rows[:, to] = stat_decay * rows[:, to] + row_factor * part
-        stores.append(pltpu.make_async_copy(rows, outs[i][4], store_sem.at[i, 4]))
-        stores[-1].start()
         own_grad = grad[:, pl.ds(mine, own)]
+        loads[i][1].wait()
+        left = jnp.dot(row_root[...], own_grad, preferred_element_type=jnp.float32)
+        left_high = left.astype(jnp.bfloat16)
+        left_low = (left - left_high.astype(jnp.float32)).astype(jnp.bfloat16)
         column_total = lax.dot_general(
             own_grad, own_grad, (((0,), (0,)), ((), ())), preferred_element_type=jnp.float32
         )
-        left = jnp.dot(row_root[...], own_grad, preferred_element_type=jnp.float32)
-        left_high = left.astype(jnp.bfloat16)
-        left_low = (left - left_high.astype(jnp.float32)).astype(jnp.bfloat16)
+        for copy in loads[i][2:]:
+            copy.wait()
         for h in range(own // HEAD):
             at = slice(h * HEAD, (h + 1) * HEAD)
             cols[h] = (
                 stat_decay * cols[h]
-                + (1.0 - stat_decay) / model * twice * column_total[at, at]
+                + (1.0 - stat_decay) / model * scale * scale * column_total[at, at]
             )
             root = col_root[h]
             precond = scale * (
@@ -332,13 +324,32 @@
             moment_next = moment_decay * moment[:, at] + (1.0 - moment_decay) * precond
             update_step = moment_decay * moment_next + (1.0 - moment_decay) * precond
             master = weight[:, at] - learn_rate * update_step
-            master_out[:, at] = master
-            copy_out[:, at] = master.astype(jnp.bfloat16)
-            step_out[:, at] = update_step
-            moment_out[:, at] = moment_next
-        for src, dst in ((master_out, 0), (copy_out, 1), (step_out, 2), (moment_out, 3), (cols, 5)):
-            stores.append(pltpu.make_async_copy(src, outs[i][dst], store_sem.at[i, dst]))
-            stores[-1].start()
+            for to, value in zip(
+                results,
+                (master, master.astype(jnp.bfloat16), update_step, moment_next),
+                strict=True,
+            ):
+                to[:, at] = value
+        for j, src in enumerate(results):
+            store(src, outs[i][j], (i, j))
+        store(cols, outs[i][5], (i, 4))
+    first = pl.multiple_of(band * rows_here, rows_here)
+    piece = 2 * own
+    for i in range(2):
+        rows = held[i][0]
+        loads[i][0].wait()
+        band_grad = grad[pl.ds(first, rows_here), i * hidden : (i + 1) * hidden]
+        factor = (1.0 - stat_decay) / hidden * scales[i] * scales[i]
+        for k in range(model // piece):
+            at = slice(k * piece, (k + 1) * piece)
+            part = lax.dot_general(
+                band_grad,
+                grad[at, i * hidden : (i + 1) * hidden],
+                (((1,), (1,)), ((), ())),
+                preferred_element_type=jnp.float32,
+            )
+            rows[:, at] = stat_decay * rows[:, at] + factor * part
+            store(rows.at[:, at], outs[i][4].at[:, at], (i, 5 + k))
     for copy in stores:
         copy.wait()
 
@@ -461,7 +472,7 @@
             pltpu.VMEM((model, total), jnp.bfloat16),
             pltpu.SemaphoreType.DMA((2,)),
             pltpu.SemaphoreType.DMA((2, 6)),
-            pltpu.SemaphoreType.DMA((2, 6)),
+            pltpu.SemaphoreType.DMA((2, 5 + model // query_weight.shape[1] // 2)),
         ]
         + held,
         compiler_params=params,

time: 74.8 us -> 75.3 us (level)
  no operation moved by 1% of the time
where the time goes in v3:
time: 75.3 us; the launch traced here: 75.1 us
  waiting for transfers between devices  34.8 us (46%)
  Pallas kernels  21.5 us (29%)
  starting transfers between devices  17.7 us (24%)
  between operations  0.94 us (1%)
    ppermute x20, waiting for transfers between devices, move(): return lax.ppermute(value, axes, linear_pairs(fs_size, tp_size, target))  34.8 us
    ppermute x20, starting transfers between devices, move(): return lax.ppermute(value, axes, linear_pairs(fs_size, tp_size, target))  17.7 us
    pallas_call x3, Pallas kernels, gathered_plan(): pl.pallas_call(partial(sum_kernel, not acc), out_shape=pltpu.VMEM((model,...  10 us
    pallas_call x1, Pallas kernels, gathered_plan(): pl.pallas_call(tail_kernel, out_shape=kinds * 2, in_specs=[smem] + [anywh...  9.83 us
    pallas_call x1, Pallas kernels, gathered_plan(): pl.pallas_call(prepare_kernel, out_shape=(pltpu.VMEM(inputs.shape, inputs...  1.61 us
  transfers between devices with their start and end apart: 20, of which 8 were waited for; matrix products, arithmetic and copies ran while one was open for 0% of the time, Pallas kernels for 13%

profile of v3, /device:TPU:0, one launch (start us, length us, event | category | flops | bytes accessed | tf_op | source)
XLA Modules:
  0.0 75.1 jit_solution(17677696522850380198)
XLA Ops:
  0.6 0.1 pad_add_fusion.place
  0.7 1.6 %prepare.1 = (bf16[128,512]{1,0:T(8,128)(2,1)S(1)}, bf16[128,512]{1,0:T(8,128)(2,1)S(1)}) custom-call(s32[3]{0:T(128)S(1)} %pad_add_fusion.place, bf16[128,512]{1,0:T(8,128)(2,1)} %refs_0_.1, bf16[128,256]{1,0:T(8,128)(2,1)} %refs_1_.1, bf16[128,256]{1,0:T(8,128)(2,1)} %refs_2_.1, bf16[128,256]{1,0:T(8,128)(2,1)} %refs_3_.1, f32[1,256]{1,0:T(1,128)} %bitcast.24), custom_call_target="tpu_custom_call" | custom-call | tf_op jit(solution)/shard_map/prepare/pallas_call | solution.py:419
  2.3 0.6 collective-permute-start
  2.9 1.0 %collective-permute-done = bf16[128,512]{1,0:T(8,128)(2,1)S(1)} collective-permute-done((bf16[128,512]{1,0:T(8,128)(2,1)S(1)}, bf16[128,512]{1,0:T(8,128)(2,1)S(1)}, u32[]{:S(2)}, u32[]{:S(2)}) %collective-permute-start) | collective-permute-done | bytes 131104 | tf_op jit(solution)/shard_map/ppermute | solution.py:167
  3.9 4.0 %collective-permute-start.1 = (bf16[2,128,512]{2,1,0:T(8,128)(2,1)S(1)}, bf16[2,128,512]{2,1,0:T(8,128)(2,1)S(1)}, u32[]{:S(2)}, u32[]{:S(2)}) collective-permute-start(bf16[2,128,512]{2,1,0:T(8,128)(2,1)S(1)} %get-tuple-element.41), channel_id=1, source_target_pairs={{0,16},{1,17},{2,18},{3,19},{4,20},{5,21},{6,22},{7,23},{8,24},{9,... | collective-permute-start | bytes 786440 | tf_op jit(solution)/shard_map/ppermute | solution.py:167
  7.9 1.5 %collective-permute-start.12 = (bf16[2,128,512]{2,1,0:T(8,128)(2,1)S(1)}, bf16[2,128,512]{2,1,0:T(8,128)(2,1)S(1)}, u32[]{:S(2)}, u32[]{:S(2)}) collective-permute-start(bf16[2,128,512]{2,1,0:T(8,128)(2,1)S(1)} %get-tuple-element.41), channel_id=1, source_target_pairs={{0,4},{1,3},{2,6},{3,1},{4,0},{5,7},{6,2},{7,5},{8,12},{9,11},{10,... | collective-permute-start | bytes 786440 | tf_op jit(solution)/shard_map/ppermute | solution.py:167
  9.4 1.6 %collective-permute-start.11 = (bf16[2,128,512]{2,1,0:T(8,128)(2,1)S(1)}, bf16[2,128,512]{2,1,0:T(8,128)(2,1)S(1)}, u32[]{:S(2)}, u32[]{:S(2)}) collective-permute-start(bf16[2,128,512]{2,1,0:T(8,128)(2,1)S(1)} %get-tuple-element.41), channel_id=1, source_target_pairs={{0,8},{1,9},{2,10},{3,11},{4,12},{5,13},{6,14},{7,15},{8,0},{9,1},... | collective-permute-start | bytes 786440 | tf_op jit(solution)/shard_map/ppermute | solution.py:167
  11.0 9.3 %collective-permute-done.1 = bf16[2,128,512]{2,1,0:T(8,128)(2,1)S(1)} collective-permute-done((bf16[2,128,512]{2,1,0:T(8,128)(2,1)S(1)}, bf16[2,128,512]{2,1,0:T(8,128)(2,1)S(1)}, u32[]{:S(2)}, u32[]{:S(2)}) %collective-permute-start.1) | collective-permute-done | bytes 262176 | tf_op jit(solution)/shard_map/ppermute | solution.py:167
  20.3 1.5 %collective-permute-start.3 = (bf16[2,128,512]{2,1,0:T(8,128)(2,1)S(1)}, bf16[2,128,512]{2,1,0:T(8,128)(2,1)S(1)}, u32[]{:S(2)}, u32[]{:S(2)}) collective-permute-start(bf16[2,128,512]{2,1,0:T(8,128)(2,1)S(1)} %collective-permute-done.1), channel_id=1, source_target_pairs={{0,4},{1,3},{2,6},{3,1},{4,0},{5,7},{6,2},{7,5},{8,12},{9,11},{10,... | collective-permute-start | bytes 786440 | tf_op jit(solution)/shard_map/ppermute | solution.py:167
  21.8 0.0 collective-permute-done.12
  21.8 0.6 collective-permute-start.13
  22.4 0.1 pad_maximum_fusion.3.refs_0_
  22.5 1.5 %collective-permute-start.17 = (bf16[2,2,128,512]{3,2,1,0:T(8,128)(2,1)S(1)}, bf16[2,2,128,512]{3,2,1,0:T(8,128)(2,1)S(1)}, u32[]{:S(2)}, u32[]{:S(2)}) collective-permute-start(bf16[2,2,128,512]{3,2,1,0:T(8,128)(2,1)S(1)} %pad_maximum_fusion.3.refs_0_), channel_id=1, source_target_pairs={{0,2},{1,5},{2,0},{3,7},{4,6},{5,1},{6,4},{7,3},{8,10},{9,13},{10,... | collective-permute-start | bytes 1572872 | tf_op jit(solution)/shard_map/ppermute | solution.py:167
  24.0 0.0 collective-permute-start.18
  24.0 0.0 collective-permute-done.11
  24.0 1.4 %collective-permute-start.2 = (bf16[2,128,512]{2,1,0:T(8,128)(2,1)S(1)}, bf16[2,128,512]{2,1,0:T(8,128)(2,1)S(1)}, u32[]{:S(2)}, u32[]{:S(2)}) collective-permute-start(bf16[2,128,512]{2,1,0:T(8,128)(2,1)S(1)} %collective-permute-done.1), channel_id=1, source_target_pairs={{0,8},{1,9},{2,10},{3,11},{4,12},{5,13},{6,14},{7,15},{8,0},{9,1},... | collective-permute-start | bytes 786440 | tf_op jit(solution)/shard_map/ppermute | solution.py:167
  25.5 3.2 %collective-permute-done.3 = bf16[2,128,512]{2,1,0:T(8,128)(2,1)S(1)} collective-permute-done((bf16[2,128,512]{2,1,0:T(8,128)(2,1)S(1)}, bf16[2,128,512]{2,1,0:T(8,128)(2,1)S(1)}, u32[]{:S(2)}, u32[]{:S(2)}) %collective-permute-start.3) | collective-permute-done | bytes 262176 | tf_op jit(solution)/shard_map/ppermute | solution.py:167
  28.7 0.7 collective-permute-start.4
  29.4 1.5 %collective-permute-done.13 = bf16[2,128,512]{2,1,0:T(8,128)(2,1)S(1)} collective-permute-done((bf16[2,128,512]{2,1,0:T(8,128)(2,1)S(1)}, bf16[2,128,512]{2,1,0:T(8,128)(2,1)S(1)}, u32[]{:S(2)}, u32[]{:S(2)}) %collective-permute-start.13) | collective-permute-done | bytes 262176 | tf_op jit(solution)/shard_map/ppermute | solution.py:167
  30.9 0.1 pad_maximum_fusion.2.refs_0_
  30.9 1.0 %collective-permute-start.14 = (bf16[2,2,128,512]{3,2,1,0:T(8,128)(2,1)S(1)}, bf16[2,2,128,512]{3,2,1,0:T(8,128)(2,1)S(1)}, u32[]{:S(2)}, u32[]{:S(2)}) collective-permute-start(bf16[2,2,128,512]{3,2,1,0:T(8,128)(2,1)S(1)} %pad_maximum_fusion.2.refs_0_), channel_id=1, source_target_pairs={{0,2},{1,5},{2,0},{3,7},{4,6},{5,1},{6,4},{7,3},{8,10},{9,13},{10,... | collective-permute-start | bytes 1572872 | tf_op jit(solution)/shard_map/ppermute | solution.py:167
  31.9 0.1 pad_maximum_fusion.1.refs_0_
  32.0 4.5 %collective-permute-done.2 = bf16[2,128,512]{2,1,0:T(8,128)(2,1)S(1)} collective-permute-done((bf16[2,128,512]{2,1,0:T(8,128)(2,1)S(1)}, bf16[2,128,512]{2,1,0:T(8,128)(2,1)S(1)}, u32[]{:S(2)}, u32[]{:S(2)}) %collective-permute-start.2) | collective-permute-done | bytes 262176 | tf_op jit(solution)/shard_map/ppermute | solution.py:167
  36.5 0.0 collective-permute-start.15
  36.5 3.7 %collective-permute-done.4 = bf16[2,128,512]{2,1,0:T(8,128)(2,1)S(1)} collective-permute-done((bf16[2,128,512]{2,1,0:T(8,128)(2,1)S(1)}, bf16[2,128,512]{2,1,0:T(8,128)(2,1)S(1)}, u32[]{:S(2)}, u32[]{:S(2)}) %collective-permute-start.4) | collective-permute-done | bytes 262176 | tf_op jit(solution)/shard_map/ppermute | solution.py:167
  40.2 0.7 collective-permute-start.8
  41.0 0.1 pad_maximum_fusion.refs_0_
  41.0 0.0 collective-permute-done.17.refs_1_
  41.0 0.1 collective-permute-start.19
  41.1 0.0 collective-permute-done.18.refs_2_
  41.1 1.4 %collective-permute-start.5 = (bf16[2,2,128,512]{3,2,1,0:T(8,128)(2,1)S(1)}, bf16[2,2,128,512]{3,2,1,0:T(8,128)(2,1)S(1)}, u32[]{:S(2)}, u32[]{:S(2)}) collective-permute-start(bf16[2,2,128,512]{3,2,1,0:T(8,128)(2,1)S(1)} %pad_maximum_fusion.refs_0_), channel_id=1, source_target_pairs={{0,2},{1,5},{2,0},{3,7},{4,6},{5,1},{6,4},{7,3},{8,10},{9,13},{10,... | collective-permute-start | bytes 1572872 | tf_op jit(solution)/shard_map/ppermute | solution.py:167
  42.5 0.0 collective-permute-done.14.refs_1_
  42.5 0.1 collective-permute-start.9
  42.6 0.0 collective-permute-done.15.refs_2_
  42.6 0.4 collective-permute-start.16
  43.0 6.4 %collective-permute-done.8.refs_1_ = bf16[2,2,128,512]{3,2,1,0:T(8,128)(2,1)S(1)} collective-permute-done((bf16[2,2,128,512]{3,2,1,0:T(8,128)(2,1)S(1)}, bf16[2,2,128,512]{3,2,1,0:T(8,128)(2,1)S(1)}, u32[]{:S(2)}, u32[]{:S(2)}) %collective-permute-start.8) | collective-permute-done | bytes 524320 | tf_op jit(solution)/shard_map/ppermute | solution.py:167
  49.4 0.0 collective-permute-start.10
  49.4 0.0 collective-permute-done.19.refs_3_
  49.4 0.5 collective-permute-start.6
  49.9 5.1 %collective-permute-done.5.refs_1_ = bf16[2,2,128,512]{3,2,1,0:T(8,128)(2,1)S(1)} collective-permute-done((bf16[2,2,128,512]{3,2,1,0:T(8,128)(2,1)S(1)}, bf16[2,2,128,512]{3,2,1,0:T(8,128)(2,1)S(1)}, u32[]{:S(2)}, u32[]{:S(2)}) %collective-permute-start.5) | collective-permute-done | bytes 524320 | tf_op jit(solution)/shard_map/ppermute | solution.py:167
  55.0 0.0 collective-permute-start.7
  55.0 3.2 %shard_map.256.refs_4_ = f32[2048,2048]{1,0:T(8,128)S(1)} custom-call(s32[3]{0:T(128)S(1)} %pad_add_fusion.place, bf16[2,2,128,512]{3,2,1,0:T(8,128)(2,1)S(1)} %pad_maximum_fusion.3.refs_0_, bf16[2,2,128,512]{3,2,1,0:T(8,128)(2,1)S(1)} %collective-permute-done.17.refs_1_, bf16[2,2,128,512]{3,2,1,0:T(8,128)(2,1)S(1)} %collective-permute-done.18.refs_2_, ...), custom_call_target="tpu_custom_call" | custom-call | tf_op jit(solution)/shard_map/pallas_call | solution.py:453
  58.3 3.4 %shard_map.257.refs_4_ = f32[2048,2048]{1,0:T(8,128)S(1)} custom-call(s32[3]{0:T(128)S(1)} %pad_add_fusion.place, bf16[2,2,128,512]{3,2,1,0:T(8,128)(2,1)S(1)} %pad_maximum_fusion.2.refs_0_, bf16[2,2,128,512]{3,2,1,0:T(8,128)(2,1)S(1)} %collective-permute-done.14.refs_1_, ...), custom_call_target="tpu_custom_call", output_to_operand_aliasing={{}: (5, {})} | custom-call | tf_op jit(solution)/shard_map/pallas_call | solution.py:453
  61.7 0.0 collective-permute-done.9.refs_2_
  61.7 3.4 %shard_map.258.refs_4_ = f32[2048,2048]{1,0:T(8,128)S(1)} custom-call(s32[3]{0:T(128)S(1)} %pad_add_fusion.place, bf16[2,2,128,512]{3,2,1,0:T(8,128)(2,1)S(1)} %pad_maximum_fusion.1.refs_0_, bf16[2,2,128,512]{3,2,1,0:T(8,128)(2,1)S(1)} %collective-permute-done.8.refs_1_, ...), custom_call_target="tpu_custom_call", output_to_operand_aliasing={{}: (5, {})} | custom-call | tf_op jit(solution)/shard_map/pallas_call | solution.py:453
  65.1 0.0 collective-permute-done.6.refs_2_
  65.1 0.0 collective-permute-done.7.refs_3_
  65.2 9.8 %tail.1 = (f32[256,256]{1,0:T(8,128)}, bf16[256,256]{1,0:T(8,128)(2,1)}, f32[256,256]{1,0:T(8,128)}, f32[256,256]{1,0:T(8,128)}, f32[256,2048]{1,0:T(8,128)}, /*...) custom-call(s32[3]{0:T(128)S(1)} %pad_add_fusion.place, ...), custom_call_target="tpu_custom_call" | custom-call | tf_op jit(solution)/shard_map/tail/pallas_call | solution.py:465
  (3 shorter events, 0.0 us)
Async XLA Ops:
  2.3 1.5 %collective-permute-start = (bf16[128,512]{1,0:T(8,128)(2,1)S(1)}, bf16[128,512]{1,0:T(8,128)(2,1)S(1)}, u32[]{:S(2)}, u32[]{:S(2)}) collective-permute-start(bf16[128,512]{1,0:T(8,128)(2,1)S(1)} %get-tuple-element.27), channel_id=1, source_target_pairs={{0,1},{1,0},{2,3},{3,2},{4,5},{5,4},{6,7},{7,6},{8,9},{9,8},{10,11... | collective-permute-start | bytes 393224 | tf_op jit(solution)/shard_map/ppermute | solution.py:167
  3.9 16.3 %collective-permute-start.1 = (bf16[2,128,512]{2,1,0:T(8,128)(2,1)S(1)}, bf16[2,128,512]{2,1,0:T(8,128)(2,1)S(1)}, u32[]{:S(2)}, u32[]{:S(2)}) collective-permute-start(bf16[2,128,512]{2,1,0:T(8,128)(2,1)S(1)} %get-tuple-element.41), channel_id=1, source_target_pairs={{0,16},{1,17},{2,18},{3,19},{4,20},{5,21},{6,22},{7,23},{8,24},{9,... | collective-permute-start | bytes 786440 | tf_op jit(solution)/shard_map/ppermute | solution.py:167
  7.9 13.9 %collective-permute-start.12 = (bf16[2,128,512]{2,1,0:T(8,128)(2,1)S(1)}, bf16[2,128,512]{2,1,0:T(8,128)(2,1)S(1)}, u32[]{:S(2)}, u32[]{:S(2)}) collective-permute-start(bf16[2,128,512]{2,1,0:T(8,128)(2,1)S(1)} %get-tuple-element.41), channel_id=1, source_target_pairs={{0,4},{1,3},{2,6},{3,1},{4,0},{5,7},{6,2},{7,5},{8,12},{9,11},{10,... | collective-permute-start | bytes 786440 | tf_op jit(solution)/shard_map/ppermute | solution.py:167
  9.4 14.6 %collective-permute-start.11 = (bf16[2,128,512]{2,1,0:T(8,128)(2,1)S(1)}, bf16[2,128,512]{2,1,0:T(8,128)(2,1)S(1)}, u32[]{:S(2)}, u32[]{:S(2)}) collective-permute-start(bf16[2,128,512]{2,1,0:T(8,128)(2,1)S(1)} %get-tuple-element.41), channel_id=1, source_target_pairs={{0,8},{1,9},{2,10},{3,11},{4,12},{5,13},{6,14},{7,15},{8,0},{9,1},... | collective-permute-start | bytes 786440 | tf_op jit(solution)/shard_map/ppermute | solution.py:167
  20.3 8.4 %collective-permute-start.3 = (bf16[2,128,512]{2,1,0:T(8,128)(2,1)S(1)}, bf16[2,128,512]{2,1,0:T(8,128)(2,1)S(1)}, u32[]{:S(2)}, u32[]{:S(2)}) collective-permute-start(bf16[2,128,512]{2,1,0:T(8,128)(2,1)S(1)} %collective-permute-done.1), channel_id=1, source_target_pairs={{0,4},{1,3},{2,6},{3,1},{4,0},{5,7},{6,2},{7,5},{8,12},{9,11},{10,... | collective-permute-start | bytes 786440 | tf_op jit(solution)/shard_map/ppermute | solution.py:167
  21.8 9.1 %collective-permute-start.13 = (bf16[2,128,512]{2,1,0:T(8,128)(2,1)S(1)}, bf16[2,128,512]{2,1,0:T(8,128)(2,1)S(1)}, u32[]{:S(2)}, u32[]{:S(2)}) collective-permute-start(bf16[2,128,512]{2,1,0:T(8,128)(2,1)S(1)} %collective-permute-done.12), channel_id=1, source_target_pairs={{0,8},{1,9},{2,10},{3,11},{4,12},{5,13},{6,14},{7,15},{8,0},{9,1},... | collective-permute-start | bytes 786440 | tf_op jit(solution)/shard_map/ppermute | solution.py:167
  22.5 18.5 %collective-permute-start.17 = (bf16[2,2,128,512]{3,2,1,0:T(8,128)(2,1)S(1)}, bf16[2,2,128,512]{3,2,1,0:T(8,128)(2,1)S(1)}, u32[]{:S(2)}, u32[]{:S(2)}) collective-permute-start(bf16[2,2,128,512]{3,2,1,0:T(8,128)(2,1)S(1)} %pad_maximum_fusion.3.refs_0_), channel_id=1, source_target_pairs={{0,2},{1,5},{2,0},{3,7},{4,6},{5,1},{6,4},{7,3},{8,10},{9,13},{10,... | collective-permute-start | bytes 1572872 | tf_op jit(solution)/shard_map/ppermute | solution.py:167
  24.0 17.1 %collective-permute-start.18 = (bf16[2,2,128,512]{3,2,1,0:T(8,128)(2,1)S(1)}, bf16[2,2,128,512]{3,2,1,0:T(8,128)(2,1)S(1)}, u32[]{:S(2)}, u32[]{:S(2)}) collective-permute-start(bf16[2,2,128,512]{3,2,1,0:T(8,128)(2,1)S(1)} %pad_maximum_fusion.3.refs_0_), channel_id=1, source_target_pairs={{0,1},{1,0},{2,3},{3,2},{4,5},{5,4},{6,7},{7,6},{8,9},{9,8},{10,11... | collective-permute-start | bytes 1572872 | tf_op jit(solution)/shard_map/ppermute | solution.py:167
  24.0 12.5 %collective-permute-start.2 = (bf16[2,128,512]{2,1,0:T(8,128)(2,1)S(1)}, bf16[2,128,512]{2,1,0:T(8,128)(2,1)S(1)}, u32[]{:S(2)}, u32[]{:S(2)}) collective-permute-start(bf16[2,128,512]{2,1,0:T(8,128)(2,1)S(1)} %collective-permute-done.1), channel_id=1, source_target_pairs={{0,8},{1,9},{2,10},{3,11},{4,12},{5,13},{6,14},{7,15},{8,0},{9,1},... | collective-permute-start | bytes 786440 | tf_op jit(solution)/shard_map/ppermute | solution.py:167
  28.7 11.6 %collective-permute-start.4 = (bf16[2,128,512]{2,1,0:T(8,128)(2,1)S(1)}, bf16[2,128,512]{2,1,0:T(8,128)(2,1)S(1)}, u32[]{:S(2)}, u32[]{:S(2)}) collective-permute-start(bf16[2,128,512]{2,1,0:T(8,128)(2,1)S(1)} %collective-permute-done.3), channel_id=1, source_target_pairs={{0,8},{1,9},{2,10},{3,11},{4,12},{5,13},{6,14},{7,15},{8,0},{9,1},... | collective-permute-start | bytes 786440 | tf_op jit(solution)/shard_map/ppermute | solution.py:167
  30.9 11.6 %collective-permute-start.14 = (bf16[2,2,128,512]{3,2,1,0:T(8,128)(2,1)S(1)}, bf16[2,2,128,512]{3,2,1,0:T(8,128)(2,1)S(1)}, u32[]{:S(2)}, u32[]{:S(2)}) collective-permute-start(bf16[2,2,128,512]{3,2,1,0:T(8,128)(2,1)S(1)} %pad_maximum_fusion.2.refs_0_), channel_id=1, source_target_pairs={{0,2},{1,5},{2,0},{3,7},{4,6},{5,1},{6,4},{7,3},{8,10},{9,13},{10,... | collective-permute-start | bytes 1572872 | tf_op jit(solution)/shard_map/ppermute | solution.py:167
  36.5 6.1 %collective-permute-start.15 = (bf16[2,2,128,512]{3,2,1,0:T(8,128)(2,1)S(1)}, bf16[2,2,128,512]{3,2,1,0:T(8,128)(2,1)S(1)}, u32[]{:S(2)}, u32[]{:S(2)}) collective-permute-start(bf16[2,2,128,512]{3,2,1,0:T(8,128)(2,1)S(1)} %pad_maximum_fusion.2.refs_0_), channel_id=1, source_target_pairs={{0,1},{1,0},{2,3},{3,2},{4,5},{5,4},{6,7},{7,6},{8,9},{9,8},{10,11... | collective-permute-start | bytes 1572872 | tf_op jit(solution)/shard_map/ppermute | solution.py:167
  40.2 9.2 %collective-permute-start.8 = (bf16[2,2,128,512]{3,2,1,0:T(8,128)(2,1)S(1)}, bf16[2,2,128,512]{3,2,1,0:T(8,128)(2,1)S(1)}, u32[]{:S(2)}, u32[]{:S(2)}) collective-permute-start(bf16[2,2,128,512]{3,2,1,0:T(8,128)(2,1)S(1)} %pad_maximum_fusion.1.refs_0_), channel_id=1, source_target_pairs={{0,2},{1,5},{2,0},{3,7},{4,6},{5,1},{6,4},{7,3},{8,10},{9,13},{10,... | collective-permute-start | bytes 1572872 | tf_op jit(solution)/shard_map/ppermute | solution.py:167
  41.0 8.4 %collective-permute-start.19 = (bf16[2,2,128,512]{3,2,1,0:T(8,128)(2,1)S(1)}, bf16[2,2,128,512]{3,2,1,0:T(8,128)(2,1)S(1)}, u32[]{:S(2)}, u32[]{:S(2)}) collective-permute-start(bf16[2,2,128,512]{3,2,1,0:T(8,128)(2,1)S(1)} %collective-permute-done.17.refs_1_), channel_id=1, source_target_pairs={{0,1},{1,0},{2,3},{3,2},{4,5},{5,4},{6,7},{7,6},{8,9},{9,8},{10,11... | collective-permute-start | bytes 1572872 | tf_op jit(solution)/shard_map/ppermute | solution.py:167
  41.1 13.9 %collective-permute-start.5 = (bf16[2,2,128,512]{3,2,1,0:T(8,128)(2,1)S(1)}, bf16[2,2,128,512]{3,2,1,0:T(8,128)(2,1)S(1)}, u32[]{:S(2)}, u32[]{:S(2)}) collective-permute-start(bf16[2,2,128,512]{3,2,1,0:T(8,128)(2,1)S(1)} %pad_maximum_fusion.refs_0_), channel_id=1, source_target_pairs={{0,2},{1,5},{2,0},{3,7},{4,6},{5,1},{6,4},{7,3},{8,10},{9,13},{10,... | collective-permute-start | bytes 1572872 | tf_op jit(solution)/shard_map/ppermute | solution.py:167
  42.5 19.2 %collective-permute-start.9 = (bf16[2,2,128,512]{3,2,1,0:T(8,128)(2,1)S(1)}, bf16[2,2,128,512]{3,2,1,0:T(8,128)(2,1)S(1)}, u32[]{:S(2)}, u32[]{:S(2)}) collective-permute-start(bf16[2,2,128,512]{3,2,1,0:T(8,128)(2,1)S(1)} %pad_maximum_fusion.1.refs_0_), channel_id=1, source_target_pairs={{0,1},{1,0},{2,3},{3,2},{4,5},{5,4},{6,7},{7,6},{8,9},{9,8},{10,11... | collective-permute-start | bytes 1572872 | tf_op jit(solution)/shard_map/ppermute | solution.py:167
  42.6 15.7 %collective-permute-start.16 = (bf16[2,2,128,512]{3,2,1,0:T(8,128)(2,1)S(1)}, bf16[2,2,128,512]{3,2,1,0:T(8,128)(2,1)S(1)}, u32[]{:S(2)}, u32[]{:S(2)}) collective-permute-start(bf16[2,2,128,512]{3,2,1,0:T(8,128)(2,1)S(1)} %collective-permute-done.14.refs_1_), channel_id=1, source_target_pairs={{0,1},{1,0},{2,3},{3,2},{4,5},{5,4},{6,7},{7,6},{8,9},{9,8},{10,11... | collective-permute-start | bytes 1572872 | tf_op jit(solution)/shard_map/ppermute | solution.py:167
  49.4 12.3 %collective-permute-start.10 = (bf16[2,2,128,512]{3,2,1,0:T(8,128)(2,1)S(1)}, bf16[2,2,128,512]{3,2,1,0:T(8,128)(2,1)S(1)}, u32[]{:S(2)}, u32[]{:S(2)}) collective-permute-start(bf16[2,2,128,512]{3,2,1,0:T(8,128)(2,1)S(1)} %collective-permute-done.8.refs_1_), channel_id=1, source_target_pairs={{0,1},{1,0},{2,3},{3,2},{4,5},{5,4},{6,7},{7,6},{8,9},{9,8},{10,11... | collective-permute-start | bytes 1572872 | tf_op jit(solution)/shard_map/ppermute | solution.py:167
  49.4 15.7 %collective-permute-start.6 = (bf16[2,2,128,512]{3,2,1,0:T(8,128)(2,1)S(1)}, bf16[2,2,128,512]{3,2,1,0:T(8,128)(2,1)S(1)}, u32[]{:S(2)}, u32[]{:S(2)}) collective-permute-start(bf16[2,2,128,512]{3,2,1,0:T(8,128)(2,1)S(1)} %pad_maximum_fusion.refs_0_), channel_id=1, source_target_pairs={{0,1},{1,0},{2,3},{3,2},{4,5},{5,4},{6,7},{7,6},{8,9},{9,8},{10,11... | collective-permute-start | bytes 1572872 | tf_op jit(solution)/shard_map/ppermute | solution.py:167
  55.0 10.1 %collective-permute-start.7 = (bf16[2,2,128,512]{3,2,1,0:T(8,128)(2,1)S(1)}, bf16[2,2,128,512]{3,2,1,0:T(8,128)(2,1)S(1)}, u32[]{:S(2)}, u32[]{:S(2)}) collective-permute-start(bf16[2,2,128,512]{3,2,1,0:T(8,128)(2,1)S(1)} %collective-permute-done.5.refs_1_), channel_id=1, source_target_pairs={{0,1},{1,0},{2,3},{3,2},{4,5},{5,4},{6,7},{7,6},{8,9},{9,8},{10,11... | collective-permute-start | bytes 1572872 | tf_op jit(solution)/shard_map/ppermute | solution.py:167

commit v4 on v3

--- a/solution.py
+++ b/solution.py
@@ -237,18 +237,27 @@
     )
 
 
-def sum_kernel(first, place, *refs):
+def sum_kernel(first, n_fetched, place, *refs):
     pieces, refs = refs[:4], refs[4:]
     if not first:
         refs = refs[1:]
-    acc, x_set, y_set, sem = refs
+    sources, refs = refs[:n_fetched], refs[n_fetched:]
+    acc, fetched, (x_set, y_set, sem, fetch_sem) = refs[0], refs[1:-4], refs[-4:]
     assemble(place, pieces, x_set, y_set, sem)
+    copies = [
+        pltpu.make_async_copy(src, dst, fetch_sem.at[j])
+        for j, (src, dst) in enumerate(zip(sources, fetched, strict=True))
+    ]
     assembled(x_set, y_set, sem)
+    for copy in copies:
+        copy.start()
     total, chunk = acc.shape[1], x_set.shape[0]
     for at in range(0, total, chunk):
         cols = slice(at, at + chunk)
         part = product(x_set, y_set, cols)
         acc[:, cols] = part if first else acc[:, cols] + part
+    for copy in copies:
+        copy.wait()
 
 
 def tail_kernel(place, *refs):
@@ -257,26 +266,16 @@
     refs = refs[12:]
     outs = [refs[6 * i : 6 * i + 6] for i in range(2)]
     refs = refs[12:]
-    x_set, y_set, grad, sem, load_sem, store_sem = refs[:6]
-    held = [refs[6 + 10 * i : 16 + 10 * i] for i in range(2)]
+    x_set, y_set, grad, sem, store_sem = refs[:5]
+    made = [refs[5 + 6 * i : 11 + 6 * i] for i in range(2)]
     odd, band = place[0], place[2]
     model, total = grad.shape
     hidden = total // 2
     own = pieces[0].shape[3] // 2
-    rows_here = held[0][0].shape[0]
+    rows_here = sides[0][0].shape[0]
 
     assemble(place, pieces, x_set, y_set, sem)
-    loads = [
-        [
-            pltpu.make_async_copy(src, dst, load_sem.at[i, j])
-            for j, (src, dst) in enumerate(zip(sides[i], held[i][:6], strict=True))
-        ]
-        for i in range(2)
-    ]
     assembled(x_set, y_set, sem)
-    for j in (1, 2, 3, 4, 5, 0):
-        for side in loads:
-            side[j].start()
 
     chunk = x_set.shape[0]
     squares = [jnp.zeros((8, chunk), jnp.float32)] * 2
@@ -294,25 +293,22 @@
 
     scales = []
     for i in range(2):
-        _, row_root, weight, moment, cols, col_root = held[i][:6]
-        results = held[i][6:]
+        _, row_root, weight, moment, cols, col_root = sides[i]
+        results, cols_next = made[i][:4], made[i][5]
         square = jnp.sum(squares[i], keepdims=True)
         scale = jnp.sqrt(model * hidden / (square + 1.0))
         scales.append(scale)
         mine = pl.multiple_of(i * hidden + odd * own, own)
         own_grad = grad[:, pl.ds(mine, own)]
-        loads[i][1].wait()
         left = jnp.dot(row_root[...], own_grad, preferred_element_type=jnp.float32)
         left_high = left.astype(jnp.bfloat16)
         left_low = (left - left_high.astype(jnp.float32)).astype(jnp.bfloat16)
         column_total = lax.dot_general(
             own_grad, own_grad, (((0,), (0,)), ((), ())), preferred_element_type=jnp.float32
         )
-        for copy in loads[i][2:]:
-            copy.wait()
         for h in range(own // HEAD):
             at = slice(h * HEAD, (h + 1) * HEAD)
-            cols[h] = (
+            cols_next[h] = (
                 stat_decay * cols[h]
                 + (1.0 - stat_decay) / model * scale * scale * column_total[at, at]
             )
@@ -332,12 +328,11 @@
                 to[:, at] = value
         for j, src in enumerate(results):
             store(src, outs[i][j], (i, j))
-        store(cols, outs[i][5], (i, 4))
+        store(cols_next, outs[i][5], (i, 4))
     first = pl.multiple_of(band * rows_here, rows_here)
     piece = 2 * own
     for i in range(2):
-        rows = held[i][0]
-        loads[i][0].wait()
+        rows, rows_next = sides[i][0], made[i][4]
         band_grad = grad[pl.ds(first, rows_here), i * hidden : (i + 1) * hidden]
         factor = (1.0 - stat_decay) / hidden * scales[i] * scales[i]
         for k in range(model // piece):
@@ -348,8 +343,8 @@
                 (((1,), (1,)), ((), ())),
                 preferred_element_type=jnp.float32,
             )
-            rows[:, at] = stat_decay * rows[:, at] + factor * part
-            store(rows.at[:, at], outs[i][4].at[:, at], (i, 5 + k))
+            rows_next[:, at] = stat_decay * rows[:, at] + factor * part
+            store(rows_next.at[:, at], outs[i][4].at[:, at], (i, 5 + k))
     for copy in stores:
         copy.wait()
 
@@ -413,7 +408,7 @@
     place = jnp.stack([tp_at & 1, tp_at >> 1, lax.axis_index("fs")]).astype(jnp.int32)
     smem = pl.BlockSpec(memory_space=pltpu.SMEM)
     vmem = pl.BlockSpec(memory_space=pltpu.VMEM)
-    params = pltpu.CompilerParams(vmem_limit_bytes=26 * 2**20)
+    params = pltpu.CompilerParams(vmem_limit_bytes=21 * 2**20)
     hbm = pl.BlockSpec(memory_space=pltpu.HBM)
     saved = (inputs, query_grad, forget_grad, forget_pre, lower_bound[None])
     keep, send = pl.pallas_call(
@@ -438,40 +433,42 @@
     row_kind = jax.ShapeDtypeStruct(query_rows.shape, jnp.float32)
     col_kind = jax.ShapeDtypeStruct(query_cols.shape, jnp.float32)
     kinds = (wide, narrow, wide, wide, row_kind, col_kind)
-    held = []
-    for side in sides:
-        held += [pltpu.VMEM(v.shape, v.dtype) for v in side]
-        held += [pltpu.VMEM(k.shape, k.dtype) for k in kinds[:4]]
+    held = [pltpu.VMEM(k.shape, k.dtype) for k in kinds * 2]
     anywhere = pl.BlockSpec(memory_space=pl.ANY)
     set_scratch = [
         pltpu.VMEM((2 * inputs.shape[0], model), jnp.bfloat16),
         pltpu.VMEM((2 * inputs.shape[0], total), jnp.bfloat16),
     ]
-    acc = []
-    for pieces in sets[:-1]:
-        acc = [
-            pl.pallas_call(
-                partial(sum_kernel, not acc),
-                out_shape=pltpu.VMEM((model, total), jnp.float32),
-                in_specs=[smem] + [anywhere] * 4 + [vmem] * len(acc),
-                out_specs=vmem,
-                scratch_shapes=set_scratch + [pltpu.SemaphoreType.DMA((2,))],
-                input_output_aliases={5: 0} if acc else {},
-                compiler_params=params,
-            )(place, *pieces, *acc)
-        ]
+    wanted = [[side[0] for side in sides], [v for side in sides for v in side[1:]]]
+    wanted += [[]] * (len(sets) - 3)
+    acc, fetched = [], []
+    for s, pieces in enumerate(sets[:-1]):
+        fetch = [pltpu.with_memory_space_constraint(v, pltpu.HBM) for v in wanted[s]]
+        made = pl.pallas_call(
+            partial(sum_kernel, not acc, len(fetch)),
+            out_shape=[pltpu.VMEM((model, total), jnp.float32)]
+            + [pltpu.VMEM(v.shape, v.dtype) for v in fetch],
+            in_specs=[smem] + [anywhere] * 4 + [vmem] * len(acc) + [hbm] * len(fetch),
+            out_specs=[vmem] * (1 + len(fetch)),
+            scratch_shapes=set_scratch
+            + [pltpu.SemaphoreType.DMA((2,)), pltpu.SemaphoreType.DMA((max(len(fetch), 1),))],
+            input_output_aliases={5: 0} if acc else {},
+            compiler_params=pltpu.CompilerParams(vmem_limit_bytes=12 * 2**20),
+        )(place, *pieces, *acc, *fetch)
+        acc, fetched = made[:1], fetched + list(made[1:])
+    half = len(fetched[2:]) // 2
+    loaded = [fetched[0], *fetched[2 : 2 + half], fetched[1], *fetched[2 + half :]]
     operands = [*sets[-1], pltpu.with_memory_space_constraint(*acc, pltpu.VMEM)]
-    operands += [pltpu.with_memory_space_constraint(v, pltpu.HBM) for side in sides for v in side]
+    operands += [pltpu.with_memory_space_constraint(v, pltpu.VMEM) for v in loaded]
     out = pl.pallas_call(
         tail_kernel,
         out_shape=kinds * 2,
-        in_specs=[smem] + [anywhere] * 4 + [vmem] + [hbm] * 12,
+        in_specs=[smem] + [anywhere] * 4 + [vmem] * 13,
         out_specs=[hbm] * 12,
         scratch_shapes=set_scratch
         + [
             pltpu.VMEM((model, total), jnp.bfloat16),
             pltpu.SemaphoreType.DMA((2,)),
-            pltpu.SemaphoreType.DMA((2, 6)),
             pltpu.SemaphoreType.DMA((2, 5 + model // query_weight.shape[1] // 2)),
         ]
         + held,

time: 75.3 us -> 74.6 us (level)
    pallas_call x1, Pallas kernels: 9.83 us -> 8.98 us  [gathered_plan(): pl.pallas_call(tail_kernel, out_shape=kinds * 2, in_specs=[smem] + [anywh...]
  transfers between devices with their start and end apart: 20 -> 20, of which waited for: 8 -> 8; matrix products, arithmetic and copies ran while one was open for 0% -> 0% of each run, Pallas kernels for 13% -> 14%
where the time goes in v4:
time: 74.6 us; the launch traced here: 74.4 us
  waiting for transfers between devices  34.8 us (47%)
  Pallas kernels  20.8 us (28%)
  starting transfers between devices  17.7 us (24%)
  between operations  0.94 us (1%)
    ppermute x20, waiting for transfers between devices, move(): return lax.ppermute(value, axes, linear_pairs(fs_size, tp_size, target))  34.8 us
    ppermute x20, starting transfers between devices, move(): return lax.ppermute(value, axes, linear_pairs(fs_size, tp_size, target))  17.7 us
    pallas_call x3, Pallas kernels, gathered_plan(): pl.pallas_call(partial(sum_kernel, not acc, len(fetch)), out_shape=[pltpu...  10.2 us
    pallas_call x1, Pallas kernels, gathered_plan(): pl.pallas_call(tail_kernel, out_shape=kinds * 2, in_specs=[smem] + [anywh...  8.98 us
    pallas_call x1, Pallas kernels, gathered_plan(): pl.pallas_call(prepare_kernel, out_shape=(pltpu.VMEM(inputs.shape, inputs...  1.61 us
  transfers between devices with their start and end apart: 20, of which 8 were waited for; matrix products, arithmetic and copies ran while one was open for 0% of the time, Pallas kernels for 14%

profile of v4, /device:TPU:0, one launch (start us, length us, event | category | flops | bytes accessed | tf_op | source)
XLA Modules:
  0.0 74.4 jit_solution(8358206129169781497)
XLA Ops:
  0.6 0.1 pad_add_fusion.place
  0.7 1.6 %prepare.1 = (bf16[128,512]{1,0:T(8,128)(2,1)S(1)}, bf16[128,512]{1,0:T(8,128)(2,1)S(1)}) custom-call(s32[3]{0:T(128)S(1)} %pad_add_fusion.place, bf16[128,512]{1,0:T(8,128)(2,1)} %refs_0_.1, bf16[128,256]{1,0:T(8,128)(2,1)} %refs_1_.1, bf16[128,256]{1,0:T(8,128)(2,1)} %refs_2_.1, bf16[128,256]{1,0:T(8,128)(2,1)} %refs_3_.1, f32[1,256]{1,0:T(1,128)} %bitcast.24), custom_call_target="tpu_custom_call" | custom-call | tf_op jit(solution)/shard_map/prepare/pallas_call | solution.py:414
  2.3 0.6 collective-permute-start
  2.9 1.0 %collective-permute-done = bf16[128,512]{1,0:T(8,128)(2,1)S(1)} collective-permute-done((bf16[128,512]{1,0:T(8,128)(2,1)S(1)}, bf16[128,512]{1,0:T(8,128)(2,1)S(1)}, u32[]{:S(2)}, u32[]{:S(2)}) %collective-permute-start) | collective-permute-done | bytes 131104 | tf_op jit(solution)/shard_map/ppermute | solution.py:167
  3.9 4.0 %collective-permute-start.1 = (bf16[2,128,512]{2,1,0:T(8,128)(2,1)S(1)}, bf16[2,128,512]{2,1,0:T(8,128)(2,1)S(1)}, u32[]{:S(2)}, u32[]{:S(2)}) collective-permute-start(bf16[2,128,512]{2,1,0:T(8,128)(2,1)S(1)} %get-tuple-element.69), channel_id=1, source_target_pairs={{0,16},{1,17},{2,18},{3,19},{4,20},{5,21},{6,22},{7,23},{8,24},{9,... | collective-permute-start | bytes 786440 | tf_op jit(solution)/shard_map/ppermute | solution.py:167
  7.9 1.5 %collective-permute-start.12 = (bf16[2,128,512]{2,1,0:T(8,128)(2,1)S(1)}, bf16[2,128,512]{2,1,0:T(8,128)(2,1)S(1)}, u32[]{:S(2)}, u32[]{:S(2)}) collective-permute-start(bf16[2,128,512]{2,1,0:T(8,128)(2,1)S(1)} %get-tuple-element.69), channel_id=1, source_target_pairs={{0,4},{1,3},{2,6},{3,1},{4,0},{5,7},{6,2},{7,5},{8,12},{9,11},{10,... | collective-permute-start | bytes 786440 | tf_op jit(solution)/shard_map/ppermute | solution.py:167
  9.4 1.6 %collective-permute-start.11 = (bf16[2,128,512]{2,1,0:T(8,128)(2,1)S(1)}, bf16[2,128,512]{2,1,0:T(8,128)(2,1)S(1)}, u32[]{:S(2)}, u32[]{:S(2)}) collective-permute-start(bf16[2,128,512]{2,1,0:T(8,128)(2,1)S(1)} %get-tuple-element.69), channel_id=1, source_target_pairs={{0,8},{1,9},{2,10},{3,11},{4,12},{5,13},{6,14},{7,15},{8,0},{9,1},... | collective-permute-start | bytes 786440 | tf_op jit(solution)/shard_map/ppermute | solution.py:167
  11.0 9.3 %collective-permute-done.1 = bf16[2,128,512]{2,1,0:T(8,128)(2,1)S(1)} collective-permute-done((bf16[2,128,512]{2,1,0:T(8,128)(2,1)S(1)}, bf16[2,128,512]{2,1,0:T(8,128)(2,1)S(1)}, u32[]{:S(2)}, u32[]{:S(2)}) %collective-permute-start.1) | collective-permute-done | bytes 262176 | tf_op jit(solution)/shard_map/ppermute | solution.py:167
  20.3 1.5 %collective-permute-start.3 = (bf16[2,128,512]{2,1,0:T(8,128)(2,1)S(1)}, bf16[2,128,512]{2,1,0:T(8,128)(2,1)S(1)}, u32[]{:S(2)}, u32[]{:S(2)}) collective-permute-start(bf16[2,128,512]{2,1,0:T(8,128)(2,1)S(1)} %collective-permute-done.1), channel_id=1, source_target_pairs={{0,4},{1,3},{2,6},{3,1},{4,0},{5,7},{6,2},{7,5},{8,12},{9,11},{10,... | collective-permute-start | bytes 786440 | tf_op jit(solution)/shard_map/ppermute | solution.py:167
  21.8 0.0 collective-permute-done.12
  21.8 0.6 collective-permute-start.13
  22.4 0.1 pad_maximum_fusion.3.refs_0_
  22.5 1.5 %collective-permute-start.17 = (bf16[2,2,128,512]{3,2,1,0:T(8,128)(2,1)S(1)}, bf16[2,2,128,512]{3,2,1,0:T(8,128)(2,1)S(1)}, u32[]{:S(2)}, u32[]{:S(2)}) collective-permute-start(bf16[2,2,128,512]{3,2,1,0:T(8,128)(2,1)S(1)} %pad_maximum_fusion.3.refs_0_), channel_id=1, source_target_pairs={{0,2},{1,5},{2,0},{3,7},{4,6},{5,1},{6,4},{7,3},{8,10},{9,13},{10,... | collective-permute-start | bytes 1572872 | tf_op jit(solution)/shard_map/ppermute | solution.py:167
  24.0 0.0 collective-permute-done.11
  24.0 1.4 %collective-permute-start.2 = (bf16[2,128,512]{2,1,0:T(8,128)(2,1)S(1)}, bf16[2,128,512]{2,1,0:T(8,128)(2,1)S(1)}, u32[]{:S(2)}, u32[]{:S(2)}) collective-permute-start(bf16[2,128,512]{2,1,0:T(8,128)(2,1)S(1)} %collective-permute-done.1), channel_id=1, source_target_pairs={{0,8},{1,9},{2,10},{3,11},{4,12},{5,13},{6,14},{7,15},{8,0},{9,1},... | collective-permute-start | bytes 786440 | tf_op jit(solution)/shard_map/ppermute | solution.py:167
  25.5 3.2 %collective-permute-done.3 = bf16[2,128,512]{2,1,0:T(8,128)(2,1)S(1)} collective-permute-done((bf16[2,128,512]{2,1,0:T(8,128)(2,1)S(1)}, bf16[2,128,512]{2,1,0:T(8,128)(2,1)S(1)}, u32[]{:S(2)}, u32[]{:S(2)}) %collective-permute-start.3) | collective-permute-done | bytes 262176 | tf_op jit(solution)/shard_map/ppermute | solution.py:167
  28.7 0.7 collective-permute-start.4
  29.4 1.5 %collective-permute-done.13 = bf16[2,128,512]{2,1,0:T(8,128)(2,1)S(1)} collective-permute-done((bf16[2,128,512]{2,1,0:T(8,128)(2,1)S(1)}, bf16[2,128,512]{2,1,0:T(8,128)(2,1)S(1)}, u32[]{:S(2)}, u32[]{:S(2)}) %collective-permute-start.13) | collective-permute-done | bytes 262176 | tf_op jit(solution)/shard_map/ppermute | solution.py:167
  30.9 0.1 pad_maximum_fusion.2.refs_0_
  30.9 1.0 %collective-permute-start.14 = (bf16[2,2,128,512]{3,2,1,0:T(8,128)(2,1)S(1)}, bf16[2,2,128,512]{3,2,1,0:T(8,128)(2,1)S(1)}, u32[]{:S(2)}, u32[]{:S(2)}) collective-permute-start(bf16[2,2,128,512]{3,2,1,0:T(8,128)(2,1)S(1)} %pad_maximum_fusion.2.refs_0_), channel_id=1, source_target_pairs={{0,2},{1,5},{2,0},{3,7},{4,6},{5,1},{6,4},{7,3},{8,10},{9,13},{10,... | collective-permute-start | bytes 1572872 | tf_op jit(solution)/shard_map/ppermute | solution.py:167
  31.9 0.1 pad_maximum_fusion.1.refs_0_
  32.0 4.5 %collective-permute-done.2 = bf16[2,128,512]{2,1,0:T(8,128)(2,1)S(1)} collective-permute-done((bf16[2,128,512]{2,1,0:T(8,128)(2,1)S(1)}, bf16[2,128,512]{2,1,0:T(8,128)(2,1)S(1)}, u32[]{:S(2)}, u32[]{:S(2)}) %collective-permute-start.2) | collective-permute-done | bytes 262176 | tf_op jit(solution)/shard_map/ppermute | solution.py:167
  36.5 0.0 collective-permute-start.15
  36.5 3.7 %collective-permute-done.4 = bf16[2,128,512]{2,1,0:T(8,128)(2,1)S(1)} collective-permute-done((bf16[2,128,512]{2,1,0:T(8,128)(2,1)S(1)}, bf16[2,128,512]{2,1,0:T(8,128)(2,1)S(1)}, u32[]{:S(2)}, u32[]{:S(2)}) %collective-permute-start.4) | collective-permute-done | bytes 262176 | tf_op jit(solution)/shard_map/ppermute | solution.py:167
  40.2 0.7 collective-permute-start.8
  41.0 0.1 pad_maximum_fusion.refs_0_
  41.0 0.0 collective-permute-done.17.refs_1_
  41.0 0.1 collective-permute-start.19
  41.1 1.4 %collective-permute-start.5 = (bf16[2,2,128,512]{3,2,1,0:T(8,128)(2,1)S(1)}, bf16[2,2,128,512]{3,2,1,0:T(8,128)(2,1)S(1)}, u32[]{:S(2)}, u32[]{:S(2)}) collective-permute-start(bf16[2,2,128,512]{3,2,1,0:T(8,128)(2,1)S(1)} %pad_maximum_fusion.refs_0_), channel_id=1, source_target_pairs={{0,2},{1,5},{2,0},{3,7},{4,6},{5,1},{6,4},{7,3},{8,10},{9,13},{10,... | collective-permute-start | bytes 1572872 | tf_op jit(solution)/shard_map/ppermute | solution.py:167
  42.5 0.0 collective-permute-done.14.refs_1_
  42.5 0.1 collective-permute-start.16
  42.6 0.0 collective-permute-done.15.refs_2_
  42.6 0.4 collective-permute-start.9
  43.0 6.4 %collective-permute-done.8.refs_1_ = bf16[2,2,128,512]{3,2,1,0:T(8,128)(2,1)S(1)} collective-permute-done((bf16[2,2,128,512]{3,2,1,0:T(8,128)(2,1)S(1)}, bf16[2,2,128,512]{3,2,1,0:T(8,128)(2,1)S(1)}, u32[]{:S(2)}, u32[]{:S(2)}) %collective-permute-start.8) | collective-permute-done | bytes 524320 | tf_op jit(solution)/shard_map/ppermute | solution.py:167
  49.4 0.0 collective-permute-start.10
  49.4 0.0 collective-permute-done.19.refs_3_
  49.4 0.5 collective-permute-start.6
  49.9 5.1 %collective-permute-done.5.refs_1_ = bf16[2,2,128,512]{3,2,1,0:T(8,128)(2,1)S(1)} collective-permute-done((bf16[2,2,128,512]{3,2,1,0:T(8,128)(2,1)S(1)}, bf16[2,2,128,512]{3,2,1,0:T(8,128)(2,1)S(1)}, u32[]{:S(2)}, u32[]{:S(2)}) %collective-permute-start.5) | collective-permute-done | bytes 524320 | tf_op jit(solution)/shard_map/ppermute | solution.py:167
  55.0 0.0 collective-permute-start.7
  55.0 3.3 %shard_map.256 = (f32[2048,2048]{1,0:T(8,128)S(1)}, f32[256,2048]{1,0:T(8,128)S(1)}, f32[256,2048]{1,0:T(8,128)S(1)}) custom-call(s32[3]{0:T(128)S(1)} %pad_add_fusion.place, bf16[2,2,128,512]{3,2,1,0:T(8,128)(2,1)S(1)} %pad_maximum_fusion.3.refs_0_, bf16[2,2,128,512]{3,2,1,0:T(8,128)(2,1)S(1)} %collective-permute-done.17.refs_1_, ...), custom_call_target="tpu_custom_call" | custom-call | tf_op jit(solution)/shard_map/pallas_call | solution.py:447
  58.3 0.0 collective-permute-done.16.refs_3_
  58.3 3.5 %shard_map.257 = (f32[2048,2048]{1,0:T(8,128)S(1)}, bf16[256,2048]{1,0:T(8,128)(2,1)S(1)}, f32[256,256]{1,0:T(8,128)S(1)}, f32[256,256]{1,0:T(8,128)S(1)}, f32[2...) custom-call(s32[3]{0:T(128)S(1)} %pad_add_fusion.place, ...), custom_call_target="tpu_custom_call", output_to_operand_aliasing={{0}: (5, {})} | custom-call | tf_op jit(solution)/shard_map/pallas_call | solution.py:447
  61.9 0.0 collective-permute-done.9.refs_2_
  61.9 0.0 collective-permute-done.10.refs_3_
  61.9 3.4 %shard_map.258.refs_4_ = f32[2048,2048]{1,0:T(8,128)S(1)} custom-call(s32[3]{0:T(128)S(1)} %pad_add_fusion.place, bf16[2,2,128,512]{3,2,1,0:T(8,128)(2,1)S(1)} %pad_maximum_fusion.1.refs_0_, bf16[2,2,128,512]{3,2,1,0:T(8,128)(2,1)S(1)} %collective-permute-done.8.refs_1_, ...), custom_call_target="tpu_custom_call", output_to_operand_aliasing={{}: (5, {})} | custom-call | tf_op jit(solution)/shard_map/pallas_call | solution.py:447
  65.3 0.0 collective-permute-done.6.refs_2_
  65.3 0.0 collective-permute-done.7.refs_3_
  65.3 9.0 %tail.1 = (f32[256,256]{1,0:T(8,128)}, bf16[256,256]{1,0:T(8,128)(2,1)}, f32[256,256]{1,0:T(8,128)}, f32[256,256]{1,0:T(8,128)}, f32[256,2048]{1,0:T(8,128)}, /*...) custom-call(s32[3]{0:T(128)S(1)} %pad_add_fusion.place, ...), custom_call_target="tpu_custom_call" | custom-call | tf_op jit(solution)/shard_map/tail/pallas_call | solution.py:463
  (3 shorter events, 0.0 us)
Async XLA Ops:
  2.3 1.5 %collective-permute-start = (bf16[128,512]{1,0:T(8,128)(2,1)S(1)}, bf16[128,512]{1,0:T(8,128)(2,1)S(1)}, u32[]{:S(2)}, u32[]{:S(2)}) collective-permute-start(bf16[128,512]{1,0:T(8,128)(2,1)S(1)} %get-tuple-element.41), channel_id=1, source_target_pairs={{0,1},{1,0},{2,3},{3,2},{4,5},{5,4},{6,7},{7,6},{8,9},{9,8},{10,11... | collective-permute-start | bytes 393224 | tf_op jit(solution)/shard_map/ppermute | solution.py:167
  3.9 16.3 %collective-permute-start.1 = (bf16[2,128,512]{2,1,0:T(8,128)(2,1)S(1)}, bf16[2,128,512]{2,1,0:T(8,128)(2,1)S(1)}, u32[]{:S(2)}, u32[]{:S(2)}) collective-permute-start(bf16[2,128,512]{2,1,0:T(8,128)(2,1)S(1)} %get-tuple-element.69), channel_id=1, source_target_pairs={{0,16},{1,17},{2,18},{3,19},{4,20},{5,21},{6,22},{7,23},{8,24},{9,... | collective-permute-start | bytes 786440 | tf_op jit(solution)/shard_map/ppermute | solution.py:167
  7.9 13.9 %collective-permute-start.12 = (bf16[2,128,512]{2,1,0:T(8,128)(2,1)S(1)}, bf16[2,128,512]{2,1,0:T(8,128)(2,1)S(1)}, u32[]{:S(2)}, u32[]{:S(2)}) collective-permute-start(bf16[2,128,512]{2,1,0:T(8,128)(2,1)S(1)} %get-tuple-element.69), channel_id=1, source_target_pairs={{0,4},{1,3},{2,6},{3,1},{4,0},{5,7},{6,2},{7,5},{8,12},{9,11},{10,... | collective-permute-start | bytes 786440 | tf_op jit(solution)/shard_map/ppermute | solution.py:167
  9.4 14.6 %collective-permute-start.11 = (bf16[2,128,512]{2,1,0:T(8,128)(2,1)S(1)}, bf16[2,128,512]{2,1,0:T(8,128)(2,1)S(1)}, u32[]{:S(2)}, u32[]{:S(2)}) collective-permute-start(bf16[2,128,512]{2,1,0:T(8,128)(2,1)S(1)} %get-tuple-element.69), channel_id=1, source_target_pairs={{0,8},{1,9},{2,10},{3,11},{4,12},{5,13},{6,14},{7,15},{8,0},{9,1},... | collective-permute-start | bytes 786440 | tf_op jit(solution)/shard_map/ppermute | solution.py:167
  20.3 8.4 %collective-permute-start.3 = (bf16[2,128,512]{2,1,0:T(8,128)(2,1)S(1)}, bf16[2,128,512]{2,1,0:T(8,128)(2,1)S(1)}, u32[]{:S(2)}, u32[]{:S(2)}) collective-permute-start(bf16[2,128,512]{2,1,0:T(8,128)(2,1)S(1)} %collective-permute-done.1), channel_id=1, source_target_pairs={{0,4},{1,3},{2,6},{3,1},{4,0},{5,7},{6,2},{7,5},{8,12},{9,11},{10,... | collective-permute-start | bytes 786440 | tf_op jit(solution)/shard_map/ppermute | solution.py:167
  21.8 9.1 %collective-permute-start.13 = (bf16[2,128,512]{2,1,0:T(8,128)(2,1)S(1)}, bf16[2,128,512]{2,1,0:T(8,128)(2,1)S(1)}, u32[]{:S(2)}, u32[]{:S(2)}) collective-permute-start(bf16[2,128,512]{2,1,0:T(8,128)(2,1)S(1)} %collective-permute-done.12), channel_id=1, source_target_pairs={{0,8},{1,9},{2,10},{3,11},{4,12},{5,13},{6,14},{7,15},{8,0},{9,1},... | collective-permute-start | bytes 786440 | tf_op jit(solution)/shard_map/ppermute | solution.py:167
  22.5 18.5 %collective-permute-start.17 = (bf16[2,2,128,512]{3,2,1,0:T(8,128)(2,1)S(1)}, bf16[2,2,128,512]{3,2,1,0:T(8,128)(2,1)S(1)}, u32[]{:S(2)}, u32[]{:S(2)}) collective-permute-start(bf16[2,2,128,512]{3,2,1,0:T(8,128)(2,1)S(1)} %pad_maximum_fusion.3.refs_0_), channel_id=1, source_target_pairs={{0,2},{1,5},{2,0},{3,7},{4,6},{5,1},{6,4},{7,3},{8,10},{9,13},{10,... | collective-permute-start | bytes 1572872 | tf_op jit(solution)/shard_map/ppermute | solution.py:167
  24.0 17.1 %collective-permute-start.18 = (bf16[2,2,128,512]{3,2,1,0:T(8,128)(2,1)S(1)}, bf16[2,2,128,512]{3,2,1,0:T(8,128)(2,1)S(1)}, u32[]{:S(2)}, u32[]{:S(2)}) collective-permute-start(bf16[2,2,128,512]{3,2,1,0:T(8,128)(2,1)S(1)} %pad_maximum_fusion.3.refs_0_), channel_id=1, source_target_pairs={{0,1},{1,0},{2,3},{3,2},{4,5},{5,4},{6,7},{7,6},{8,9},{9,8},{10,11... | collective-permute-start | bytes 1572872 | tf_op jit(solution)/shard_map/ppermute | solution.py:167
  24.0 12.5 %collective-permute-start.2 = (bf16[2,128,512]{2,1,0:T(8,128)(2,1)S(1)}, bf16[2,128,512]{2,1,0:T(8,128)(2,1)S(1)}, u32[]{:S(2)}, u32[]{:S(2)}) collective-permute-start(bf16[2,128,512]{2,1,0:T(8,128)(2,1)S(1)} %collective-permute-done.1), channel_id=1, source_target_pairs={{0,8},{1,9},{2,10},{3,11},{4,12},{5,13},{6,14},{7,15},{8,0},{9,1},... | collective-permute-start | bytes 786440 | tf_op jit(solution)/shard_map/ppermute | solution.py:167
  28.7 11.6 %collective-permute-start.4 = (bf16[2,128,512]{2,1,0:T(8,128)(2,1)S(1)}, bf16[2,128,512]{2,1,0:T(8,128)(2,1)S(1)}, u32[]{:S(2)}, u32[]{:S(2)}) collective-permute-start(bf16[2,128,512]{2,1,0:T(8,128)(2,1)S(1)} %collective-permute-done.3), channel_id=1, source_target_pairs={{0,8},{1,9},{2,10},{3,11},{4,12},{5,13},{6,14},{7,15},{8,0},{9,1},... | collective-permute-start | bytes 786440 | tf_op jit(solution)/shard_map/ppermute | solution.py:167
  30.9 11.6 %collective-permute-start.14 = (bf16[2,2,128,512]{3,2,1,0:T(8,128)(2,1)S(1)}, bf16[2,2,128,512]{3,2,1,0:T(8,128)(2,1)S(1)}, u32[]{:S(2)}, u32[]{:S(2)}) collective-permute-start(bf16[2,2,128,512]{3,2,1,0:T(8,128)(2,1)S(1)} %pad_maximum_fusion.2.refs_0_), channel_id=1, source_target_pairs={{0,2},{1,5},{2,0},{3,7},{4,6},{5,1},{6,4},{7,3},{8,10},{9,13},{10,... | collective-permute-start | bytes 1572872 | tf_op jit(solution)/shard_map/ppermute | solution.py:167
  36.5 6.1 %collective-permute-start.15 = (bf16[2,2,128,512]{3,2,1,0:T(8,128)(2,1)S(1)}, bf16[2,2,128,512]{3,2,1,0:T(8,128)(2,1)S(1)}, u32[]{:S(2)}, u32[]{:S(2)}) collective-permute-start(bf16[2,2,128,512]{3,2,1,0:T(8,128)(2,1)S(1)} %pad_maximum_fusion.2.refs_0_), channel_id=1, source_target_pairs={{0,1},{1,0},{2,3},{3,2},{4,5},{5,4},{6,7},{7,6},{8,9},{9,8},{10,11... | collective-permute-start | bytes 1572872 | tf_op jit(solution)/shard_map/ppermute | solution.py:167
  40.2 9.2 %collective-permute-start.8 = (bf16[2,2,128,512]{3,2,1,0:T(8,128)(2,1)S(1)}, bf16[2,2,128,512]{3,2,1,0:T(8,128)(2,1)S(1)}, u32[]{:S(2)}, u32[]{:S(2)}) collective-permute-start(bf16[2,2,128,512]{3,2,1,0:T(8,128)(2,1)S(1)} %pad_maximum_fusion.1.refs_0_), channel_id=1, source_target_pairs={{0,2},{1,5},{2,0},{3,7},{4,6},{5,1},{6,4},{7,3},{8,10},{9,13},{10,... | collective-permute-start | bytes 1572872 | tf_op jit(solution)/shard_map/ppermute | solution.py:167
  41.0 8.4 %collective-permute-start.19 = (bf16[2,2,128,512]{3,2,1,0:T(8,128)(2,1)S(1)}, bf16[2,2,128,512]{3,2,1,0:T(8,128)(2,1)S(1)}, u32[]{:S(2)}, u32[]{:S(2)}) collective-permute-start(bf16[2,2,128,512]{3,2,1,0:T(8,128)(2,1)S(1)} %collective-permute-done.17.refs_1_), channel_id=1, source_target_pairs={{0,1},{1,0},{2,3},{3,2},{4,5},{5,4},{6,7},{7,6},{8,9},{9,8},{10,11... | collective-permute-start | bytes 1572872 | tf_op jit(solution)/shard_map/ppermute | solution.py:167
  41.1 13.9 %collective-permute-start.5 = (bf16[2,2,128,512]{3,2,1,0:T(8,128)(2,1)S(1)}, bf16[2,2,128,512]{3,2,1,0:T(8,128)(2,1)S(1)}, u32[]{:S(2)}, u32[]{:S(2)}) collective-permute-start(bf16[2,2,128,512]{3,2,1,0:T(8,128)(2,1)S(1)} %pad_maximum_fusion.refs_0_), channel_id=1, source_target_pairs={{0,2},{1,5},{2,0},{3,7},{4,6},{5,1},{6,4},{7,3},{8,10},{9,13},{10,... | collective-permute-start | bytes 1572872 | tf_op jit(solution)/shard_map/ppermute | solution.py:167
  42.5 15.8 %collective-permute-start.16 = (bf16[2,2,128,512]{3,2,1,0:T(8,128)(2,1)S(1)}, bf16[2,2,128,512]{3,2,1,0:T(8,128)(2,1)S(1)}, u32[]{:S(2)}, u32[]{:S(2)}) collective-permute-start(bf16[2,2,128,512]{3,2,1,0:T(8,128)(2,1)S(1)} %collective-permute-done.14.refs_1_), channel_id=1, source_target_pairs={{0,1},{1,0},{2,3},{3,2},{4,5},{5,4},{6,7},{7,6},{8,9},{9,8},{10,11... | collective-permute-start | bytes 1572872 | tf_op jit(solution)/shard_map/ppermute | solution.py:167
  42.6 19.3 %collective-permute-start.9 = (bf16[2,2,128,512]{3,2,1,0:T(8,128)(2,1)S(1)}, bf16[2,2,128,512]{3,2,1,0:T(8,128)(2,1)S(1)}, u32[]{:S(2)}, u32[]{:S(2)}) collective-permute-start(bf16[2,2,128,512]{3,2,1,0:T(8,128)(2,1)S(1)} %pad_maximum_fusion.1.refs_0_), channel_id=1, source_target_pairs={{0,1},{1,0},{2,3},{3,2},{4,5},{5,4},{6,7},{7,6},{8,9},{9,8},{10,11... | collective-permute-start | bytes 1572872 | tf_op jit(solution)/shard_map/ppermute | solution.py:167
  49.4 12.4 %collective-permute-start.10 = (bf16[2,2,128,512]{3,2,1,0:T(8,128)(2,1)S(1)}, bf16[2,2,128,512]{3,2,1,0:T(8,128)(2,1)S(1)}, u32[]{:S(2)}, u32[]{:S(2)}) collective-permute-start(bf16[2,2,128,512]{3,2,1,0:T(8,128)(2,1)S(1)} %collective-permute-done.8.refs_1_), channel_id=1, source_target_pairs={{0,1},{1,0},{2,3},{3,2},{4,5},{5,4},{6,7},{7,6},{8,9},{9,8},{10,11... | collective-permute-start | bytes 1572872 | tf_op jit(solution)/shard_map/ppermute | solution.py:167
  49.4 15.9 %collective-permute-start.6 = (bf16[2,2,128,512]{3,2,1,0:T(8,128)(2,1)S(1)}, bf16[2,2,128,512]{3,2,1,0:T(8,128)(2,1)S(1)}, u32[]{:S(2)}, u32[]{:S(2)}) collective-permute-start(bf16[2,2,128,512]{3,2,1,0:T(8,128)(2,1)S(1)} %pad_maximum_fusion.refs_0_), channel_id=1, source_target_pairs={{0,1},{1,0},{2,3},{3,2},{4,5},{5,4},{6,7},{7,6},{8,9},{9,8},{10,11... | collective-permute-start | bytes 1572872 | tf_op jit(solution)/shard_map/ppermute | solution.py:167
  55.0 10.3 %collective-permute-start.7 = (bf16[2,2,128,512]{3,2,1,0:T(8,128)(2,1)S(1)}, bf16[2,2,128,512]{3,2,1,0:T(8,128)(2,1)S(1)}, u32[]{:S(2)}, u32[]{:S(2)}) collective-permute-start(bf16[2,2,128,512]{3,2,1,0:T(8,128)(2,1)S(1)} %collective-permute-done.5.refs_1_), channel_id=1, source_target_pairs={{0,1},{1,0},{2,3},{3,2},{4,5},{5,4},{6,7},{7,6},{8,9},{9,8},{10,11... | collective-permute-start | bytes 1572872 | tf_op jit(solution)/shard_map/ppermute | solution.py:167

commit v5 on v4

--- a/solution.py
+++ b/solution.py
@@ -266,8 +266,8 @@
     refs = refs[12:]
     outs = [refs[6 * i : 6 * i + 6] for i in range(2)]
     refs = refs[12:]
-    x_set, y_set, grad, sem, store_sem = refs[:5]
-    made = [refs[5 + 6 * i : 11 + 6 * i] for i in range(2)]
+    x_set, y_set, grad, roots, sem, store_sem = refs[:6]
+    made = [refs[6 + 6 * i : 12 + 6 * i] for i in range(2)]
     odd, band = place[0], place[2]
     model, total = grad.shape
     hidden = total // 2
@@ -275,6 +275,12 @@
     rows_here = sides[0][0].shape[0]
 
     assemble(place, pieces, x_set, y_set, sem)
+    roots[...] = jnp.zeros(roots.shape, roots.dtype)
+    for i in range(2):
+        for k in range(2):
+            for h in range(own // HEAD):
+                at = slice(h * HEAD, (h + 1) * HEAD)
+                roots[i, k * own + h * HEAD : k * own + (h + 1) * HEAD, at] = sides[i][5][h]
     assembled(x_set, y_set, sem)
 
     chunk = x_set.shape[0]
@@ -293,7 +299,7 @@
 
     scales = []
     for i in range(2):
-        _, row_root, weight, moment, cols, col_root = sides[i]
+        _, row_root, weight, moment, cols, _ = sides[i]
         results, cols_next = made[i][:4], made[i][5]
         square = jnp.sum(squares[i], keepdims=True)
         scale = jnp.sqrt(model * hidden / (square + 1.0))
@@ -312,20 +318,18 @@
                 stat_decay * cols[h]
                 + (1.0 - stat_decay) / model * scale * scale * column_total[at, at]
             )
-            root = col_root[h]
-            precond = scale * (
-                jnp.dot(left_high[:, at], root, preferred_element_type=jnp.float32)
-                + jnp.dot(left_low[:, at], root, preferred_element_type=jnp.float32)
-            )
-            moment_next = moment_decay * moment[:, at] + (1.0 - moment_decay) * precond
-            update_step = moment_decay * moment_next + (1.0 - moment_decay) * precond
-            master = weight[:, at] - learn_rate * update_step
-            for to, value in zip(
-                results,
-                (master, master.astype(jnp.bfloat16), update_step, moment_next),
-                strict=True,
-            ):
-                to[:, at] = value
+        precond = scale * jnp.dot(
+            jnp.concatenate([left_high, left_low], axis=1),
+            roots[i],
+            preferred_element_type=jnp.float32,
+        )
+        moment_next = moment_decay * moment[...] + (1.0 - moment_decay) * precond
+        update_step = moment_decay * moment_next + (1.0 - moment_decay) * precond
+        master = weight[...] - learn_rate * update_step
+        for to, value in zip(
+            results, (master, master.astype(jnp.bfloat16), update_step, moment_next), strict=True
+        ):
+            to[...] = value
         for j, src in enumerate(results):
             store(src, outs[i][j], (i, j))
         store(cols_next, outs[i][5], (i, 4))
@@ -468,6 +472,7 @@
         scratch_shapes=set_scratch
         + [
             pltpu.VMEM((model, total), jnp.bfloat16),
+            pltpu.VMEM((2, 2 * query_weight.shape[1], query_weight.shape[1]), jnp.bfloat16),
             pltpu.SemaphoreType.DMA((2,)),
             pltpu.SemaphoreType.DMA((2, 5 + model // query_weight.shape[1] // 2)),
         ]

time: 74.6 us -> 74.4 us (level)
  no operation moved by 1% of the time
where the time goes in v5:
time: 74.4 us; the launch traced here: 74.2 us
  waiting for transfers between devices  34.8 us (47%)
  Pallas kernels  20.6 us (28%)
  starting transfers between devices  17.7 us (24%)
  between operations  0.94 us (1%)
    ppermute x20, waiting for transfers between devices, move(): return lax.ppermute(value, axes, linear_pairs(fs_size, tp_size, target))  34.8 us
    ppermute x20, starting transfers between devices, move(): return lax.ppermute(value, axes, linear_pairs(fs_size, tp_size, target))  17.7 us
    pallas_call x3, Pallas kernels, gathered_plan(): pl.pallas_call(partial(sum_kernel, not acc, len(fetch)), out_shape=[pltpu...  10.2 us
    pallas_call x1, Pallas kernels, gathered_plan(): pl.pallas_call(tail_kernel, out_shape=kinds * 2, in_specs=[smem] + [anywh...  8.77 us
    pallas_call x1, Pallas kernels, gathered_plan(): pl.pallas_call(prepare_kernel, out_shape=(pltpu.VMEM(inputs.shape, inputs...  1.61 us
  transfers between devices with their start and end apart: 20, of which 8 were waited for; matrix products, arithmetic and copies ran while one was open for 0% of the time, Pallas kernels for 14%

profile of v5, /device:TPU:0, one launch (start us, length us, event | category | flops | bytes accessed | tf_op | source)
XLA Modules:
  0.0 74.2 jit_solution(13366706290290023597)
XLA Ops:
  0.6 0.1 pad_add_fusion.place
  0.7 1.6 %prepare.1 = (bf16[128,512]{1,0:T(8,128)(2,1)S(1)}, bf16[128,512]{1,0:T(8,128)(2,1)S(1)}) custom-call(s32[3]{0:T(128)S(1)} %pad_add_fusion.place, bf16[128,512]{1,0:T(8,128)(2,1)} %refs_0_.1, bf16[128,256]{1,0:T(8,128)(2,1)} %refs_1_.1, bf16[128,256]{1,0:T(8,128)(2,1)} %refs_2_.1, bf16[128,256]{1,0:T(8,128)(2,1)} %refs_3_.1, f32[1,256]{1,0:T(1,128)} %bitcast.24), custom_call_target="tpu_custom_call" | custom-call | tf_op jit(solution)/shard_map/prepare/pallas_call | solution.py:418
  2.3 0.6 collective-permute-start
  2.9 1.0 %collective-permute-done = bf16[128,512]{1,0:T(8,128)(2,1)S(1)} collective-permute-done((bf16[128,512]{1,0:T(8,128)(2,1)S(1)}, bf16[128,512]{1,0:T(8,128)(2,1)S(1)}, u32[]{:S(2)}, u32[]{:S(2)}) %collective-permute-start) | collective-permute-done | bytes 131104 | tf_op jit(solution)/shard_map/ppermute | solution.py:167
  3.9 4.0 %collective-permute-start.1 = (bf16[2,128,512]{2,1,0:T(8,128)(2,1)S(1)}, bf16[2,128,512]{2,1,0:T(8,128)(2,1)S(1)}, u32[]{:S(2)}, u32[]{:S(2)}) collective-permute-start(bf16[2,128,512]{2,1,0:T(8,128)(2,1)S(1)} %get-tuple-element.69), channel_id=1, source_target_pairs={{0,16},{1,17},{2,18},{3,19},{4,20},{5,21},{6,22},{7,23},{8,24},{9,... | collective-permute-start | bytes 786440 | tf_op jit(solution)/shard_map/ppermute | solution.py:167
  7.9 1.5 %collective-permute-start.12 = (bf16[2,128,512]{2,1,0:T(8,128)(2,1)S(1)}, bf16[2,128,512]{2,1,0:T(8,128)(2,1)S(1)}, u32[]{:S(2)}, u32[]{:S(2)}) collective-permute-start(bf16[2,128,512]{2,1,0:T(8,128)(2,1)S(1)} %get-tuple-element.69), channel_id=1, source_target_pairs={{0,4},{1,3},{2,6},{3,1},{4,0},{5,7},{6,2},{7,5},{8,12},{9,11},{10,... | collective-permute-start | bytes 786440 | tf_op jit(solution)/shard_map/ppermute | solution.py:167
  9.4 1.6 %collective-permute-start.11 = (bf16[2,128,512]{2,1,0:T(8,128)(2,1)S(1)}, bf16[2,128,512]{2,1,0:T(8,128)(2,1)S(1)}, u32[]{:S(2)}, u32[]{:S(2)}) collective-permute-start(bf16[2,128,512]{2,1,0:T(8,128)(2,1)S(1)} %get-tuple-element.69), channel_id=1, source_target_pairs={{0,8},{1,9},{2,10},{3,11},{4,12},{5,13},{6,14},{7,15},{8,0},{9,1},... | collective-permute-start | bytes 786440 | tf_op jit(solution)/shard_map/ppermute | solution.py:167
  11.0 9.3 %collective-permute-done.1 = bf16[2,128,512]{2,1,0:T(8,128)(2,1)S(1)} collective-permute-done((bf16[2,128,512]{2,1,0:T(8,128)(2,1)S(1)}, bf16[2,128,512]{2,1,0:T(8,128)(2,1)S(1)}, u32[]{:S(2)}, u32[]{:S(2)}) %collective-permute-start.1) | collective-permute-done | bytes 262176 | tf_op jit(solution)/shard_map/ppermute | solution.py:167
  20.3 1.5 %collective-permute-start.3 = (bf16[2,128,512]{2,1,0:T(8,128)(2,1)S(1)}, bf16[2,128,512]{2,1,0:T(8,128)(2,1)S(1)}, u32[]{:S(2)}, u32[]{:S(2)}) collective-permute-start(bf16[2,128,512]{2,1,0:T(8,128)(2,1)S(1)} %collective-permute-done.1), channel_id=1, source_target_pairs={{0,4},{1,3},{2,6},{3,1},{4,0},{5,7},{6,2},{7,5},{8,12},{9,11},{10,... | collective-permute-start | bytes 786440 | tf_op jit(solution)/shard_map/ppermute | solution.py:167
  21.8 0.0 collective-permute-done.12
  21.8 0.6 collective-permute-start.13
  22.4 0.1 pad_maximum_fusion.3.refs_0_
  22.5 1.5 %collective-permute-start.17 = (bf16[2,2,128,512]{3,2,1,0:T(8,128)(2,1)S(1)}, bf16[2,2,128,512]{3,2,1,0:T(8,128)(2,1)S(1)}, u32[]{:S(2)}, u32[]{:S(2)}) collective-permute-start(bf16[2,2,128,512]{3,2,1,0:T(8,128)(2,1)S(1)} %pad_maximum_fusion.3.refs_0_), channel_id=1, source_target_pairs={{0,2},{1,5},{2,0},{3,7},{4,6},{5,1},{6,4},{7,3},{8,10},{9,13},{10,... | collective-permute-start | bytes 1572872 | tf_op jit(solution)/shard_map/ppermute | solution.py:167
  24.0 0.0 collective-permute-done.11
  24.0 1.4 %collective-permute-start.2 = (bf16[2,128,512]{2,1,0:T(8,128)(2,1)S(1)}, bf16[2,128,512]{2,1,0:T(8,128)(2,1)S(1)}, u32[]{:S(2)}, u32[]{:S(2)}) collective-permute-start(bf16[2,128,512]{2,1,0:T(8,128)(2,1)S(1)} %collective-permute-done.1), channel_id=1, source_target_pairs={{0,8},{1,9},{2,10},{3,11},{4,12},{5,13},{6,14},{7,15},{8,0},{9,1},... | collective-permute-start | bytes 786440 | tf_op jit(solution)/shard_map/ppermute | solution.py:167
  25.5 3.2 %collective-permute-done.3 = bf16[2,128,512]{2,1,0:T(8,128)(2,1)S(1)} collective-permute-done((bf16[2,128,512]{2,1,0:T(8,128)(2,1)S(1)}, bf16[2,128,512]{2,1,0:T(8,128)(2,1)S(1)}, u32[]{:S(2)}, u32[]{:S(2)}) %collective-permute-start.3) | collective-permute-done | bytes 262176 | tf_op jit(solution)/shard_map/ppermute | solution.py:167
  28.7 0.7 collective-permute-start.4
  29.4 1.5 %collective-permute-done.13 = bf16[2,128,512]{2,1,0:T(8,128)(2,1)S(1)} collective-permute-done((bf16[2,128,512]{2,1,0:T(8,128)(2,1)S(1)}, bf16[2,128,512]{2,1,0:T(8,128)(2,1)S(1)}, u32[]{:S(2)}, u32[]{:S(2)}) %collective-permute-start.13) | collective-permute-done | bytes 262176 | tf_op jit(solution)/shard_map/ppermute | solution.py:167
  30.9 0.1 pad_maximum_fusion.2.refs_0_
  30.9 1.0 %collective-permute-start.14 = (bf16[2,2,128,512]{3,2,1,0:T(8,128)(2,1)S(1)}, bf16[2,2,128,512]{3,2,1,0:T(8,128)(2,1)S(1)}, u32[]{:S(2)}, u32[]{:S(2)}) collective-permute-start(bf16[2,2,128,512]{3,2,1,0:T(8,128)(2,1)S(1)} %pad_maximum_fusion.2.refs_0_), channel_id=1, source_target_pairs={{0,2},{1,5},{2,0},{3,7},{4,6},{5,1},{6,4},{7,3},{8,10},{9,13},{10,... | collective-permute-start | bytes 1572872 | tf_op jit(solution)/shard_map/ppermute | solution.py:167
  31.9 0.1 pad_maximum_fusion.1.refs_0_
  32.0 4.5 %collective-permute-done.2 = bf16[2,128,512]{2,1,0:T(8,128)(2,1)S(1)} collective-permute-done((bf16[2,128,512]{2,1,0:T(8,128)(2,1)S(1)}, bf16[2,128,512]{2,1,0:T(8,128)(2,1)S(1)}, u32[]{:S(2)}, u32[]{:S(2)}) %collective-permute-start.2) | collective-permute-done | bytes 262176 | tf_op jit(solution)/shard_map/ppermute | solution.py:167
  36.5 0.0 collective-permute-start.15
  36.5 3.7 %collective-permute-done.4 = bf16[2,128,512]{2,1,0:T(8,128)(2,1)S(1)} collective-permute-done((bf16[2,128,512]{2,1,0:T(8,128)(2,1)S(1)}, bf16[2,128,512]{2,1,0:T(8,128)(2,1)S(1)}, u32[]{:S(2)}, u32[]{:S(2)}) %collective-permute-start.4) | collective-permute-done | bytes 262176 | tf_op jit(solution)/shard_map/ppermute | solution.py:167
  40.2 0.7 collective-permute-start.8
  41.0 0.1 pad_maximum_fusion.refs_0_
  41.0 0.0 collective-permute-done.17.refs_1_
  41.0 0.1 collective-permute-start.19
  41.1 1.4 %collective-permute-start.5 = (bf16[2,2,128,512]{3,2,1,0:T(8,128)(2,1)S(1)}, bf16[2,2,128,512]{3,2,1,0:T(8,128)(2,1)S(1)}, u32[]{:S(2)}, u32[]{:S(2)}) collective-permute-start(bf16[2,2,128,512]{3,2,1,0:T(8,128)(2,1)S(1)} %pad_maximum_fusion.refs_0_), channel_id=1, source_target_pairs={{0,2},{1,5},{2,0},{3,7},{4,6},{5,1},{6,4},{7,3},{8,10},{9,13},{10,... | collective-permute-start | bytes 1572872 | tf_op jit(solution)/shard_map/ppermute | solution.py:167
  42.5 0.0 collective-permute-done.14.refs_1_
  42.5 0.1 collective-permute-start.16
  42.6 0.0 collective-permute-done.15.refs_2_
  42.6 0.4 collective-permute-start.9
  43.0 6.4 %collective-permute-done.8.refs_1_ = bf16[2,2,128,512]{3,2,1,0:T(8,128)(2,1)S(1)} collective-permute-done((bf16[2,2,128,512]{3,2,1,0:T(8,128)(2,1)S(1)}, bf16[2,2,128,512]{3,2,1,0:T(8,128)(2,1)S(1)}, u32[]{:S(2)}, u32[]{:S(2)}) %collective-permute-start.8) | collective-permute-done | bytes 524320 | tf_op jit(solution)/shard_map/ppermute | solution.py:167
  49.4 0.0 collective-permute-start.10
  49.4 0.0 collective-permute-done.19.refs_3_
  49.4 0.5 collective-permute-start.6
  49.9 5.1 %collective-permute-done.5.refs_1_ = bf16[2,2,128,512]{3,2,1,0:T(8,128)(2,1)S(1)} collective-permute-done((bf16[2,2,128,512]{3,2,1,0:T(8,128)(2,1)S(1)}, bf16[2,2,128,512]{3,2,1,0:T(8,128)(2,1)S(1)}, u32[]{:S(2)}, u32[]{:S(2)}) %collective-permute-start.5) | collective-permute-done | bytes 524320 | tf_op jit(solution)/shard_map/ppermute | solution.py:167
  55.0 0.0 collective-permute-start.7
  55.0 3.3 %shard_map.256 = (f32[2048,2048]{1,0:T(8,128)S(1)}, f32[256,2048]{1,0:T(8,128)S(1)}, f32[256,2048]{1,0:T(8,128)S(1)}) custom-call(s32[3]{0:T(128)S(1)} %pad_add_fusion.place, bf16[2,2,128,512]{3,2,1,0:T(8,128)(2,1)S(1)} %pad_maximum_fusion.3.refs_0_, bf16[2,2,128,512]{3,2,1,0:T(8,128)(2,1)S(1)} %collective-permute-done.17.refs_1_, ...), custom_call_target="tpu_custom_call" | custom-call | tf_op jit(solution)/shard_map/pallas_call | solution.py:451
  58.3 0.0 collective-permute-done.16.refs_3_
  58.3 3.5 %shard_map.257 = (f32[2048,2048]{1,0:T(8,128)S(1)}, bf16[256,2048]{1,0:T(8,128)(2,1)S(1)}, f32[256,256]{1,0:T(8,128)S(1)}, f32[256,256]{1,0:T(8,128)S(1)}, f32[2...) custom-call(s32[3]{0:T(128)S(1)} %pad_add_fusion.place, ...), custom_call_target="tpu_custom_call", output_to_operand_aliasing={{0}: (5, {})} | custom-call | tf_op jit(solution)/shard_map/pallas_call | solution.py:451
  61.9 0.0 collective-permute-done.9.refs_2_
  61.9 0.0 collective-permute-done.10.refs_3_
  61.9 3.4 %shard_map.258.refs_4_ = f32[2048,2048]{1,0:T(8,128)S(1)} custom-call(s32[3]{0:T(128)S(1)} %pad_add_fusion.place, bf16[2,2,128,512]{3,2,1,0:T(8,128)(2,1)S(1)} %pad_maximum_fusion.1.refs_0_, bf16[2,2,128,512]{3,2,1,0:T(8,128)(2,1)S(1)} %collective-permute-done.8.refs_1_, ...), custom_call_target="tpu_custom_call", output_to_operand_aliasing={{}: (5, {})} | custom-call | tf_op jit(solution)/shard_map/pallas_call | solution.py:451
  65.3 0.0 collective-permute-done.6.refs_2_
  65.3 0.0 collective-permute-done.7.refs_3_
  65.3 8.8 %tail.1 = (f32[256,256]{1,0:T(8,128)}, bf16[256,256]{1,0:T(8,128)(2,1)}, f32[256,256]{1,0:T(8,128)}, f32[256,256]{1,0:T(8,128)}, f32[256,2048]{1,0:T(8,128)}, /*...) custom-call(s32[3]{0:T(128)S(1)} %pad_add_fusion.place, ...), custom_call_target="tpu_custom_call" | custom-call | tf_op jit(solution)/shard_map/tail/pallas_call | solution.py:467
  (3 shorter events, 0.0 us)
Async XLA Ops:
  2.3 1.5 %collective-permute-start = (bf16[128,512]{1,0:T(8,128)(2,1)S(1)}, bf16[128,512]{1,0:T(8,128)(2,1)S(1)}, u32[]{:S(2)}, u32[]{:S(2)}) collective-permute-start(bf16[128,512]{1,0:T(8,128)(2,1)S(1)} %get-tuple-element.41), channel_id=1, source_target_pairs={{0,1},{1,0},{2,3},{3,2},{4,5},{5,4},{6,7},{7,6},{8,9},{9,8},{10,11... | collective-permute-start | bytes 393224 | tf_op jit(solution)/shard_map/ppermute | solution.py:167
  3.9 16.3 %collective-permute-start.1 = (bf16[2,128,512]{2,1,0:T(8,128)(2,1)S(1)}, bf16[2,128,512]{2,1,0:T(8,128)(2,1)S(1)}, u32[]{:S(2)}, u32[]{:S(2)}) collective-permute-start(bf16[2,128,512]{2,1,0:T(8,128)(2,1)S(1)} %get-tuple-element.69), channel_id=1, source_target_pairs={{0,16},{1,17},{2,18},{3,19},{4,20},{5,21},{6,22},{7,23},{8,24},{9,... | collective-permute-start | bytes 786440 | tf_op jit(solution)/shard_map/ppermute | solution.py:167
  7.9 13.9 %collective-permute-start.12 = (bf16[2,128,512]{2,1,0:T(8,128)(2,1)S(1)}, bf16[2,128,512]{2,1,0:T(8,128)(2,1)S(1)}, u32[]{:S(2)}, u32[]{:S(2)}) collective-permute-start(bf16[2,128,512]{2,1,0:T(8,128)(2,1)S(1)} %get-tuple-element.69), channel_id=1, source_target_pairs={{0,4},{1,3},{2,6},{3,1},{4,0},{5,7},{6,2},{7,5},{8,12},{9,11},{10,... | collective-permute-start | bytes 786440 | tf_op jit(solution)/shard_map/ppermute | solution.py:167
  9.4 14.6 %collective-permute-start.11 = (bf16[2,128,512]{2,1,0:T(8,128)(2,1)S(1)}, bf16[2,128,512]{2,1,0:T(8,128)(2,1)S(1)}, u32[]{:S(2)}, u32[]{:S(2)}) collective-permute-start(bf16[2,128,512]{2,1,0:T(8,128)(2,1)S(1)} %get-tuple-element.69), channel_id=1, source_target_pairs={{0,8},{1,9},{2,10},{3,11},{4,12},{5,13},{6,14},{7,15},{8,0},{9,1},... | collective-permute-start | bytes 786440 | tf_op jit(solution)/shard_map/ppermute | solution.py:167
  20.3 8.4 %collective-permute-start.3 = (bf16[2,128,512]{2,1,0:T(8,128)(2,1)S(1)}, bf16[2,128,512]{2,1,0:T(8,128)(2,1)S(1)}, u32[]{:S(2)}, u32[]{:S(2)}) collective-permute-start(bf16[2,128,512]{2,1,0:T(8,128)(2,1)S(1)} %collective-permute-done.1), channel_id=1, source_target_pairs={{0,4},{1,3},{2,6},{3,1},{4,0},{5,7},{6,2},{7,5},{8,12},{9,11},{10,... | collective-permute-start | bytes 786440 | tf_op jit(solution)/shard_map/ppermute | solution.py:167
  21.8 9.1 %collective-permute-start.13 = (bf16[2,128,512]{2,1,0:T(8,128)(2,1)S(1)}, bf16[2,128,512]{2,1,0:T(8,128)(2,1)S(1)}, u32[]{:S(2)}, u32[]{:S(2)}) collective-permute-start(bf16[2,128,512]{2,1,0:T(8,128)(2,1)S(1)} %collective-permute-done.12), channel_id=1, source_target_pairs={{0,8},{1,9},{2,10},{3,11},{4,12},{5,13},{6,14},{7,15},{8,0},{9,1},... | collective-permute-start | bytes 786440 | tf_op jit(solution)/shard_map/ppermute | solution.py:167
  22.5 18.5 %collective-permute-start.17 = (bf16[2,2,128,512]{3,2,1,0:T(8,128)(2,1)S(1)}, bf16[2,2,128,512]{3,2,1,0:T(8,128)(2,1)S(1)}, u32[]{:S(2)}, u32[]{:S(2)}) collective-permute-start(bf16[2,2,128,512]{3,2,1,0:T(8,128)(2,1)S(1)} %pad_maximum_fusion.3.refs_0_), channel_id=1, source_target_pairs={{0,2},{1,5},{2,0},{3,7},{4,6},{5,1},{6,4},{7,3},{8,10},{9,13},{10,... | collective-permute-start | bytes 1572872 | tf_op jit(solution)/shard_map/ppermute | solution.py:167
  24.0 17.1 %collective-permute-start.18 = (bf16[2,2,128,512]{3,2,1,0:T(8,128)(2,1)S(1)}, bf16[2,2,128,512]{3,2,1,0:T(8,128)(2,1)S(1)}, u32[]{:S(2)}, u32[]{:S(2)}) collective-permute-start(bf16[2,2,128,512]{3,2,1,0:T(8,128)(2,1)S(1)} %pad_maximum_fusion.3.refs_0_), channel_id=1, source_target_pairs={{0,1},{1,0},{2,3},{3,2},{4,5},{5,4},{6,7},{7,6},{8,9},{9,8},{10,11... | collective-permute-start | bytes 1572872 | tf_op jit(solution)/shard_map/ppermute | solution.py:167
  24.0 12.5 %collective-permute-start.2 = (bf16[2,128,512]{2,1,0:T(8,128)(2,1)S(1)}, bf16[2,128,512]{2,1,0:T(8,128)(2,1)S(1)}, u32[]{:S(2)}, u32[]{:S(2)}) collective-permute-start(bf16[2,128,512]{2,1,0:T(8,128)(2,1)S(1)} %collective-permute-done.1), channel_id=1, source_target_pairs={{0,8},{1,9},{2,10},{3,11},{4,12},{5,13},{6,14},{7,15},{8,0},{9,1},... | collective-permute-start | bytes 786440 | tf_op jit(solution)/shard_map/ppermute | solution.py:167
  28.7 11.6 %collective-permute-start.4 = (bf16[2,128,512]{2,1,0:T(8,128)(2,1)S(1)}, bf16[2,128,512]{2,1,0:T(8,128)(2,1)S(1)}, u32[]{:S(2)}, u32[]{:S(2)}) collective-permute-start(bf16[2,128,512]{2,1,0:T(8,128)(2,1)S(1)} %collective-permute-done.3), channel_id=1, source_target_pairs={{0,8},{1,9},{2,10},{3,11},{4,12},{5,13},{6,14},{7,15},{8,0},{9,1},... | collective-permute-start | bytes 786440 | tf_op jit(solution)/shard_map/ppermute | solution.py:167
  30.9 11.6 %collective-permute-start.14 = (bf16[2,2,128,512]{3,2,1,0:T(8,128)(2,1)S(1)}, bf16[2,2,128,512]{3,2,1,0:T(8,128)(2,1)S(1)}, u32[]{:S(2)}, u32[]{:S(2)}) collective-permute-start(bf16[2,2,128,512]{3,2,1,0:T(8,128)(2,1)S(1)} %pad_maximum_fusion.2.refs_0_), channel_id=1, source_target_pairs={{0,2},{1,5},{2,0},{3,7},{4,6},{5,1},{6,4},{7,3},{8,10},{9,13},{10,... | collective-permute-start | bytes 1572872 | tf_op jit(solution)/shard_map/ppermute | solution.py:167
  36.5 6.1 %collective-permute-start.15 = (bf16[2,2,128,512]{3,2,1,0:T(8,128)(2,1)S(1)}, bf16[2,2,128,512]{3,2,1,0:T(8,128)(2,1)S(1)}, u32[]{:S(2)}, u32[]{:S(2)}) collective-permute-start(bf16[2,2,128,512]{3,2,1,0:T(8,128)(2,1)S(1)} %pad_maximum_fusion.2.refs_0_), channel_id=1, source_target_pairs={{0,1},{1,0},{2,3},{3,2},{4,5},{5,4},{6,7},{7,6},{8,9},{9,8},{10,11... | collective-permute-start | bytes 1572872 | tf_op jit(solution)/shard_map/ppermute | solution.py:167
  40.2 9.2 %collective-permute-start.8 = (bf16[2,2,128,512]{3,2,1,0:T(8,128)(2,1)S(1)}, bf16[2,2,128,512]{3,2,1,0:T(8,128)(2,1)S(1)}, u32[]{:S(2)}, u32[]{:S(2)}) collective-permute-start(bf16[2,2,128,512]{3,2,1,0:T(8,128)(2,1)S(1)} %pad_maximum_fusion.1.refs_0_), channel_id=1, source_target_pairs={{0,2},{1,5},{2,0},{3,7},{4,6},{5,1},{6,4},{7,3},{8,10},{9,13},{10,... | collective-permute-start | bytes 1572872 | tf_op jit(solution)/shard_map/ppermute | solution.py:167
  41.0 8.4 %collective-permute-start.19 = (bf16[2,2,128,512]{3,2,1,0:T(8,128)(2,1)S(1)}, bf16[2,2,128,512]{3,2,1,0:T(8,128)(2,1)S(1)}, u32[]{:S(2)}, u32[]{:S(2)}) collective-permute-start(bf16[2,2,128,512]{3,2,1,0:T(8,128)(2,1)S(1)} %collective-permute-done.17.refs_1_), channel_id=1, source_target_pairs={{0,1},{1,0},{2,3},{3,2},{4,5},{5,4},{6,7},{7,6},{8,9},{9,8},{10,11... | collective-permute-start | bytes 1572872 | tf_op jit(solution)/shard_map/ppermute | solution.py:167
  41.1 13.9 %collective-permute-start.5 = (bf16[2,2,128,512]{3,2,1,0:T(8,128)(2,1)S(1)}, bf16[2,2,128,512]{3,2,1,0:T(8,128)(2,1)S(1)}, u32[]{:S(2)}, u32[]{:S(2)}) collective-permute-start(bf16[2,2,128,512]{3,2,1,0:T(8,128)(2,1)S(1)} %pad_maximum_fusion.refs_0_), channel_id=1, source_target_pairs={{0,2},{1,5},{2,0},{3,7},{4,6},{5,1},{6,4},{7,3},{8,10},{9,13},{10,... | collective-permute-start | bytes 1572872 | tf_op jit(solution)/shard_map/ppermute | solution.py:167
  42.5 15.8 %collective-permute-start.16 = (bf16[2,2,128,512]{3,2,1,0:T(8,128)(2,1)S(1)}, bf16[2,2,128,512]{3,2,1,0:T(8,128)(2,1)S(1)}, u32[]{:S(2)}, u32[]{:S(2)}) collective-permute-start(bf16[2,2,128,512]{3,2,1,0:T(8,128)(2,1)S(1)} %collective-permute-done.14.refs_1_), channel_id=1, source_target_pairs={{0,1},{1,0},{2,3},{3,2},{4,5},{5,4},{6,7},{7,6},{8,9},{9,8},{10,11... | collective-permute-start | bytes 1572872 | tf_op jit(solution)/shard_map/ppermute | solution.py:167
  42.6 19.3 %collective-permute-start.9 = (bf16[2,2,128,512]{3,2,1,0:T(8,128)(2,1)S(1)}, bf16[2,2,128,512]{3,2,1,0:T(8,128)(2,1)S(1)}, u32[]{:S(2)}, u32[]{:S(2)}) collective-permute-start(bf16[2,2,128,512]{3,2,1,0:T(8,128)(2,1)S(1)} %pad_maximum_fusion.1.refs_0_), channel_id=1, source_target_pairs={{0,1},{1,0},{2,3},{3,2},{4,5},{5,4},{6,7},{7,6},{8,9},{9,8},{10,11... | collective-permute-start | bytes 1572872 | tf_op jit(solution)/shard_map/ppermute | solution.py:167
  49.4 12.4 %collective-permute-start.10 = (bf16[2,2,128,512]{3,2,1,0:T(8,128)(2,1)S(1)}, bf16[2,2,128,512]{3,2,1,0:T(8,128)(2,1)S(1)}, u32[]{:S(2)}, u32[]{:S(2)}) collective-permute-start(bf16[2,2,128,512]{3,2,1,0:T(8,128)(2,1)S(1)} %collective-permute-done.8.refs_1_), channel_id=1, source_target_pairs={{0,1},{1,0},{2,3},{3,2},{4,5},{5,4},{6,7},{7,6},{8,9},{9,8},{10,11... | collective-permute-start | bytes 1572872 | tf_op jit(solution)/shard_map/ppermute | solution.py:167
  49.4 15.9 %collective-permute-start.6 = (bf16[2,2,128,512]{3,2,1,0:T(8,128)(2,1)S(1)}, bf16[2,2,128,512]{3,2,1,0:T(8,128)(2,1)S(1)}, u32[]{:S(2)}, u32[]{:S(2)}) collective-permute-start(bf16[2,2,128,512]{3,2,1,0:T(8,128)(2,1)S(1)} %pad_maximum_fusion.refs_0_), channel_id=1, source_target_pairs={{0,1},{1,0},{2,3},{3,2},{4,5},{5,4},{6,7},{7,6},{8,9},{9,8},{10,11... | collective-permute-start | bytes 1572872 | tf_op jit(solution)/shard_map/ppermute | solution.py:167
  55.0 10.3 %collective-permute-start.7 = (bf16[2,2,128,512]{3,2,1,0:T(8,128)(2,1)S(1)}, bf16[2,2,128,512]{3,2,1,0:T(8,128)(2,1)S(1)}, u32[]{:S(2)}, u32[]{:S(2)}) collective-permute-start(bf16[2,2,128,512]{3,2,1,0:T(8,128)(2,1)S(1)} %collective-permute-done.5.refs_1_), channel_id=1, source_target_pairs={{0,1},{1,0},{2,3},{3,2},{4,5},{5,4},{6,7},{7,6},{8,9},{9,8},{10,11... | collective-permute-start | bytes 1572872 | tf_op jit(solution)/shard_map/ppermute | solution.py:167

commit v6 on v5

--- a/solution.py
+++ b/solution.py
@@ -193,6 +193,11 @@
     return sets
 
 
+def position():
+    tp_at = lax.axis_index("tp")
+    return tp_at & 1, tp_at >> 1, lax.axis_index("fs")
+
+
 def assemble(place, pieces, x_set, y_set, sem):
     odd, upper = place[0], place[1]
     tokens, width = pieces[0].shape[2:]
@@ -237,7 +242,8 @@
     )
 
 
-def sum_kernel(first, n_fetched, place, *refs):
+def sum_kernel(first, n_fetched, *refs):
+    place = position()
     pieces, refs = refs[:4], refs[4:]
     if not first:
         refs = refs[1:]
@@ -260,7 +266,8 @@
         copy.wait()
 
 
-def tail_kernel(place, *refs):
+def tail_kernel(*refs):
+    place = position()
     pieces, acc, refs = refs[:4], refs[4], refs[5:]
     sides = [refs[6 * i : 6 * i + 6] for i in range(2)]
     refs = refs[12:]
@@ -353,7 +360,8 @@
         copy.wait()
 
 
-def prepare_kernel(place, *refs):
+def prepare_kernel(*refs):
+    place = position()
     sources, (keep, send), held, sem = refs[:5], refs[5:7], refs[7:12], refs[12]
     copies = [
         pltpu.make_async_copy(src, dst, sem.at[j])
@@ -408,9 +416,6 @@
     fs_size,
     tp_size,
 ):
-    tp_at = lax.axis_index("tp")
-    place = jnp.stack([tp_at & 1, tp_at >> 1, lax.axis_index("fs")]).astype(jnp.int32)
-    smem = pl.BlockSpec(memory_space=pltpu.SMEM)
     vmem = pl.BlockSpec(memory_space=pltpu.VMEM)
     params = pltpu.CompilerParams(vmem_limit_bytes=21 * 2**20)
     hbm = pl.BlockSpec(memory_space=pltpu.HBM)
@@ -418,13 +423,13 @@
     keep, send = pl.pallas_call(
         prepare_kernel,
         out_shape=(pltpu.VMEM(inputs.shape, inputs.dtype),) * 2,
-        in_specs=[smem] + [hbm] * 5,
+        in_specs=[hbm] * 5,
         out_specs=[vmem] * 2,
         scratch_shapes=[pltpu.VMEM(v.shape, v.dtype) for v in saved]
         + [pltpu.SemaphoreType.DMA((5,))],
         compiler_params=params,
         name="prepare",
-    )(place, *(pltpu.with_memory_space_constraint(v, pltpu.HBM) for v in saved))
+    )(*(pltpu.with_memory_space_constraint(v, pltpu.HBM) for v in saved))
     sets = gather_operands(keep, send, fs_size, tp_size)
     model = inputs.shape[1] * tp_size
     total = 2 * query_grad.shape[1] * tp_size
@@ -452,13 +457,13 @@
             partial(sum_kernel, not acc, len(fetch)),
             out_shape=[pltpu.VMEM((model, total), jnp.float32)]
             + [pltpu.VMEM(v.shape, v.dtype) for v in fetch],
-            in_specs=[smem] + [anywhere] * 4 + [vmem] * len(acc) + [hbm] * len(fetch),
+            in_specs=[anywhere] * 4 + [vmem] * len(acc) + [hbm] * len(fetch),
             out_specs=[vmem] * (1 + len(fetch)),
             scratch_shapes=set_scratch
             + [pltpu.SemaphoreType.DMA((2,)), pltpu.SemaphoreType.DMA((max(len(fetch), 1),))],
-            input_output_aliases={5: 0} if acc else {},
+            input_output_aliases={4: 0} if acc else {},
             compiler_params=pltpu.CompilerParams(vmem_limit_bytes=12 * 2**20),
-        )(place, *pieces, *acc, *fetch)
+        )(*pieces, *acc, *fetch)
         acc, fetched = made[:1], fetched + list(made[1:])
     half = len(fetched[2:]) // 2
     loaded = [fetched[0], *fetched[2 : 2 + half], fetched[1], *fetched[2 + half :]]
@@ -467,7 +472,7 @@
     out = pl.pallas_call(
         tail_kernel,
         out_shape=kinds * 2,
-        in_specs=[smem] + [anywhere] * 4 + [vmem] * 13,
+        in_specs=[anywhere] * 4 + [vmem] * 13,
         out_specs=[hbm] * 12,
         scratch_shapes=set_scratch
         + [
@@ -479,7 +484,7 @@
         + held,
         compiler_params=params,
         name="tail",
-    )(place, *operands)
+    )(*operands)
     return tuple(v for both in zip(out[:6], out[6:], strict=True) for v in both)
 
 

time: 74.4 us -> 71.3 us (0.958)
  Pallas kernels: 20.6 us -> 17.5 us
    pallas_call x3, Pallas kernels: 10.2 us -> 8.28 us  [gathered_plan(): pl.pallas_call(partial(sum_kernel, not acc, len(fetch)), out_shape=[pltpu...]
  transfers between devices with their start and end apart: 20 -> 20, of which waited for: 8 -> 8; matrix products, arithmetic and copies ran while one was open for 0% -> 0% of each run, Pallas kernels for 14% -> 12%
where the time goes in v6:
time: 71.3 us; the launch traced here: 71.1 us
  waiting for transfers between devices  34.8 us (49%)
  starting transfers between devices  17.7 us (25%)
  Pallas kernels  17.5 us (25%)
  between operations  0.93 us (1%)
    ppermute x20, waiting for transfers between devices, move(): return lax.ppermute(value, axes, linear_pairs(fs_size, tp_size, target))  34.8 us
    ppermute x20, starting transfers between devices, move(): return lax.ppermute(value, axes, linear_pairs(fs_size, tp_size, target))  17.7 us
    pallas_call x3, Pallas kernels, gathered_plan(): pl.pallas_call(partial(sum_kernel, not acc, len(fetch)), out_shape=[pltpu...  8.28 us
    pallas_call x1, Pallas kernels, gathered_plan(): pl.pallas_call(tail_kernel, out_shape=kinds * 2, in_specs=[anywhere] * 4...  8.15 us
  transfers between devices with their start and end apart: 20, of which 8 were waited for; matrix products, arithmetic and copies ran while one was open for 0% of the time, Pallas kernels for 12%

profile of v6, /device:TPU:0, one launch (start us, length us, event | category | flops | bytes accessed | tf_op | source)
XLA Modules:
  0.0 71.1 jit_solution(1314463987183080895)
XLA Ops:
  0.6 1.1 %prepare.1 = (bf16[128,512]{1,0:T(8,128)(2,1)S(1)}, bf16[128,512]{1,0:T(8,128)(2,1)S(1)}) custom-call(bf16[128,512]{1,0:T(8,128)(2,1)} %refs_0_.1, bf16[128,256]{1,0:T(8,128)(2,1)} %refs_1_.1, bf16[128,256]{1,0:T(8,128)(2,1)} %refs_2_.1, bf16[128,256]{1,0:T(8,128)(2,1)} %refs_3_.1, f32[1,256]{1,0:T(1,128)} %bitcast.21), custom_call_target="tpu_custom_call" | custom-call | tf_op jit(solution)/shard_map/prepare/pallas_call | solution.py:423
  1.7 0.6 collective-permute-start
  2.3 1.0 %collective-permute-done = bf16[128,512]{1,0:T(8,128)(2,1)S(1)} collective-permute-done((bf16[128,512]{1,0:T(8,128)(2,1)S(1)}, bf16[128,512]{1,0:T(8,128)(2,1)S(1)}, u32[]{:S(2)}, u32[]{:S(2)}) %collective-permute-start) | collective-permute-done | bytes 131104 | tf_op jit(solution)/shard_map/ppermute | solution.py:167
  3.3 4.0 %collective-permute-start.1 = (bf16[2,128,512]{2,1,0:T(8,128)(2,1)S(1)}, bf16[2,128,512]{2,1,0:T(8,128)(2,1)S(1)}, u32[]{:S(2)}, u32[]{:S(2)}) collective-permute-start(bf16[2,128,512]{2,1,0:T(8,128)(2,1)S(1)} %get-tuple-element.69), channel_id=1, source_target_pairs={{0,16},{1,17},{2,18},{3,19},{4,20},{5,21},{6,22},{7,23},{8,24},{9,... | collective-permute-start | bytes 786440 | tf_op jit(solution)/shard_map/ppermute | solution.py:167
  7.3 1.5 %collective-permute-start.12 = (bf16[2,128,512]{2,1,0:T(8,128)(2,1)S(1)}, bf16[2,128,512]{2,1,0:T(8,128)(2,1)S(1)}, u32[]{:S(2)}, u32[]{:S(2)}) collective-permute-start(bf16[2,128,512]{2,1,0:T(8,128)(2,1)S(1)} %get-tuple-element.69), channel_id=1, source_target_pairs={{0,4},{1,3},{2,6},{3,1},{4,0},{5,7},{6,2},{7,5},{8,12},{9,11},{10,... | collective-permute-start | bytes 786440 | tf_op jit(solution)/shard_map/ppermute | solution.py:167
  8.8 1.6 %collective-permute-start.11 = (bf16[2,128,512]{2,1,0:T(8,128)(2,1)S(1)}, bf16[2,128,512]{2,1,0:T(8,128)(2,1)S(1)}, u32[]{:S(2)}, u32[]{:S(2)}) collective-permute-start(bf16[2,128,512]{2,1,0:T(8,128)(2,1)S(1)} %get-tuple-element.69), channel_id=1, source_target_pairs={{0,8},{1,9},{2,10},{3,11},{4,12},{5,13},{6,14},{7,15},{8,0},{9,1},... | collective-permute-start | bytes 786440 | tf_op jit(solution)/shard_map/ppermute | solution.py:167
  10.4 9.3 %collective-permute-done.1 = bf16[2,128,512]{2,1,0:T(8,128)(2,1)S(1)} collective-permute-done((bf16[2,128,512]{2,1,0:T(8,128)(2,1)S(1)}, bf16[2,128,512]{2,1,0:T(8,128)(2,1)S(1)}, u32[]{:S(2)}, u32[]{:S(2)}) %collective-permute-start.1) | collective-permute-done | bytes 262176 | tf_op jit(solution)/shard_map/ppermute | solution.py:167
  19.6 1.5 %collective-permute-start.3 = (bf16[2,128,512]{2,1,0:T(8,128)(2,1)S(1)}, bf16[2,128,512]{2,1,0:T(8,128)(2,1)S(1)}, u32[]{:S(2)}, u32[]{:S(2)}) collective-permute-start(bf16[2,128,512]{2,1,0:T(8,128)(2,1)S(1)} %collective-permute-done.1), channel_id=1, source_target_pairs={{0,4},{1,3},{2,6},{3,1},{4,0},{5,7},{6,2},{7,5},{8,12},{9,11},{10,... | collective-permute-start | bytes 786440 | tf_op jit(solution)/shard_map/ppermute | solution.py:167
  21.2 0.0 collective-permute-done.12
  21.2 0.6 collective-permute-start.13
  21.8 0.1 pad_maximum_fusion.3.refs_0_
  21.9 1.5 %collective-permute-start.17 = (bf16[2,2,128,512]{3,2,1,0:T(8,128)(2,1)S(1)}, bf16[2,2,128,512]{3,2,1,0:T(8,128)(2,1)S(1)}, u32[]{:S(2)}, u32[]{:S(2)}) collective-permute-start(bf16[2,2,128,512]{3,2,1,0:T(8,128)(2,1)S(1)} %pad_maximum_fusion.3.refs_0_), channel_id=1, source_target_pairs={{0,2},{1,5},{2,0},{3,7},{4,6},{5,1},{6,4},{7,3},{8,10},{9,13},{10,... | collective-permute-start | bytes 1572872 | tf_op jit(solution)/shard_map/ppermute | solution.py:167
  23.4 0.0 collective-permute-start.18
  23.4 0.0 collective-permute-done.11
  23.4 1.4 %collective-permute-start.2 = (bf16[2,128,512]{2,1,0:T(8,128)(2,1)S(1)}, bf16[2,128,512]{2,1,0:T(8,128)(2,1)S(1)}, u32[]{:S(2)}, u32[]{:S(2)}) collective-permute-start(bf16[2,128,512]{2,1,0:T(8,128)(2,1)S(1)} %collective-permute-done.1), channel_id=1, source_target_pairs={{0,8},{1,9},{2,10},{3,11},{4,12},{5,13},{6,14},{7,15},{8,0},{9,1},... | collective-permute-start | bytes 786440 | tf_op jit(solution)/shard_map/ppermute | solution.py:167
  24.9 3.2 %collective-permute-done.3 = bf16[2,128,512]{2,1,0:T(8,128)(2,1)S(1)} collective-permute-done((bf16[2,128,512]{2,1,0:T(8,128)(2,1)S(1)}, bf16[2,128,512]{2,1,0:T(8,128)(2,1)S(1)}, u32[]{:S(2)}, u32[]{:S(2)}) %collective-permute-start.3) | collective-permute-done | bytes 262176 | tf_op jit(solution)/shard_map/ppermute | solution.py:167
  28.1 0.7 collective-permute-start.4
  28.8 1.5 %collective-permute-done.13 = bf16[2,128,512]{2,1,0:T(8,128)(2,1)S(1)} collective-permute-done((bf16[2,128,512]{2,1,0:T(8,128)(2,1)S(1)}, bf16[2,128,512]{2,1,0:T(8,128)(2,1)S(1)}, u32[]{:S(2)}, u32[]{:S(2)}) %collective-permute-start.13) | collective-permute-done | bytes 262176 | tf_op jit(solution)/shard_map/ppermute | solution.py:167
  30.3 0.1 pad_maximum_fusion.2.refs_0_
  30.3 1.0 %collective-permute-start.14 = (bf16[2,2,128,512]{3,2,1,0:T(8,128)(2,1)S(1)}, bf16[2,2,128,512]{3,2,1,0:T(8,128)(2,1)S(1)}, u32[]{:S(2)}, u32[]{:S(2)}) collective-permute-start(bf16[2,2,128,512]{3,2,1,0:T(8,128)(2,1)S(1)} %pad_maximum_fusion.2.refs_0_), channel_id=1, source_target_pairs={{0,2},{1,5},{2,0},{3,7},{4,6},{5,1},{6,4},{7,3},{8,10},{9,13},{10,... | collective-permute-start | bytes 1572872 | tf_op jit(solution)/shard_map/ppermute | solution.py:167
  31.3 0.1 pad_maximum_fusion.1.refs_0_
  31.3 4.5 %collective-permute-done.2 = bf16[2,128,512]{2,1,0:T(8,128)(2,1)S(1)} collective-permute-done((bf16[2,128,512]{2,1,0:T(8,128)(2,1)S(1)}, bf16[2,128,512]{2,1,0:T(8,128)(2,1)S(1)}, u32[]{:S(2)}, u32[]{:S(2)}) %collective-permute-start.2) | collective-permute-done | bytes 262176 | tf_op jit(solution)/shard_map/ppermute | solution.py:167
  35.9 0.0 collective-permute-start.15
  35.9 3.7 %collective-permute-done.4 = bf16[2,128,512]{2,1,0:T(8,128)(2,1)S(1)} collective-permute-done((bf16[2,128,512]{2,1,0:T(8,128)(2,1)S(1)}, bf16[2,128,512]{2,1,0:T(8,128)(2,1)S(1)}, u32[]{:S(2)}, u32[]{:S(2)}) %collective-permute-start.4) | collective-permute-done | bytes 262176 | tf_op jit(solution)/shard_map/ppermute | solution.py:167
  39.6 0.7 %collective-permute-start.8 = (bf16[2,2,128,512]{3,2,1,0:T(8,128)(2,1)S(1)}, bf16[2,2,128,512]{3,2,1,0:T(8,128)(2,1)S(1)}, u32[]{:S(2)}, u32[]{:S(2)}) collective-permute-start(bf16[2,2,128,512]{3,2,1,0:T(8,128)(2,1)S(1)} %pad_maximum_fusion.1.refs_0_), channel_id=1, source_target_pairs={{0,2},{1,5},{2,0},{3,7},{4,6},{5,1},{6,4},{7,3},{8,10},{9,13},{10,... | collective-permute-start | bytes 1572872 | tf_op jit(solution)/shard_map/ppermute | solution.py:167
  40.4 0.1 pad_maximum_fusion.refs_0_
  40.4 0.0 collective-permute-done.17.refs_1_
  40.4 0.1 collective-permute-start.19
  40.5 0.0 collective-permute-done.18.refs_2_
  40.5 1.4 %collective-permute-start.5 = (bf16[2,2,128,512]{3,2,1,0:T(8,128)(2,1)S(1)}, bf16[2,2,128,512]{3,2,1,0:T(8,128)(2,1)S(1)}, u32[]{:S(2)}, u32[]{:S(2)}) collective-permute-start(bf16[2,2,128,512]{3,2,1,0:T(8,128)(2,1)S(1)} %pad_maximum_fusion.refs_0_), channel_id=1, source_target_pairs={{0,2},{1,5},{2,0},{3,7},{4,6},{5,1},{6,4},{7,3},{8,10},{9,13},{10,... | collective-permute-start | bytes 1572872 | tf_op jit(solution)/shard_map/ppermute | solution.py:167
  41.9 0.0 collective-permute-done.14.refs_1_
  41.9 0.1 collective-permute-start.16
  42.0 0.0 collective-permute-done.15.refs_2_
  42.0 0.4 collective-permute-start.9
  42.4 6.4 %collective-permute-done.8.refs_1_ = bf16[2,2,128,512]{3,2,1,0:T(8,128)(2,1)S(1)} collective-permute-done((bf16[2,2,128,512]{3,2,1,0:T(8,128)(2,1)S(1)}, bf16[2,2,128,512]{3,2,1,0:T(8,128)(2,1)S(1)}, u32[]{:S(2)}, u32[]{:S(2)}) %collective-permute-start.8) | collective-permute-done | bytes 524320 | tf_op jit(solution)/shard_map/ppermute | solution.py:167
  48.8 0.0 collective-permute-start.10
  48.8 0.0 collective-permute-done.19.refs_3_
  48.8 0.5 collective-permute-start.6
  49.3 5.1 %collective-permute-done.5.refs_1_ = bf16[2,2,128,512]{3,2,1,0:T(8,128)(2,1)S(1)} collective-permute-done((bf16[2,2,128,512]{3,2,1,0:T(8,128)(2,1)S(1)}, bf16[2,2,128,512]{3,2,1,0:T(8,128)(2,1)S(1)}, u32[]{:S(2)}, u32[]{:S(2)}) %collective-permute-start.5) | collective-permute-done | bytes 524320 | tf_op jit(solution)/shard_map/ppermute | solution.py:167
  54.4 0.0 collective-permute-start.7
  54.4 2.7 %shard_map.256 = (f32[2048,2048]{1,0:T(8,128)S(1)}, f32[256,2048]{1,0:T(8,128)S(1)}, f32[256,2048]{1,0:T(8,128)S(1)}) custom-call(bf16[2,2,128,512]{3,2,1,0:T(8,128)(2,1)S(1)} %pad_maximum_fusion.3.refs_0_, bf16[2,2,128,512]{3,2,1,0:T(8,128)(2,1)S(1)} %collective-permute-done.17.refs_1_, bf16[2,2,128,512]{3,2,1,0:T(8,128)(2,1)S(1)} %collective-permute-done.18.refs_2_, ...), custom_call_target="tpu_custom_call" | custom-call | tf_op jit(solution)/shard_map/pallas_call | solution.py:456
  57.2 0.0 collective-permute-done.16.refs_3_
  57.2 2.8 %shard_map.257 = (f32[2048,2048]{1,0:T(8,128)S(1)}, bf16[256,2048]{1,0:T(8,128)(2,1)S(1)}, f32[256,256]{1,0:T(8,128)S(1)}, f32[256,256]{1,0:T(8,128)S(1)}, f32[2...) custom-call(bf16[2,2,128,512]{3,2,1,0:T(8,128)(2,1)S(1)} %pad_maximu, ...), custom_call_target="tpu_custom_call", output_to_operand_aliasing={{0}: (4, {})} | custom-call | tf_op jit(solution)/shard_map/pallas_call | solution.py:456
  60.0 0.0 collective-permute-done.9.refs_2_
  60.0 0.0 collective-permute-done.10.refs_3_
  60.0 2.7 %shard_map.258.refs_4_ = f32[2048,2048]{1,0:T(8,128)S(1)} custom-call(bf16[2,2,128,512]{3,2,1,0:T(8,128)(2,1)S(1)} %pad_maximum_fusion.1.refs_0_, bf16[2,2,128,512]{3,2,1,0:T(8,128)(2,1)S(1)} %collective-permute-done.8.refs_1_, bf16[2,2,128,512]{3,2,1,0:T(8,128)(2,1)S(1)} %collective-permute-done.9.refs_2_, ...), custom_call_target="tpu_custom_call", output_to_operand_aliasing={{}: (4, {})} | custom-call | tf_op jit(solution)/shard_map/pallas_call | solution.py:456
  62.8 0.0 collective-permute-done.6.refs_2_
  62.8 8.2 %tail.1 = (f32[256,256]{1,0:T(8,128)}, bf16[256,256]{1,0:T(8,128)(2,1)}, f32[256,256]{1,0:T(8,128)}, f32[256,256]{1,0:T(8,128)}, f32[256,2048]{1,0:T(8,128)}, /*...) custom-call(bf16[2,2,128,512]{3,2,1,0:T(8,128)(2,1)S(1)} %pad_maximu, ...), custom_call_target="tpu_custom_call" | custom-call | tf_op jit(solution)/shard_map/tail/pallas_call | solution.py:472
  (2 shorter events, 0.0 us)
Async XLA Ops:
  1.7 1.5 %collective-permute-start = (bf16[128,512]{1,0:T(8,128)(2,1)S(1)}, bf16[128,512]{1,0:T(8,128)(2,1)S(1)}, u32[]{:S(2)}, u32[]{:S(2)}) collective-permute-start(bf16[128,512]{1,0:T(8,128)(2,1)S(1)} %get-tuple-element.41), channel_id=1, source_target_pairs={{0,1},{1,0},{2,3},{3,2},{4,5},{5,4},{6,7},{7,6},{8,9},{9,8},{10,11... | collective-permute-start | bytes 393224 | tf_op jit(solution)/shard_map/ppermute | solution.py:167
  3.3 16.3 %collective-permute-start.1 = (bf16[2,128,512]{2,1,0:T(8,128)(2,1)S(1)}, bf16[2,128,512]{2,1,0:T(8,128)(2,1)S(1)}, u32[]{:S(2)}, u32[]{:S(2)}) collective-permute-start(bf16[2,128,512]{2,1,0:T(8,128)(2,1)S(1)} %get-tuple-element.69), channel_id=1, source_target_pairs={{0,16},{1,17},{2,18},{3,19},{4,20},{5,21},{6,22},{7,23},{8,24},{9,... | collective-permute-start | bytes 786440 | tf_op jit(solution)/shard_map/ppermute | solution.py:167
  7.3 13.9 %collective-permute-start.12 = (bf16[2,128,512]{2,1,0:T(8,128)(2,1)S(1)}, bf16[2,128,512]{2,1,0:T(8,128)(2,1)S(1)}, u32[]{:S(2)}, u32[]{:S(2)}) collective-permute-start(bf16[2,128,512]{2,1,0:T(8,128)(2,1)S(1)} %get-tuple-element.69), channel_id=1, source_target_pairs={{0,4},{1,3},{2,6},{3,1},{4,0},{5,7},{6,2},{7,5},{8,12},{9,11},{10,... | collective-permute-start | bytes 786440 | tf_op jit(solution)/shard_map/ppermute | solution.py:167
  8.8 14.6 %collective-permute-start.11 = (bf16[2,128,512]{2,1,0:T(8,128)(2,1)S(1)}, bf16[2,128,512]{2,1,0:T(8,128)(2,1)S(1)}, u32[]{:S(2)}, u32[]{:S(2)}) collective-permute-start(bf16[2,128,512]{2,1,0:T(8,128)(2,1)S(1)} %get-tuple-element.69), channel_id=1, source_target_pairs={{0,8},{1,9},{2,10},{3,11},{4,12},{5,13},{6,14},{7,15},{8,0},{9,1},... | collective-permute-start | bytes 786440 | tf_op jit(solution)/shard_map/ppermute | solution.py:167
  19.6 8.4 %collective-permute-start.3 = (bf16[2,128,512]{2,1,0:T(8,128)(2,1)S(1)}, bf16[2,128,512]{2,1,0:T(8,128)(2,1)S(1)}, u32[]{:S(2)}, u32[]{:S(2)}) collective-permute-start(bf16[2,128,512]{2,1,0:T(8,128)(2,1)S(1)} %collective-permute-done.1), channel_id=1, source_target_pairs={{0,4},{1,3},{2,6},{3,1},{4,0},{5,7},{6,2},{7,5},{8,12},{9,11},{10,... | collective-permute-start | bytes 786440 | tf_op jit(solution)/shard_map/ppermute | solution.py:167
  21.2 9.1 %collective-permute-start.13 = (bf16[2,128,512]{2,1,0:T(8,128)(2,1)S(1)}, bf16[2,128,512]{2,1,0:T(8,128)(2,1)S(1)}, u32[]{:S(2)}, u32[]{:S(2)}) collective-permute-start(bf16[2,128,512]{2,1,0:T(8,128)(2,1)S(1)} %collective-permute-done.12), channel_id=1, source_target_pairs={{0,8},{1,9},{2,10},{3,11},{4,12},{5,13},{6,14},{7,15},{8,0},{9,1},... | collective-permute-start | bytes 786440 | tf_op jit(solution)/shard_map/ppermute | solution.py:167
  21.9 18.5 %collective-permute-start.17 = (bf16[2,2,128,512]{3,2,1,0:T(8,128)(2,1)S(1)}, bf16[2,2,128,512]{3,2,1,0:T(8,128)(2,1)S(1)}, u32[]{:S(2)}, u32[]{:S(2)}) collective-permute-start(bf16[2,2,128,512]{3,2,1,0:T(8,128)(2,1)S(1)} %pad_maximum_fusion.3.refs_0_), channel_id=1, source_target_pairs={{0,2},{1,5},{2,0},{3,7},{4,6},{5,1},{6,4},{7,3},{8,10},{9,13},{10,... | collective-permute-start | bytes 1572872 | tf_op jit(solution)/shard_map/ppermute | solution.py:167
  23.4 17.1 %collective-permute-start.18 = (bf16[2,2,128,512]{3,2,1,0:T(8,128)(2,1)S(1)}, bf16[2,2,128,512]{3,2,1,0:T(8,128)(2,1)S(1)}, u32[]{:S(2)}, u32[]{:S(2)}) collective-permute-start(bf16[2,2,128,512]{3,2,1,0:T(8,128)(2,1)S(1)} %pad_maximum_fusion.3.refs_0_), channel_id=1, source_target_pairs={{0,1},{1,0},{2,3},{3,2},{4,5},{5,4},{6,7},{7,6},{8,9},{9,8},{10,11... | collective-permute-start | bytes 1572872 | tf_op jit(solution)/shard_map/ppermute | solution.py:167
  23.4 12.5 %collective-permute-start.2 = (bf16[2,128,512]{2,1,0:T(8,128)(2,1)S(1)}, bf16[2,128,512]{2,1,0:T(8,128)(2,1)S(1)}, u32[]{:S(2)}, u32[]{:S(2)}) collective-permute-start(bf16[2,128,512]{2,1,0:T(8,128)(2,1)S(1)} %collective-permute-done.1), channel_id=1, source_target_pairs={{0,8},{1,9},{2,10},{3,11},{4,12},{5,13},{6,14},{7,15},{8,0},{9,1},... | collective-permute-start | bytes 786440 | tf_op jit(solution)/shard_map/ppermute | solution.py:167
  28.1 11.6 %collective-permute-start.4 = (bf16[2,128,512]{2,1,0:T(8,128)(2,1)S(1)}, bf16[2,128,512]{2,1,0:T(8,128)(2,1)S(1)}, u32[]{:S(2)}, u32[]{:S(2)}) collective-permute-start(bf16[2,128,512]{2,1,0:T(8,128)(2,1)S(1)} %collective-permute-done.3), channel_id=1, source_target_pairs={{0,8},{1,9},{2,10},{3,11},{4,12},{5,13},{6,14},{7,15},{8,0},{9,1},... | collective-permute-start | bytes 786440 | tf_op jit(solution)/shard_map/ppermute | solution.py:167
  30.3 11.6 %collective-permute-start.14 = (bf16[2,2,128,512]{3,2,1,0:T(8,128)(2,1)S(1)}, bf16[2,2,128,512]{3,2,1,0:T(8,128)(2,1)S(1)}, u32[]{:S(2)}, u32[]{:S(2)}) collective-permute-start(bf16[2,2,128,512]{3,2,1,0:T(8,128)(2,1)S(1)} %pad_maximum_fusion.2.refs_0_), channel_id=1, source_target_pairs={{0,2},{1,5},{2,0},{3,7},{4,6},{5,1},{6,4},{7,3},{8,10},{9,13},{10,... | collective-permute-start | bytes 1572872 | tf_op jit(solution)/shard_map/ppermute | solution.py:167
  35.9 6.1 %collective-permute-start.15 = (bf16[2,2,128,512]{3,2,1,0:T(8,128)(2,1)S(1)}, bf16[2,2,128,512]{3,2,1,0:T(8,128)(2,1)S(1)}, u32[]{:S(2)}, u32[]{:S(2)}) collective-permute-start(bf16[2,2,128,512]{3,2,1,0:T(8,128)(2,1)S(1)} %pad_maximum_fusion.2.refs_0_), channel_id=1, source_target_pairs={{0,1},{1,0},{2,3},{3,2},{4,5},{5,4},{6,7},{7,6},{8,9},{9,8},{10,11... | collective-permute-start | bytes 1572872 | tf_op jit(solution)/shard_map/ppermute | solution.py:167
  39.6 9.2 %collective-permute-start.8 = (bf16[2,2,128,512]{3,2,1,0:T(8,128)(2,1)S(1)}, bf16[2,2,128,512]{3,2,1,0:T(8,128)(2,1)S(1)}, u32[]{:S(2)}, u32[]{:S(2)}) collective-permute-start(bf16[2,2,128,512]{3,2,1,0:T(8,128)(2,1)S(1)} %pad_maximum_fusion.1.refs_0_), channel_id=1, source_target_pairs={{0,2},{1,5},{2,0},{3,7},{4,6},{5,1},{6,4},{7,3},{8,10},{9,13},{10,... | collective-permute-start | bytes 1572872 | tf_op jit(solution)/shard_map/ppermute | solution.py:167
  40.4 8.4 %collective-permute-start.19 = (bf16[2,2,128,512]{3,2,1,0:T(8,128)(2,1)S(1)}, bf16[2,2,128,512]{3,2,1,0:T(8,128)(2,1)S(1)}, u32[]{:S(2)}, u32[]{:S(2)}) collective-permute-start(bf16[2,2,128,512]{3,2,1,0:T(8,128)(2,1)S(1)} %collective-permute-done.17.refs_1_), channel_id=1, source_target_pairs={{0,1},{1,0},{2,3},{3,2},{4,5},{5,4},{6,7},{7,6},{8,9},{9,8},{10,11... | collective-permute-start | bytes 1572872 | tf_op jit(solution)/shard_map/ppermute | solution.py:167
  40.5 13.9 %collective-permute-start.5 = (bf16[2,2,128,512]{3,2,1,0:T(8,128)(2,1)S(1)}, bf16[2,2,128,512]{3,2,1,0:T(8,128)(2,1)S(1)}, u32[]{:S(2)}, u32[]{:S(2)}) collective-permute-start(bf16[2,2,128,512]{3,2,1,0:T(8,128)(2,1)S(1)} %pad_maximum_fusion.refs_0_), channel_id=1, source_target_pairs={{0,2},{1,5},{2,0},{3,7},{4,6},{5,1},{6,4},{7,3},{8,10},{9,13},{10,... | collective-permute-start | bytes 1572872 | tf_op jit(solution)/shard_map/ppermute | solution.py:167
  41.9 15.3 %collective-permute-start.16 = (bf16[2,2,128,512]{3,2,1,0:T(8,128)(2,1)S(1)}, bf16[2,2,128,512]{3,2,1,0:T(8,128)(2,1)S(1)}, u32[]{:S(2)}, u32[]{:S(2)}) collective-permute-start(bf16[2,2,128,512]{3,2,1,0:T(8,128)(2,1)S(1)} %collective-permute-done.14.refs_1_), channel_id=1, source_target_pairs={{0,1},{1,0},{2,3},{3,2},{4,5},{5,4},{6,7},{7,6},{8,9},{9,8},{10,11... | collective-permute-start | bytes 1572872 | tf_op jit(solution)/shard_map/ppermute | solution.py:167
  42.0 18.0 %collective-permute-start.9 = (bf16[2,2,128,512]{3,2,1,0:T(8,128)(2,1)S(1)}, bf16[2,2,128,512]{3,2,1,0:T(8,128)(2,1)S(1)}, u32[]{:S(2)}, u32[]{:S(2)}) collective-permute-start(bf16[2,2,128,512]{3,2,1,0:T(8,128)(2,1)S(1)} %pad_maximum_fusion.1.refs_0_), channel_id=1, source_target_pairs={{0,1},{1,0},{2,3},{3,2},{4,5},{5,4},{6,7},{7,6},{8,9},{9,8},{10,11... | collective-permute-start | bytes 1572872 | tf_op jit(solution)/shard_map/ppermute | solution.py:167
  48.8 11.2 %collective-permute-start.10 = (bf16[2,2,128,512]{3,2,1,0:T(8,128)(2,1)S(1)}, bf16[2,2,128,512]{3,2,1,0:T(8,128)(2,1)S(1)}, u32[]{:S(2)}, u32[]{:S(2)}) collective-permute-start(bf16[2,2,128,512]{3,2,1,0:T(8,128)(2,1)S(1)} %collective-permute-done.8.refs_1_), channel_id=1, source_target_pairs={{0,1},{1,0},{2,3},{3,2},{4,5},{5,4},{6,7},{7,6},{8,9},{9,8},{10,11... | collective-permute-start | bytes 1572872 | tf_op jit(solution)/shard_map/ppermute | solution.py:167
  48.8 14.0 %collective-permute-start.6 = (bf16[2,2,128,512]{3,2,1,0:T(8,128)(2,1)S(1)}, bf16[2,2,128,512]{3,2,1,0:T(8,128)(2,1)S(1)}, u32[]{:S(2)}, u32[]{:S(2)}) collective-permute-start(bf16[2,2,128,512]{3,2,1,0:T(8,128)(2,1)S(1)} %pad_maximum_fusion.refs_0_), channel_id=1, source_target_pairs={{0,1},{1,0},{2,3},{3,2},{4,5},{5,4},{6,7},{7,6},{8,9},{9,8},{10,11... | collective-permute-start | bytes 1572872 | tf_op jit(solution)/shard_map/ppermute | solution.py:167
  54.4 8.4 %collective-permute-start.7 = (bf16[2,2,128,512]{3,2,1,0:T(8,128)(2,1)S(1)}, bf16[2,2,128,512]{3,2,1,0:T(8,128)(2,1)S(1)}, u32[]{:S(2)}, u32[]{:S(2)}) collective-permute-start(bf16[2,2,128,512]{3,2,1,0:T(8,128)(2,1)S(1)} %collective-permute-done.5.refs_1_), channel_id=1, source_target_pairs={{0,1},{1,0},{2,3},{3,2},{4,5},{5,4},{6,7},{7,6},{8,9},{9,8},{10,11... | collective-permute-start | bytes 1572872 | tf_op jit(solution)/shard_map/ppermute | solution.py:167
